TPU v7x, 512 devices: a whole 4x8x8 slice. The times are simulated.
512 devices in a mesh: sp: 32 (over z, x), tp: 16 (over y, core).
Axes of the slice: x: 4, y: 8, z: 8, core: 2. Of those that a mesh axis runs over, the one named last changes fastest.
Arguments:
- residual: bfloat16 [16384, 2048], P('sp', 'tp'), may hold values from -64 to 64
- gains: float32 [2, 2, 2048], replicated, may hold values from 0.1 to 1.9
- w_query: bfloat16 [2, 2048, 2048], P(None, None, 'tp'), may hold values from -0.125 to 0.125
- w_key: bfloat16 [2, 2048, 2048], P(None, None, 'tp'), may hold values from -0.125 to 0.125
- w_value: bfloat16 [2, 2048, 2048], P(None, None, 'tp'), may hold values from -0.125 to 0.125
- w_out: bfloat16 [2, 2048, 2048], P(None, None, 'tp'), may hold values from -1 to 1
- rel_bias: float32 [2, 32, 257], P(None, 'tp'), may hold values from -6 to 300
Outputs:
- encoded: bfloat16 [16384, 2048], P('sp', 'tp')
All inputs are finite; a program needn't handle non-finite values.
Results may differ from a plain program's by a relative error of at most 0.0058.
Values may be sent and summed in bfloat16 or wider, within the bound.
No kernel may reach another device: no remote copies, remote signals or barrier semaphores. Data moves between devices by JAX's collectives and lax.ppermute only.
A program may use at most 64 MiB of HBM per device.

v0:
```python
import jax
import jax.numpy as jnp
from jax import lax
from jax.sharding import Mesh
from jax.sharding import PartitionSpec as P

D = 2048
HEAD = 64
SEG = 64
LEFT = 8
MAXREL = 128
TP = ("tp_0", "tp_1")


norm_eps = 1e-06


def passed_along(value, axis, steps):
    count = lax.axis_size(axis)
    first, last = (max(0, -steps), min(count, count - steps))
    return lax.ppermute(value, axis, [(source, source + steps) for source in range(first, last)])


def gathered_by_axis(value, axes, dim):
    filled = value
    for number in range(len(axes) - 1, -1, -1):
        filled = lax.all_gather(filled, axes[number], axis=dim, tiled=True)
    return filled


def copy_for_each(value, axis):
    copies = jnp.broadcast_to(value, (lax.axis_size(axis), *value.shape))
    return lax.all_to_all(copies, axis, split_axis=0, concat_axis=0, tiled=True)


def over_copies(value, axis):
    everything = copy_for_each(value, axis)
    return jnp.sum(everything, axis=0)


def project(stream, gain_pre, weight_q, weight_k, weight_v):
    full_rows = lax.all_gather(stream, TP, axis=1, tiled=True)
    widened = full_rows.astype(jnp.float32)
    inv_rms = lax.rsqrt(jnp.mean(widened * widened, axis=1, keepdims=True) + norm_eps)
    normed = (widened * inv_rms * gain_pre).astype(jnp.bfloat16)
    return tuple(
        (
            jnp.dot(normed, weight, preferred_element_type=jnp.float32).astype(jnp.bfloat16)
            for weight in (weight_q, weight_k, weight_v)
        )
    )


def bias_rows(bias_table, reach_rows, key_span):
    head_count = bias_table.shape[0]
    repeats = reach_rows + 127 - MAXREL
    tail = jnp.broadcast_to(bias_table[:, -1:], (head_count, repeats))
    extended = jnp.concatenate([bias_table[:, MAXREL - 127 :], tail], axis=1)
    reversed_table = extended[:, ::-1]
    length = reversed_table.shape[1]
    tiled = jnp.tile(reversed_table, (1, 128))
    skewed = tiled[:, 127 : 127 + 128 * (length - 1)].reshape(head_count, 128, length - 1)
    return skewed[:, :, :key_span]


def attend(queries, key_rows, value_rows, bias_table, first_pos):
    reach_rows = LEFT * SEG
    key_span = reach_rows + 128
    query_count = queries.shape[0]
    sub_count = query_count // 128
    head_count = queries.shape[1] // HEAD
    window_blocks = key_span // 128
    query_sub = queries.reshape(sub_count, 128, head_count, HEAD)
    key_blocks = key_rows.reshape(sub_count + window_blocks - 1, 128, queries.shape[1])
    value_blocks = value_rows.reshape(sub_count + window_blocks - 1, 128, queries.shape[1])
    key_window = jnp.concatenate(
        [key_blocks[offset_blk : offset_blk + sub_count] for offset_blk in range(window_blocks)],
        axis=1,
    )
    value_window = jnp.concatenate(
        [value_blocks[offset_blk : offset_blk + sub_count] for offset_blk in range(window_blocks)],
        axis=1,
    )
    key_window = key_window.reshape(sub_count, key_span, head_count, HEAD)
    value_window = value_window.reshape(sub_count, key_span, head_count, HEAD)
    scores = jnp.einsum(
        "nqhd,nkhd->nhqk", query_sub, key_window, preferred_element_type=jnp.float32
    ) * HEAD ** (-0.5)
    row_idx = jnp.arange(128, dtype=jnp.int32)[:, None]
    col_idx = jnp.arange(key_span, dtype=jnp.int32)[None, :]
    rel_terms = bias_rows(bias_table, reach_rows, key_span)
    block_base = first_pos + jnp.arange(sub_count, dtype=jnp.int32)[:, None, None] * 128
    query_pos = block_base + row_idx[None]
    key_pos = block_base - reach_rows + col_idx[None]
    seg_gap = jnp.floor_divide(query_pos, SEG) - jnp.floor_divide(key_pos, SEG)
    allowed = ((key_pos >= 0) | (query_pos < 0)) & (seg_gap >= 0) & (seg_gap <= LEFT)
    scores = jnp.where(allowed[:, None], scores + rel_terms[None], -jnp.inf)
    row_max = jnp.max(scores, axis=3, keepdims=True)
    weights_raw = jnp.exp(scores - row_max)
    prob_bf = (weights_raw / jnp.sum(weights_raw, axis=3, keepdims=True)).astype(jnp.bfloat16)
    result = jnp.einsum(
        "nhqk,nkhd->nqhd", prob_bf, value_window, preferred_element_type=jnp.float32
    )
    return result.astype(jnp.bfloat16).reshape(query_count, head_count * HEAD)


def on_device(residual, gains, w_query, w_key, w_value, w_out, rel_bias):
    tok_rows = residual.shape[0]
    columns = residual.shape[1]
    layer_count = w_query.shape[0]
    seq_start = lax.axis_index("sp") * tok_rows
    col_start = lax.axis_index(TP) * columns
    stream = residual
    for layer_idx in range(layer_count):
        queries, key_rows, value_rows = project(
            stream, gains[layer_idx, 0], w_query[layer_idx], w_key[layer_idx], w_value[layer_idx]
        )
        previous = passed_along((key_rows, value_rows), "sp", 1)
        key_rows = jnp.concatenate([previous[0], key_rows], axis=0)
        value_rows = jnp.concatenate([previous[1], value_rows], axis=0)
        attended = attend(queries, key_rows, value_rows, rel_bias[layer_idx], seq_start)
        all_heads = gathered_by_axis(attended, TP, 1)
        branch = jnp.dot(all_heads, w_out[layer_idx], preferred_element_type=jnp.float32)
        squares = over_copies(jnp.sum(branch * branch, axis=1), TP)
        inv_rms = lax.rsqrt(squares / D + norm_eps)
        own_gain = lax.dynamic_slice_in_dim(gains[layer_idx, 1], col_start, columns, 0)
        carried = stream
        stream = (carried.astype(jnp.float32) + branch * inv_rms[:, None] * own_gain).astype(
            jnp.bfloat16
        )
    return stream


def solution(mesh):
    finer = Mesh(mesh.devices.reshape(mesh.shape["sp"], 8, 2), ("sp", "tp_0", "tp_1"))
    in_specs = (
        P("sp", TP),
        P(),
        P(None, None, TP),
        P(None, None, TP),
        P(None, None, TP),
        P(None, None, TP),
        P(None, TP, None),
    )
    out_specs = P("sp", TP)
    return jax.shard_map(
        on_device, mesh=finer, in_specs=in_specs, out_specs=out_specs, check_vma=False
    )
```

profile of v0, /device:TPU:1, one launch (start us, length us, event | category | flops | bytes accessed | tf_op | source)
XLA Modules:
  0.0 278.0 jit_solution(1145219755789919648)
XLA Ops:
  6.5 0.7 all-gather.5.cloned.1.call-update
  7.3 0.7 slice_bitcast_fusion
  8.1 0.1 slice_reduce_fusion
  8.3 0.5 reverse
  9.0 1.1 tile.9
  10.1 0.9 slice.174
  11.0 1.1 reshape.308
  12.4 0.5 fusion.19
  13.0 45.4 %all-gather.5.cloned.1.call-done = bf16[512,2048]{1,0:T(8,128)(2,1)} async-done(((bf16[512,128]{1,0:T(8,128)(2,1)}), bf16[512,2048]{1,0:T(8,128)(2,1)}) %all-gather.5.cloned.1.call-update) | async-done | bytes 2097168 | tf_op jit(solution)/shard_map/all_gather | solution.py:42
  58.4 2.2 fusion.2
  60.7 0.5 fusion.4
  61.2 0.6 copy-done.9
  61.9 0.7 convolution_convert_fusion.5
  62.6 3.1 %collective-permute-start = (bf16[512,128]{1,0:T(8,128)(2,1)S(1)}, bf16[512,128]{1,0:T(8,128)(2,1)S(1)}, u32[]{:S(2)}, u32[]{:S(2)}) collective-permute-start(bf16[512,128]{1,0:T(8,128)(2,1)S(1)} %convolution_convert_fusion.5), channel_id=1, source_target_pairs={{0,16},{16,32},{32,48},{48,64},{64,80},{80,96},{96,112},{112,128},... | collective-permute-start | bytes 393224 | tf_op jit(solution)/shard_map/ppermute | solution.py:21
  65.7 0.7 convolution_convert_fusion.3
  66.4 0.7 convolution_convert_fusion.4
  67.3 3.1 %collective-permute-start.1 = (bf16[512,128]{1,0:T(8,128)(2,1)S(1)}, bf16[512,128]{1,0:T(8,128)(2,1)S(1)}, u32[]{:S(2)}, u32[]{:S(2)}) collective-permute-start(bf16[512,128]{1,0:T(8,128)(2,1)S(1)} %convolution_convert_fusion.3), channel_id=1, source_target_pairs={{0,16},{16,32},{32,48},{48,64},{64,80},{80,96},{96,112},{112,128},... | collective-permute-start | bytes 393224 | tf_op jit(solution)/shard_map/ppermute | solution.py:21
  70.8 0.1 reshape.318
  71.6 0.1 reshape.315
  72.2 0.7 constant_dynamic-update-slice_fusion.4
  73.5 0.1 reshape.321
  74.1 0.7 constant_dynamic-update-slice_fusion.3
  74.8 0.7 constant_dynamic-update-slice_fusion.2
  75.5 0.7 constant_dynamic-update-slice_fusion.1
  76.1 0.7 constant_dynamic-update-slice_fusion
  77.0 2.6 fusion.80
  79.6 2.5 fusion.24
  82.2 3.0 %all_gather.19 = bf16[512,256]{0,1:T(8,128)(2,1)} all-gather(bf16[512,128]{0,1:T(8,128)(2,1)S(1)} %bitcast.70), channel_id=1, replica_groups=mesh['sp'=32,'tp_0'=8,'tp_1'=2] {'tp_1'}, dimensions={1}, use_global_device_ids=true | all-gather | bytes 393216 | tf_op jit(solution)/shard_map/all_gather | solution.py:27
  85.4 40.2 %all-gather.7.cloned.1.call-done = bf16[512,2048]{0,1:T(8,128)(2,1)} async-done(((bf16[512,256]{0,1:T(8,128)(2,1)}), bf16[512,2048]{0,1:T(8,128)(2,1)}) %all-gather.7.cloned.1.call-update) | async-done | bytes 2097168 | tf_op jit(solution)/shard_map/all_gather | solution.py:27
  125.6 2.2 multiply_reduce_fusion.1
  127.8 0.6 broadcast_in_dim.56
  128.4 9.0 %all-to-all-start = ((f32[16,1,512]{2,1,0:T(1,128)}), f32[16,1,512]{2,1,0:T(1,128)S(1)}, u32[]{:S(2)}, u32[]{:S(2)}) async-start(f32[16,1,512]{2,1,0:T(1,128)} %broadcast_in_dim.56), calls=%async_computation | async-start | bytes 65536 | tf_op jit(solution)/shard_map/all_to_all | solution.py:33
  137.5 7.3 %all-to-all-done = f32[16,1,512]{2,1,0:T(1,128)S(1)} async-done(((f32[16,1,512]{2,1,0:T(1,128)}), f32[16,1,512]{2,1,0:T(1,128)S(1)}, u32[]{:S(2)}, u32[]{:S(2)}) %all-to-all-start) | async-done | bytes 32800 | tf_op jit(solution)/shard_map/all_to_all | solution.py:33
  144.9 0.8 add_convert_fusion.1
  145.9 0.5 reverse.1
  146.6 1.1 tile.21
  147.7 0.9 slice.186
  148.6 1.1 reshape.311
  149.7 34.7 %all-gather.9.cloned.1.call-done = bf16[512,2048]{0,1:T(8,128)(2,1)} async-done(((bf16[512,128]{0,1:T(8,128)(2,1)}), bf16[512,2048]{0,1:T(8,128)(2,1)}) %all-gather.9.cloned.1.call-update) | async-done | bytes 2097168 | tf_op jit(solution)/shard_map/all_gather | solution.py:42
  184.4 2.2 fusion.5
  186.7 0.5 fusion.7
  187.2 0.6 copy-done.10
  187.9 0.8 convolution_convert_fusion.2
  188.6 0.8 convolution_convert_fusion
  189.4 3.1 %collective-permute-start.2 = (bf16[512,128]{1,0:T(8,128)(2,1)S(1)}, bf16[512,128]{1,0:T(8,128)(2,1)S(1)}, u32[]{:S(2)}, u32[]{:S(2)}) collective-permute-start(bf16[512,128]{1,0:T(8,128)(2,1)S(1)} %convolution_convert_fusion.2), channel_id=1, source_target_pairs={{0,16},{16,32},{32,48},{48,64},{64,80},{80,96},{96,112},{112,128},... | collective-permute-start | bytes 393224 | tf_op jit(solution)/shard_map/ppermute | solution.py:21
  192.5 0.8 convolution_convert_fusion.1
  193.4 3.1 %collective-permute-start.3 = (bf16[512,128]{1,0:T(8,128)(2,1)S(1)}, bf16[512,128]{1,0:T(8,128)(2,1)S(1)}, u32[]{:S(2)}, u32[]{:S(2)}) collective-permute-start(bf16[512,128]{1,0:T(8,128)(2,1)S(1)} %convolution_convert_fusion), channel_id=1, source_target_pairs={{0,16},{16,32},{32,48},{48,64},{64,80},{80,96},{96,112},{112,128},... | collective-permute-start | bytes 393224 | tf_op jit(solution)/shard_map/ppermute | solution.py:21
  196.8 0.1 copy.173
  197.7 0.1 reshape.326
  198.3 0.7 constant_dynamic-update-slice_fusion.14
  200.0 0.1 reshape.333
  200.3 0.7 constant_dynamic-update-slice_fusion.13
  200.9 0.7 constant_dynamic-update-slice_fusion.12
  201.6 0.7 constant_dynamic-update-slice_fusion.11
  202.3 0.7 constant_dynamic-update-slice_fusion.10
  203.2 2.6 fusion.83
  205.8 2.5 fusion.25
  208.5 3.0 %all_gather.22 = bf16[512,256]{0,1:T(8,128)(2,1)} all-gather(bf16[512,128]{0,1:T(8,128)(2,1)S(1)} %bitcast.71), channel_id=1, replica_groups=mesh['sp'=32,'tp_0'=8,'tp_1'=2] {'tp_1'}, dimensions={1}, use_global_device_ids=true | all-gather | bytes 393216 | tf_op jit(solution)/shard_map/all_gather | solution.py:27
  211.5 39.9 %all-gather.11.cloned.1.call-done = bf16[512,2048]{0,1:T(8,128)(2,1)} async-done(((bf16[512,256]{0,1:T(8,128)(2,1)}), bf16[512,2048]{0,1:T(8,128)(2,1)}) %all-gather.11.cloned.1.call-update) | async-done | bytes 2097168 | tf_op jit(solution)/shard_map/all_gather | solution.py:27
  251.4 2.1 multiply_reduce_fusion
  253.5 0.6 broadcast_in_dim.59
  254.1 9.0 %all-to-all-start.1 = ((f32[16,1,512]{2,1,0:T(1,128)}), f32[16,1,512]{2,1,0:T(1,128)S(1)}, u32[]{:S(2)}, u32[]{:S(2)}) async-start(f32[16,1,512]{2,1,0:T(1,128)} %broadcast_in_dim.59), calls=%async_computation.1 | async-start | bytes 65536 | tf_op jit(solution)/shard_map/all_to_all | solution.py:33
  263.2 7.4 %all-to-all-done.1 = f32[16,1,512]{2,1,0:T(1,128)S(1)} async-done(((f32[16,1,512]{2,1,0:T(1,128)}), f32[16,1,512]{2,1,0:T(1,128)S(1)}, u32[]{:S(2)}, u32[]{:S(2)}) %all-to-all-start.1) | async-done | bytes 32800 | tf_op jit(solution)/shard_map/all_to_all | solution.py:33
  270.7 0.8 copy.177
  (125 shorter events, 7.2 us)
Async XLA Ops:
  6.5 51.9 %all-gather.5.cloned.1.call-start = ((), (), s32[]{:S(2)}) async-start(), calls=%async_computation.2 | async-start | bytes 2228224 | tf_op jit(solution)/shard_map/all_gather | solution.py:42
  7.3 118.4 %all-gather.7.cloned.1.call-start = ((), (), s32[]{:S(2)}) async-start(), calls=%async_computation.3 | async-start | bytes 2359296 | tf_op jit(solution)/shard_map/all_gather | solution.py:27
  10.1 2.9 %copy-start.6 = (f32[2,2,2048]{2,1,0:T(2,128)S(1)}, f32[2,2,2048]{2,1,0:T(2,128)}, u32[]{:S(2)}) copy-start(f32[2,2,2048]{2,1,0:T(2,128)} %param.8) | copy-start | bytes 98308
  12.1 49.1 %copy-start.2 = (f32[2,128,766]{2,1,0:T(8,128)}, f32[2,128,766]{2,1,0:T(8,128)S(1)}, u32[]{:S(2)}) copy-start(f32[2,128,766]{2,1,0:T(8,128)S(1)} %reshape.308) | copy-start | bytes 2353156
  58.4 2.2 copy-start
  60.6 1.2 copy-start.9
  60.7 5.0 %copy-start.11 = (bf16[2,2048,128]{2,1,0:T(8,128)(2,1)S(1)}, bf16[2,2048,128]{2,1,0:T(8,128)(2,1)}, u32[]{:S(2)}) copy-start(bf16[2,2048,128]{2,1,0:T(8,128)(2,1)} %param.10) | copy-start | bytes 3145732
  61.9 4.5 %copy-start.13 = (bf16[2,2048,128]{2,1,0:T(8,128)(2,1)S(1)}, bf16[2,2048,128]{2,1,0:T(8,128)(2,1)}, u32[]{:S(2)}) copy-start(bf16[2,2048,128]{2,1,0:T(8,128)(2,1)} %param.9) | copy-start | bytes 3145732
  62.6 8.4 %collective-permute-start = (bf16[512,128]{1,0:T(8,128)(2,1)S(1)}, bf16[512,128]{1,0:T(8,128)(2,1)S(1)}, u32[]{:S(2)}, u32[]{:S(2)}) collective-permute-start(bf16[512,128]{1,0:T(8,128)(2,1)S(1)} %convolution_convert_fusion.5), channel_id=1, source_target_pairs={{0,16},{16,32},{32,48},{48,64},{64,80},{80,96},{96,112},{112,128},... | collective-permute-start | bytes 393224 | tf_op jit(solution)/shard_map/ppermute | solution.py:21
  67.3 5.6 %collective-permute-start.1 = (bf16[512,128]{1,0:T(8,128)(2,1)S(1)}, bf16[512,128]{1,0:T(8,128)(2,1)S(1)}, u32[]{:S(2)}, u32[]{:S(2)}) collective-permute-start(bf16[512,128]{1,0:T(8,128)(2,1)S(1)} %convolution_convert_fusion.3), channel_id=1, source_target_pairs={{0,16},{16,32},{32,48},{48,64},{64,80},{80,96},{96,112},{112,128},... | collective-permute-start | bytes 393224 | tf_op jit(solution)/shard_map/ppermute | solution.py:21
  73.2 3.8 %slice-start = ((f32[2,128,766]{2,1,0:T(8,128)}), f32[2,128,640]{2,1,0:T(8,128)S(1)}, s32[]{:S(2)}) async-start(f32[2,128,766]{2,1,0:T(8,128)} %copy-done.2), calls=%async_computation.6 | async-start | bytes 1310720 | tf_op jit(solution)/shard_map/slice | solution.py:63
  77.0 2.6 copy-start.7
  79.6 5.6 %copy-start.5 = (bf16[512,128]{1,0:T(8,128)(2,1)S(1)}, bf16[512,128]{1,0:T(8,128)(2,1)}, u32[]{:S(2)}) copy-start(bf16[512,128]{1,0:T(8,128)(2,1)} %param.7) | copy-start | bytes 393220
  128.4 16.4 %all-to-all-start = ((f32[16,1,512]{2,1,0:T(1,128)}), f32[16,1,512]{2,1,0:T(1,128)S(1)}, u32[]{:S(2)}, u32[]{:S(2)}) async-start(f32[16,1,512]{2,1,0:T(1,128)} %broadcast_in_dim.56), calls=%async_computation | async-start | bytes 65536 | tf_op jit(solution)/shard_map/all_to_all | solution.py:33
  137.5 46.9 %all-gather.9.cloned.1.call-start = ((), (), s32[]{:S(2)}) async-start(), calls=%async_computation.4 | async-start | bytes 2228224 | tf_op jit(solution)/shard_map/all_gather | solution.py:42
  145.7 105.7 %all-gather.11.cloned.1.call-start = ((), (), s32[]{:S(2)}) async-start(), calls=%async_computation.5 | async-start | bytes 2359296 | tf_op jit(solution)/shard_map/all_gather | solution.py:27
  149.7 37.5 %copy-start.3 = (f32[2,128,766]{2,1,0:T(8,128)}, f32[2,128,766]{2,1,0:T(8,128)S(1)}, u32[]{:S(2)}) copy-start(f32[2,128,766]{2,1,0:T(8,128)S(1)} %reshape.311) | copy-start | bytes 2353156
  184.4 2.3 copy-start.1
  186.6 1.2 copy-start.10
  186.7 2.0 copy-start.12
  187.9 4.6 %copy-start.14 = (bf16[2,2048,128]{2,1,0:T(8,128)(2,1)S(1)}, bf16[2,2048,128]{2,1,0:T(8,128)(2,1)}, u32[]{:S(2)}) copy-start(bf16[2,2048,128]{2,1,0:T(8,128)(2,1)} %param.9) | copy-start | bytes 3145732
  189.4 7.7 %collective-permute-start.2 = (bf16[512,128]{1,0:T(8,128)(2,1)S(1)}, bf16[512,128]{1,0:T(8,128)(2,1)S(1)}, u32[]{:S(2)}, u32[]{:S(2)}) collective-permute-start(bf16[512,128]{1,0:T(8,128)(2,1)S(1)} %convolution_convert_fusion.2), channel_id=1, source_target_pairs={{0,16},{16,32},{32,48},{48,64},{64,80},{80,96},{96,112},{112,128},... | collective-permute-start | bytes 393224 | tf_op jit(solution)/shard_map/ppermute | solution.py:21
  193.4 5.6 %collective-permute-start.3 = (bf16[512,128]{1,0:T(8,128)(2,1)S(1)}, bf16[512,128]{1,0:T(8,128)(2,1)S(1)}, u32[]{:S(2)}, u32[]{:S(2)}) collective-permute-start(bf16[512,128]{1,0:T(8,128)(2,1)S(1)} %convolution_convert_fusion), channel_id=1, source_target_pairs={{0,16},{16,32},{32,48},{48,64},{64,80},{80,96},{96,112},{112,128},... | collective-permute-start | bytes 393224 | tf_op jit(solution)/shard_map/ppermute | solution.py:21
  199.3 3.8 %slice-start.1 = ((f32[2,128,766]{2,1,0:T(8,128)}), f32[2,128,640]{2,1,0:T(8,128)S(1)}, s32[]{:S(2)}) async-start(f32[2,128,766]{2,1,0:T(8,128)} %copy-done.3), calls=%async_computation.7 | async-start | bytes 1310720 | tf_op jit(solution)/shard_map/slice | solution.py:63
  203.1 2.6 copy-start.8
  205.8 45.6 %copy-start.15 = (bf16[2,2048,128]{2,1,0:T(8,128)(2,1)S(1)}, bf16[2,2048,128]{2,1,0:T(8,128)(2,1)}, u32[]{:S(2)}) copy-start(bf16[2,2048,128]{2,1,0:T(8,128)(2,1)} %param.12) | copy-start | bytes 3145732
  208.3 62.3 %copy-start.4 = (bf16[512,128]{0,1:T(8,128)(2,1)S(1)}, bf16[512,128]{0,1:T(8,128)(2,1)}, u32[]{:S(2)}) copy-start(bf16[512,128]{0,1:T(8,128)(2,1)} %add_convert_fusion.1) | copy-start | bytes 393220
  254.1 16.4 %all-to-all-start.1 = ((f32[16,1,512]{2,1,0:T(1,128)}), f32[16,1,512]{2,1,0:T(1,128)S(1)}, u32[]{:S(2)}, u32[]{:S(2)}) async-start(f32[16,1,512]{2,1,0:T(1,128)} %broadcast_in_dim.59), calls=%async_computation.1 | async-start | bytes 65536 | tf_op jit(solution)/shard_map/all_to_all | solution.py:33
Sparse Core Ops, SparseCore 0:
  9.4 48.9 all-gather.4
  85.4 40.1 all-gather.6
  145.8 38.5 all-gather.8
  211.6 39.7 all-gather.10
where the time goes:
time: 279 us; the launch traced here: 278 us
  waiting for transfers between devices  176 us (63%)
  starting transfers between devices  30.6 us (11%)
  local copies, waits for them, and re-layouts  25.3 us (9%)
  matrix products  18.9 us (7%)
  between operations  14 us (5%)
  other arithmetic  7.57 us (3%)
  blocking collectives  5.94 us (2%)
    all_gather x2, waiting for transfers between devices, gathered_by_axis(): filled = lax.all_gather(filled, axes[number], axis=dim, tiled=True)  80.2 us
    all_gather x2, waiting for transfers between devices, project(): full_rows = lax.all_gather(stream, TP, axis=1, tiled=True)  80.1 us
    all_to_all x2, starting transfers between devices, copy_for_each(): return lax.all_to_all(copies, axis, split_axis=0, concat_axis=0, tiled=True)  18.1 us
    all_to_all x2, waiting for transfers between devices, copy_for_each(): return lax.all_to_all(copies, axis, split_axis=0, concat_axis=0, tiled=True)  14.7 us
    ppermute x4, starting transfers between devices, passed_along(): lax.ppermute(value, axis, [(source, source + steps) for source in range(f...  12.4 us
    unnamed x55, local copies, waits for them, and re-layouts  8.42 us
    all_gather x2, blocking collectives, gathered_by_axis(): filled = lax.all_gather(filled, axes[number], axis=dim, tiled=True)  5.94 us
  transfers between devices with their start and end apart: 10, of which 6 were waited for; matrix products, arithmetic and copies ran while one was open for 6% of the time, Pallas kernels for 0%

commit v1 on v0

v1 whole, which is shorter than its diff:
```python
import functools

import jax
import jax.numpy as jnp
from jax import lax
from jax.experimental import pallas as pl
from jax.experimental.pallas import tpu as pltpu
from jax.sharding import Mesh
from jax.sharding import PartitionSpec as P

D = 2048
HEAD = 64
BLK = 128
NB = 16
EPS = 1e-06
NEG = -1e30
VMEM = pl.BlockSpec(memory_space=pltpu.VMEM)
SMEM = pl.BlockSpec(memory_space=pltpu.SMEM)


def params(mib):
    return pltpu.CompilerParams(vmem_limit_bytes=mib * 1024 * 1024)


def core_pairs(step):
    pairs = []
    for y in range(8):
        for c in range(2):
            target = (y + (step if c == 0 else -step)) % 8
            pairs.append((2 * y + c, 2 * target + c))
    return pairs


def gather_blocks(x):
    core = lax.axis_index("c")
    own = lax.all_gather(x, "c", axis=0)
    one = lax.ppermute(own, ("y", "c"), core_pairs(1))
    two = lax.ppermute(own, ("y", "c"), core_pairs(2))
    three = lax.ppermute(two, ("y", "c"), core_pairs(1))
    half = lax.dynamic_index_in_dim(two, core, 0, keepdims=True)
    four = lax.ppermute(half, ("y", "c"), core_pairs(2))
    received = jnp.concatenate([one, two, three, four], axis=0)
    other = lax.ppermute(received, "c", [(0, 1), (1, 0)])
    return own, received, other


def block_ids():
    y = lax.axis_index("y")
    c = lax.axis_index("c")
    sign = 1 - 2 * c
    near = [(y - sign * d) % 8 for d in (1, 2, 3)]
    far = [(y + sign * d) % 8 for d in (1, 2, 3)]
    across = (y + 4) % 8
    ids = [2 * y, 2 * y + 1]
    for chip in near:
        ids += [2 * chip, 2 * chip + 1]
    ids.append(2 * across + c)
    for chip in far:
        ids += [2 * chip, 2 * chip + 1]
    ids.append(2 * across + 1 - c)
    return jnp.stack(ids).astype(jnp.int32)


def part(refs, k):
    own, received, other = refs
    if k < 2:
        return own, k
    if k < 9:
        return received, k - 2
    return other, k - 9


def qkv_tail(ids, xs, total, gain, rows, norm):
    inv = lax.rsqrt(jnp.sum(total, axis=1, keepdims=True) / D + EPS)
    for k in range(NB):
        t = ids[k]
        col = pl.multiple_of(t * BLK, BLK)
        norm[rows, pl.ds(col, BLK)] = (
            xs(k) * inv * gain[pl.ds(t, 1), :]
        ).astype(jnp.bfloat16)


def project(norm, wq, wk, wv, q_out, kv_out):
    full = norm[...]
    kv_out[:, :BLK] = jnp.dot(full, wk[...], preferred_element_type=jnp.float32).astype(jnp.bfloat16)
    kv_out[:, BLK:] = jnp.dot(full, wv[...], preferred_element_type=jnp.float32).astype(jnp.bfloat16)
    q = jnp.dot(full, wq[...], preferred_element_type=jnp.float32)
    q_out[...] = (q * HEAD ** (-0.5)).astype(jnp.bfloat16)


def first_kernel(ids, own, received, other, gain, wq, wk, wv, q_out, kv_out, norm):
    refs = (own, received, other)

    def tile(i, carry):
        rows = pl.ds(pl.multiple_of(i * 64, 64), 64)

        def load(k):
            ref, j = part(refs, k)
            return ref[j, rows, :].astype(jnp.float32)

        total = jnp.zeros((64, BLK), jnp.float32)
        for k in range(NB):
            x = load(k)
            total += x * x
        qkv_tail(ids, load, total, gain, rows, norm)
        return carry

    lax.fori_loop(0, own.shape[1] // 64, tile, 0)
    project(norm, wq, wk, wv, q_out, kv_out)


def next_kernel(
    ids, mine, own, received, other, b_own, b_received, b_other, gain_post, gain, wq, wk, wv,
    q_out, kv_out, stream_out, norm, stream,
):
    refs = (own, received, other)
    b_refs = (b_own, b_received, b_other)

    def tile(i, carry):
        rows = pl.ds(pl.multiple_of(i * 64, 64), 64)

        def load(group, k):
            ref, j = part(group, k)
            return ref[j, rows, :].astype(jnp.float32)

        total = jnp.zeros((64, BLK), jnp.float32)
        for k in range(NB):
            x = load(b_refs, k)
            total += x * x
        inv_post = lax.rsqrt(jnp.sum(total, axis=1, keepdims=True) / D + EPS)
        total = jnp.zeros((64, BLK), jnp.float32)
        for k in range(NB):
            x = load(refs, k) + load(b_refs, k) * inv_post * gain_post[pl.ds(ids[k], 1), :]
            x = x.astype(jnp.bfloat16)
            stream[k, rows, :] = x
            x = x.astype(jnp.float32)
            total += x * x
        qkv_tail(ids, lambda k: stream[k, rows, :].astype(jnp.float32), total, gain, rows, norm)
        stream_out[rows, :] = stream[mine[0], rows, :]
        return carry

    lax.fori_loop(0, own.shape[1] // 64, tile, 0)
    project(norm, wq, wk, wv, q_out, kv_out)


def attend_kernel(layer, first, q, kv, kv_prev, bias, out):
    lane = lax.broadcasted_iota(jnp.int32, (BLK, BLK), 1)
    row = lax.broadcasted_iota(jnp.int32, (BLK, BLK), 0)
    hidden = jnp.where(first[0] == 1, NEG, 0.0)
    tables = []
    for h in range(2):
        low = bias[layer, h : h + 1, 0:BLK]
        high = bias[layer, h : h + 1, BLK : 2 * BLK]
        last = bias[layer, h : h + 1, 2 * BLK : 2 * BLK + 1]
        last_row = jnp.broadcast_to(last, (1, BLK))
        shape = (BLK, 2 * BLK)
        diag = jnp.broadcast_to(jnp.concatenate([high, low], axis=1), shape)
        diag = pltpu.roll(diag, 0, 1, stride=1, stride_axis=0)[:, :BLK].T
        near = jnp.broadcast_to(jnp.concatenate([last_row, high], axis=1), shape)
        near = pltpu.roll(near, 0, 1, stride=1, stride_axis=0)[:, :BLK].T
        diag = jnp.where((lane >= 64) & (row < 64), NEG, diag)
        full_last = jnp.broadcast_to(last, (BLK, BLK))
        edge = jnp.where((lane < 64) & (row >= 64), NEG, full_last)
        tables.append((diag, near, full_last, edge))
    for i in range(4):
        rows = slice(i * BLK, (i + 1) * BLK)
        results = []
        for h in range(2):
            diag, near, full_last, edge = tables[h]
            qh = q[rows, :]
            qh = jnp.where((lane < HEAD) == (h == 0), qh, jnp.zeros_like(qh))
            dims = (((1,), (1,)), ((), ()))
            left = lax.dot_general(
                qh, kv_prev[i * BLK :, :BLK], dims, preferred_element_type=jnp.float32
            )
            right = lax.dot_general(
                qh, kv[: (i + 1) * BLK, :BLK], dims, preferred_element_type=jnp.float32
            )
            scores = []
            for j in range(5):
                gap = 4 - j
                block = i + j
                if block < 4:
                    piece = left[:, j * BLK : (j + 1) * BLK] + hidden
                else:
                    piece = right[:, (block - 4) * BLK : (block - 3) * BLK]
                term = diag if gap == 0 else near if gap == 1 else edge if gap == 4 else full_last
                scores.append(piece + term)
            top = functools.reduce(jnp.maximum, scores)
            top = jnp.max(top, axis=1, keepdims=True)
            weights = [jnp.exp(s - top) for s in scores]
            norm = jnp.sum(functools.reduce(jnp.add, weights), axis=1, keepdims=True)
            inv = 1.0 / norm
            probs = [(w * inv).astype(jnp.bfloat16) for w in weights]
            split = 4 - i
            acc = jnp.dot(
                jnp.concatenate(probs[:split], axis=1),
                kv_prev[i * BLK :, BLK:],
                preferred_element_type=jnp.float32,
            )
            acc += jnp.dot(
                jnp.concatenate(probs[split:], axis=1),
                kv[: (i + 1) * BLK, BLK:],
                preferred_element_type=jnp.float32,
            )
            results.append(acc)
        out[rows, :] = jnp.where(lane < HEAD, results[0], results[1]).astype(jnp.bfloat16)


def branch_of(ids, refs, w, acc):
    acc[...] = jnp.zeros_like(acc)
    for k in (0, 2, 4, 6, 9, 11, 13):
        ref, j = part(refs, k)
        pair = jnp.concatenate([ref[j], ref[j + 1]], axis=1)
        rows = pl.ds(pl.multiple_of(ids[k] * BLK, 2 * BLK), 2 * BLK)
        acc[...] += jnp.dot(pair, w[rows, :], preferred_element_type=jnp.float32)
    for k in (8, 15):
        ref, j = part(refs, k)
        rows = pl.ds(pl.multiple_of(ids[k] * BLK, BLK), BLK)
        acc[...] += jnp.dot(ref[j], w[rows, :], preferred_element_type=jnp.float32)


def out_kernel(ids, own, received, other, w, out, acc):
    branch_of(ids, (own, received, other), w, acc)
    out[...] = acc[...].astype(jnp.bfloat16)


def last_kernel(ids, own, received, other, w, out, squares):
    branch_of(ids, (own, received, other), w, out)
    for i in range(4):
        x = out[i * BLK : (i + 1) * BLK, :]
        squares[i : i + 1, :] = jnp.sum((x * x).T, axis=0, keepdims=True)


def finish_kernel(squares, branch, stream, gain, out):
    total = jnp.sum(squares[...], axis=0)
    inv = lax.rsqrt(total / D + EPS)
    for i in range(4):
        rows = slice(i * BLK, (i + 1) * BLK)
        scale = jnp.broadcast_to(inv[i : i + 1, :], (BLK, BLK)).T
        x = stream[rows, :].astype(jnp.float32)
        out[rows, :] = (x + branch[rows, :] * scale * gain[...]).astype(jnp.bfloat16)


def call(kernel, ins, outs, scratch, mib, flops, args):
    size = sum(a.size * a.dtype.itemsize for a in args)
    return pl.pallas_call(
        kernel,
        out_shape=outs,
        in_specs=ins,
        out_specs=jax.tree.map(lambda _: VMEM, outs),
        scratch_shapes=scratch,
        compiler_params=params(mib),
        cost_estimate=pl.CostEstimate(flops=flops, bytes_accessed=size, transcendentals=0),
    )(*args)


def on_device(residual, gains, w_query, w_key, w_value, w_out, rel_bias):
    tokens = residual.shape[0]
    half = jnp.bfloat16
    ids = block_ids()
    core = lax.axis_index("c")
    mine = core.reshape(1).astype(jnp.int32)
    first = (lax.axis_index("sp") == 0).reshape(1).astype(jnp.int32)
    gain_rows = gains.reshape(2, 2, NB, BLK)
    own_gain = lax.dynamic_slice_in_dim(gain_rows[1, 1], lax.axis_index(("y", "c")), 1, 0)
    block = jax.ShapeDtypeStruct((tokens, BLK), half)
    pair = jax.ShapeDtypeStruct((tokens, 2 * BLK), half)
    wide = jax.ShapeDtypeStruct((tokens, BLK), jnp.float32)
    norm = pltpu.VMEM((tokens, D), half)
    flow = lax.axis_size("sp")
    shift = [(i, i + 1) for i in range(flow - 1)]

    def attention(layer, q, kv):
        previous = lax.ppermute(kv, "sp", shift)
        return call(
            functools.partial(attend_kernel, layer), [SMEM] + [VMEM] * 4, block, [], 8,
            10**9, (first, q, kv, previous, rel_bias),
        )

    stream = gather_blocks(residual)
    q, kv = call(
        first_kernel, [SMEM] + [VMEM] * 7, (block, pair), [norm], 16, 2 * 10**9,
        (ids, *stream, gain_rows[0, 0], w_query[0], w_key[0], w_value[0]),
    )
    attended = gather_blocks(attention(0, q, kv))
    branch = call(
        out_kernel, [SMEM] + [VMEM] * 4, block, [pltpu.VMEM((tokens, BLK), jnp.float32)], 8,
        10**9, (ids, *attended, w_out[0]),
    )
    branch = gather_blocks(branch)
    q, kv, carried = call(
        next_kernel, [SMEM] * 2 + [VMEM] * 11, (block, pair, block),
        [norm, pltpu.VMEM((NB, tokens, BLK), half)], 20, 2 * 10**9,
        (ids, mine, *stream, *branch, gain_rows[0, 1], gain_rows[1, 0],
         w_query[1], w_key[1], w_value[1]),
    )
    attended = gather_blocks(attention(1, q, kv))
    branch, squares = call(
        last_kernel, [SMEM] + [VMEM] * 4,
        (wide, jax.ShapeDtypeStruct((tokens // BLK, BLK), jnp.float32)), [], 8, 10**9,
        (ids, *attended, w_out[1]),
    )
    copies = jnp.broadcast_to(squares, (NB, *squares.shape))
    everything = lax.all_to_all(copies, ("y", "c"), split_axis=0, concat_axis=0, tiled=True)
    return call(
        finish_kernel, [VMEM] * 4, block, [], 8, 10**7, (everything, branch, carried, own_gain)
    )


def solution(mesh):
    finer = Mesh(mesh.devices.reshape(mesh.shape["sp"], 8, 2), ("sp", "y", "c"))
    tp = ("y", "c")
    in_specs = (
        P("sp", tp),
        P(),
        P(None, None, tp),
        P(None, None, tp),
        P(None, None, tp),
        P(None, None, tp),
        P(None, tp, None),
    )
    return jax.shard_map(
        on_device, mesh=finer, in_specs=in_specs, out_specs=P("sp", tp), check_vma=False
    )
```

time: 279 us -> 194 us (0.70)
  the two profiles are of different devices: /device:TPU:1 before, /device:TPU:257 now
where the time goes in v1:
time: 194 us; the launch traced here: 193 us
  starting transfers between devices  97.3 us (50%)
  waiting for transfers between devices  60.2 us (31%)
  Pallas kernels  21 us (11%)
  blocking collectives  10.2 us (5%)
  local copies, waits for them, and re-layouts  3.85 us (2%)
    ppermute x4, starting transfers between devices, gather_blocks(): three = lax.ppermute(two, ('y', 'c'), core_pairs(1))  21.4 us
    pallas_call x7, Pallas kernels, call(): pl.pallas_call(kernel, out_shape=outs, in_specs=ins, out_specs=jax.tree.m...  21 us
    ppermute x2, waiting for transfers between devices, attention(): previous = lax.ppermute(kv, 'sp', shift)  20.5 us
    ppermute x4, starting transfers between devices, gather_blocks(): other = lax.ppermute(received, 'c', [(0, 1), (1, 0)])  19.4 us
    ppermute x4, waiting for transfers between devices, gather_blocks(): four = lax.ppermute(half, ('y', 'c'), core_pairs(2))  17.1 us
    ppermute x4, starting transfers between devices, gather_blocks(): one = lax.ppermute(own, ('y', 'c'), core_pairs(1))  17 us
    ppermute x4, starting transfers between devices, gather_blocks(): two = lax.ppermute(own, ('y', 'c'), core_pairs(2))  15.6 us
    ppermute x4, starting transfers between devices, gather_blocks(): four = lax.ppermute(half, ('y', 'c'), core_pairs(2))  12.6 us
  transfers between devices with their start and end apart: 23, of which 15 were waited for; matrix products, arithmetic and copies ran while one was open for 0% of the time, Pallas kernels for 0%

profile of v1, /device:TPU:257, one launch (start us, length us, event | category | flops | bytes accessed | tf_op | source)
XLA Modules:
  0.0 193.2 jit_solution(9368842744399771955)
XLA Ops:
  0.0 2.5 %all-gather = bf16[1024,128]{1,0:T(8,128)(2,1)S(1)} all-gather(bf16[512,128]{1,0:T(8,128)(2,1)} %param.7), channel_id=2, replica_groups=mesh['sp'=32,'y'=8,'c'=2] {'c'}, dimensions={0}, use_global_device_ids=true | all-gather | bytes 393216 | tf_op jit(solution)/shard_map/all_gather | solution.py:36
  2.5 5.9 %collective-permute-start.1 = (bf16[2,512,128]{2,1,0:T(8,128)(2,1)S(1)}, bf16[2,512,128]{2,1,0:T(8,128)(2,1)S(1)}, u32[]{:S(2)}, u32[]{:S(2)}) collective-permute-start(bf16[2,512,128]{2,1,0:T(8,128)(2,1)S(1)} %bitcast.46), channel_id=1, source_target_pairs={{0,4},{1,13},{2,6},{3,15},{4,8},{5,1},{6,10},{7,3},{8,12},{9,5},{1... | collective-permute-start | bytes 786440 | tf_op jit(solution)/shard_map/ppermute | solution.py:38
  8.4 3.0 %collective-permute-start = (bf16[2,512,128]{2,1,0:T(8,128)(2,1)S(1)}, bf16[2,512,128]{2,1,0:T(8,128)(2,1)S(1)}, u32[]{:S(2)}, u32[]{:S(2)}) collective-permute-start(bf16[2,512,128]{2,1,0:T(8,128)(2,1)S(1)} %bitcast.47), channel_id=1, source_target_pairs={{0,2},{1,15},{2,4},{3,1},{4,6},{5,3},{6,8},{7,5},{8,10},{9,7},{10,... | collective-permute-start | bytes 786440 | tf_op jit(solution)/shard_map/ppermute | solution.py:37
  11.5 0.0 copy-start.9
  11.5 0.7 copy-done.9
  12.2 0.1 stack.67.ids
  12.4 0.0 copy-start.5
  12.4 2.1 %collective-permute-done.1 = bf16[2,512,128]{2,1,0:T(8,128)(2,1)S(1)} collective-permute-done((bf16[2,512,128]{2,1,0:T(8,128)(2,1)S(1)}, bf16[2,512,128]{2,1,0:T(8,128)(2,1)S(1)}, u32[]{:S(2)}, u32[]{:S(2)}) %collective-permute-start.1) | collective-permute-done | bytes 262176 | tf_op jit(solution)/shard_map/ppermute | solution.py:38
  14.5 4.1 %collective-permute-start.2 = (bf16[2,512,128]{2,1,0:T(8,128)(2,1)S(1)}, bf16[2,512,128]{2,1,0:T(8,128)(2,1)S(1)}, u32[]{:S(2)}, u32[]{:S(2)}) collective-permute-start(bf16[2,512,128]{2,1,0:T(8,128)(2,1)S(1)} %collective-permute-done.1), channel_id=1, source_target_pairs={{0,2},{1,15},{2,4},{3,1},{4,6},{5,3},{6,8},{7,5},{8,10},{9,7},{10,... | collective-permute-start | bytes 786440 | tf_op jit(solution)/shard_map/ppermute | solution.py:39
  18.6 3.9 %collective-permute-start.3 = (bf16[1,512,128]{2,1,0:T(8,128)(2,1)S(1)}, bf16[1,512,128]{2,1,0:T(8,128)(2,1)S(1)}, u32[]{:S(2)}, u32[]{:S(2)}) collective-permute-start(bf16[1,512,128]{2,1,0:T(8,128)(2,1)S(1)} %constant_dynamic-slice_fusion.4), channel_id=1, source_target_pairs={{0,4},{1,13},{2,6},{3,15},{4,8},{5,1},{6,10},{7,3},{8,12},{9,5},{1... | collective-permute-start | bytes 393224 | tf_op jit(solution)/shard_map/ppermute | solution.py:41
  22.6 3.9 %collective-permute-done.3 = bf16[1,512,128]{2,1,0:T(8,128)(2,1)S(1)} collective-permute-done((bf16[1,512,128]{2,1,0:T(8,128)(2,1)S(1)}, bf16[1,512,128]{2,1,0:T(8,128)(2,1)S(1)}, u32[]{:S(2)}, u32[]{:S(2)}) %collective-permute-start.3) | collective-permute-done | bytes 131104 | tf_op jit(solution)/shard_map/ppermute | solution.py:41
  26.5 0.0 copy-start.7
  26.6 0.0 copy-start.8
  26.6 4.6 %collective-permute-start.4 = (bf16[7,512,128]{2,1,0:T(8,128)(2,1)S(1)}, bf16[7,512,128]{2,1,0:T(8,128)(2,1)S(1)}, u32[]{:S(2)}, u32[]{:S(2)}) collective-permute-start(bf16[7,512,128]{2,1,0:T(8,128)(2,1)S(1)} %constant_dynamic-update-slice_fusion.received), channel_id=1, source_target_pairs={{0,1},{1,0},{2,3},{3,2},{4,5},{5,4},{6,7},{7,6},{8,9},{9,8},{10,11... | collective-permute-start | bytes 2752520 | tf_op jit(solution)/shard_map/ppermute | solution.py:43
  31.2 0.1 slice_bitcast_fusion.3
  31.2 0.1 slice_bitcast_fusion.1
  31.4 1.8 collective-permute-done.4.other
  33.2 4.6 %shard_map.73 = (bf16[512,128]{1,0:T(8,128)(2,1)S(1)}, bf16[512,256]{1,0:T(8,128)(2,1)}) custom-call(s32[16]{0:T(128)S(1)} %stack.67.ids, bf16[2,512,128]{2,1,0:T(8,128)(2,1)S(1)} %bitcast.48, bf16[7,512,128]{2,1,0:T(8,128)(2,1)S(1)} %constant_dynamic-update-slice_fusion.received, bf16[7,512,128]{2,1,0:T(8,128)(2,1)S(1)} %collective-permute-done.4.other, ...), custom_call_target="tpu_custom_call" | custom-call | flops 2000000000 | bytes 3678272 | tf_op jit(solution)/shard_map/pallas_call | solution.py:247
  37.8 0.7 copy-done.3
  38.4 3.1 %collective-permute-start.5 = (bf16[512,256]{1,0:T(8,128)(2,1)}, bf16[512,256]{1,0:T(8,128)(2,1)S(1)}, u32[]{:S(2)}, u32[]{:S(2)}) collective-permute-start(bf16[512,256]{1,0:T(8,128)(2,1)} %get-tuple-element.13.kv), channel_id=1, source_target_pairs={{0,16},{16,32},{32,48},{48,64},{64,80},{80,96},{96,112},{112,128},... | collective-permute-start | bytes 786440 | tf_op jit(solution)/shard_map/ppermute | solution.py:275
  41.5 0.0 copy-start.2
  41.6 9.8 %collective-permute-done.5.kv_prev = bf16[512,256]{1,0:T(8,128)(2,1)S(1)} collective-permute-done((bf16[512,256]{1,0:T(8,128)(2,1)}, bf16[512,256]{1,0:T(8,128)(2,1)S(1)}, u32[]{:S(2)}, u32[]{:S(2)}) %collective-permute-start.5) | collective-permute-done | bytes 262176 | tf_op jit(solution)/shard_map/ppermute | solution.py:275
  51.3 0.9 copy-done.4
  52.2 4.3 %shard_map.74 = bf16[512,128]{1,0:T(8,128)(2,1)S(1)} custom-call(s32[1]{0:T(128)} %bitcast.16.first, bf16[512,128]{1,0:T(8,128)(2,1)S(1)} %copy-done.4, bf16[512,256]{1,0:T(8,128)(2,1)} %get-tuple-element.13.kv, bf16[512,256]{1,0:T(8,128)(2,1)S(1)} %collective-permute-done.5.kv_prev, f32[2,2,257]{2,1,0:T(2,128)S(1)} %copy-done.2), custom_call_target="tpu_custom_call" | custom-call | flops 1000000000 | bytes 659476 | tf_op jit(solution)/shard_map/pallas_call | solution.py:247
  56.5 2.9 %all-gather.1 = bf16[1024,128]{1,0:T(8,128)(2,1)S(1)} all-gather(bf16[512,128]{1,0:T(8,128)(2,1)S(1)} %shard_map.74), channel_id=3, replica_groups=mesh['sp'=32,'y'=8,'c'=2] {'c'}, dimensions={0}, use_global_device_ids=true | all-gather | bytes 393216 | tf_op jit(solution)/shard_map/all_gather | solution.py:36
  59.4 2.8 %collective-permute-start.7 = (bf16[2,512,128]{2,1,0:T(8,128)(2,1)S(1)}, bf16[2,512,128]{2,1,0:T(8,128)(2,1)S(1)}, u32[]{:S(2)}, u32[]{:S(2)}) collective-permute-start(bf16[2,512,128]{2,1,0:T(8,128)(2,1)S(1)} %bitcast.56), channel_id=1, source_target_pairs={{0,4},{1,13},{2,6},{3,15},{4,8},{5,1},{6,10},{7,3},{8,12},{9,5},{1... | collective-permute-start | bytes 786440 | tf_op jit(solution)/shard_map/ppermute | solution.py:38
  62.2 6.3 %collective-permute-start.6 = (bf16[2,512,128]{2,1,0:T(8,128)(2,1)S(1)}, bf16[2,512,128]{2,1,0:T(8,128)(2,1)S(1)}, u32[]{:S(2)}, u32[]{:S(2)}) collective-permute-start(bf16[2,512,128]{2,1,0:T(8,128)(2,1)S(1)} %bitcast.57), channel_id=1, source_target_pairs={{0,2},{1,15},{2,4},{3,1},{4,6},{5,3},{6,8},{7,5},{8,10},{9,7},{10,... | collective-permute-start | bytes 786440 | tf_op jit(solution)/shard_map/ppermute | solution.py:37
  68.5 6.2 %collective-permute-start.8 = (bf16[2,512,128]{2,1,0:T(8,128)(2,1)S(1)}, bf16[2,512,128]{2,1,0:T(8,128)(2,1)S(1)}, u32[]{:S(2)}, u32[]{:S(2)}) collective-permute-start(bf16[2,512,128]{2,1,0:T(8,128)(2,1)S(1)} %collective-permute-done.7), channel_id=1, source_target_pairs={{0,2},{1,15},{2,4},{3,1},{4,6},{5,3},{6,8},{7,5},{8,10},{9,7},{10,... | collective-permute-start | bytes 786440 | tf_op jit(solution)/shard_map/ppermute | solution.py:39
  74.7 3.0 %collective-permute-start.9 = (bf16[1,512,128]{2,1,0:T(8,128)(2,1)S(1)}, bf16[1,512,128]{2,1,0:T(8,128)(2,1)S(1)}, u32[]{:S(2)}, u32[]{:S(2)}) collective-permute-start(bf16[1,512,128]{2,1,0:T(8,128)(2,1)S(1)} %constant_dynamic-slice_fusion.3), channel_id=1, source_target_pairs={{0,4},{1,13},{2,6},{3,15},{4,8},{5,1},{6,10},{7,3},{8,12},{9,5},{1... | collective-permute-start | bytes 393224 | tf_op jit(solution)/shard_map/ppermute | solution.py:41
  77.8 0.2 collective-permute-done.8
  78.0 4.3 %collective-permute-done.9 = bf16[1,512,128]{2,1,0:T(8,128)(2,1)S(1)} collective-permute-done((bf16[1,512,128]{2,1,0:T(8,128)(2,1)S(1)}, bf16[1,512,128]{2,1,0:T(8,128)(2,1)S(1)}, u32[]{:S(2)}, u32[]{:S(2)}) %collective-permute-start.9) | collective-permute-done | bytes 131104 | tf_op jit(solution)/shard_map/ppermute | solution.py:41
  82.4 5.9 %collective-permute-start.10 = (bf16[7,512,128]{2,1,0:T(8,128)(2,1)S(1)}, bf16[7,512,128]{2,1,0:T(8,128)(2,1)S(1)}, u32[]{:S(2)}, u32[]{:S(2)}) collective-permute-start(bf16[7,512,128]{2,1,0:T(8,128)(2,1)S(1)} %constant_dynamic-update-slice_fusion.4.received), channel_id=1, source_target_pairs={{0,1},{1,0},{2,3},{3,2},{4,5},{5,4},{6,7},{7,6},{8,9},{9,8},{10,11... | collective-permute-start | bytes 2752520 | tf_op jit(solution)/shard_map/ppermute | solution.py:43
  88.3 0.1 slice_bitcast_fusion
  88.4 2.0 %collective-permute-done.10.other = bf16[7,512,128]{2,1,0:T(8,128)(2,1)S(1)} collective-permute-done((bf16[7,512,128]{2,1,0:T(8,128)(2,1)S(1)}, bf16[7,512,128]{2,1,0:T(8,128)(2,1)S(1)}, u32[]{:S(2)}, u32[]{:S(2)}) %collective-permute-start.10) | collective-permute-done | bytes 917536 | tf_op jit(solution)/shard_map/ppermute | solution.py:43
  90.4 1.3 shard_map.75
  91.6 2.0 %all-gather.2 = bf16[1024,128]{1,0:T(8,128)(2,1)S(1)} all-gather(bf16[512,128]{1,0:T(8,128)(2,1)S(1)} %shard_map.75), channel_id=4, replica_groups=mesh['sp'=32,'y'=8,'c'=2] {'c'}, dimensions={0}, use_global_device_ids=true | all-gather | bytes 393216 | tf_op jit(solution)/shard_map/all_gather | solution.py:36
  93.6 3.8 %collective-permute-start.12 = (bf16[2,512,128]{2,1,0:T(8,128)(2,1)S(1)}, bf16[2,512,128]{2,1,0:T(8,128)(2,1)S(1)}, u32[]{:S(2)}, u32[]{:S(2)}) collective-permute-start(bf16[2,512,128]{2,1,0:T(8,128)(2,1)S(1)} %bitcast.53), channel_id=1, source_target_pairs={{0,4},{1,13},{2,6},{3,15},{4,8},{5,1},{6,10},{7,3},{8,12},{9,5},{1... | collective-permute-start | bytes 786440 | tf_op jit(solution)/shard_map/ppermute | solution.py:38
  97.5 2.1 %collective-permute-start.11 = (bf16[2,512,128]{2,1,0:T(8,128)(2,1)S(1)}, bf16[2,512,128]{2,1,0:T(8,128)(2,1)S(1)}, u32[]{:S(2)}, u32[]{:S(2)}) collective-permute-start(bf16[2,512,128]{2,1,0:T(8,128)(2,1)S(1)} %bitcast.54), channel_id=1, source_target_pairs={{0,2},{1,15},{2,4},{3,1},{4,6},{5,3},{6,8},{7,5},{8,10},{9,7},{10,... | collective-permute-start | bytes 786440 | tf_op jit(solution)/shard_map/ppermute | solution.py:37
  99.6 4.1 %collective-permute-done.12 = bf16[2,512,128]{2,1,0:T(8,128)(2,1)S(1)} collective-permute-done((bf16[2,512,128]{2,1,0:T(8,128)(2,1)S(1)}, bf16[2,512,128]{2,1,0:T(8,128)(2,1)S(1)}, u32[]{:S(2)}, u32[]{:S(2)}) %collective-permute-start.12) | collective-permute-done | bytes 262176 | tf_op jit(solution)/shard_map/ppermute | solution.py:38
  103.7 4.7 %collective-permute-start.13 = (bf16[2,512,128]{2,1,0:T(8,128)(2,1)S(1)}, bf16[2,512,128]{2,1,0:T(8,128)(2,1)S(1)}, u32[]{:S(2)}, u32[]{:S(2)}) collective-permute-start(bf16[2,512,128]{2,1,0:T(8,128)(2,1)S(1)} %collective-permute-done.12), channel_id=1, source_target_pairs={{0,2},{1,15},{2,4},{3,1},{4,6},{5,3},{6,8},{7,5},{8,10},{9,7},{10,... | collective-permute-start | bytes 786440 | tf_op jit(solution)/shard_map/ppermute | solution.py:39
  108.5 2.4 %collective-permute-start.14 = (bf16[1,512,128]{2,1,0:T(8,128)(2,1)S(1)}, bf16[1,512,128]{2,1,0:T(8,128)(2,1)S(1)}, u32[]{:S(2)}, u32[]{:S(2)}) collective-permute-start(bf16[1,512,128]{2,1,0:T(8,128)(2,1)S(1)} %constant_dynamic-slice_fusion.2), channel_id=1, source_target_pairs={{0,4},{1,13},{2,6},{3,15},{4,8},{5,1},{6,10},{7,3},{8,12},{9,5},{1... | collective-permute-start | bytes 393224 | tf_op jit(solution)/shard_map/ppermute | solution.py:41
  110.9 0.0 collective-permute-done.11
  111.0 0.8 collective-permute-done.13
  111.8 4.6 %collective-permute-done.14 = bf16[1,512,128]{2,1,0:T(8,128)(2,1)S(1)} collective-permute-done((bf16[1,512,128]{2,1,0:T(8,128)(2,1)S(1)}, bf16[1,512,128]{2,1,0:T(8,128)(2,1)S(1)}, u32[]{:S(2)}, u32[]{:S(2)}) %collective-permute-start.14) | collective-permute-done | bytes 131104 | tf_op jit(solution)/shard_map/ppermute | solution.py:41
  116.5 3.2 %collective-permute-start.15 = (bf16[7,512,128]{2,1,0:T(8,128)(2,1)S(1)}, bf16[7,512,128]{2,1,0:T(8,128)(2,1)S(1)}, u32[]{:S(2)}, u32[]{:S(2)}) collective-permute-start(bf16[7,512,128]{2,1,0:T(8,128)(2,1)S(1)} %constant_dynamic-update-slice_fusion.8.b_received), channel_id=1, source_target_pairs={{0,1},{1,0},{2,3},{3,2},{4,5},{5,4},{6,7},{7,6},{8,9},{9,8},{10,11... | collective-permute-start | bytes 2752520 | tf_op jit(solution)/shard_map/ppermute | solution.py:43
  119.7 2.1 %collective-permute-done.15.b_other = bf16[7,512,128]{2,1,0:T(8,128)(2,1)S(1)} collective-permute-done((bf16[7,512,128]{2,1,0:T(8,128)(2,1)S(1)}, bf16[7,512,128]{2,1,0:T(8,128)(2,1)S(1)}, u32[]{:S(2)}, u32[]{:S(2)}) %collective-permute-start.15) | collective-permute-done | bytes 917536 | tf_op jit(solution)/shard_map/ppermute | solution.py:43
  121.8 5.4 %shard_map.76 = (bf16[512,128]{1,0:T(8,128)(2,1)S(1)}, bf16[512,256]{1,0:T(8,128)(2,1)S(1)}, bf16[512,128]{1,0:T(8,128)(2,1)S(1)}) custom-call(s32[16]{0:T(128)S(1)} %stack.67.ids, s32[1]{0:T(128)} %bitcast.17.mine, bf16[2,512,128]{2,1,0:T(8,128)(2,1)S(1)} %bitcast.49, bf16[7,512,128]{2,1,0:T(8,128)(2,1)S(1)} %constant_dynamic-update-slice_fusion.received, ...), custom_call_target="tpu_custom_call" | custom-call | flops 2000000000 | bytes 5783620 | tf_op jit(solution)/shard_map/pallas_call | solution.py:247
  127.1 1.9 collective-permute-start.16
  129.1 10.8 %collective-permute-done.16.kv_prev = bf16[512,256]{1,0:T(8,128)(2,1)S(1)} collective-permute-done((bf16[512,256]{1,0:T(8,128)(2,1)S(1)}, bf16[512,256]{1,0:T(8,128)(2,1)S(1)}, u32[]{:S(2)}, u32[]{:S(2)}) %collective-permute-start.16) | collective-permute-done | bytes 262176 | tf_op jit(solution)/shard_map/ppermute | solution.py:275
  139.8 3.3 %shard_map.77 = bf16[512,128]{1,0:T(8,128)(2,1)S(1)} custom-call(s32[1]{0:T(128)} %bitcast.16.first, bf16[512,128]{1,0:T(8,128)(2,1)S(1)} %get-tuple-element.14.q, bf16[512,256]{1,0:T(8,128)(2,1)S(1)} %get-tuple-element.15.kv, bf16[512,256]{1,0:T(8,128)(2,1)S(1)} %collective-permute-done.16.kv_prev, f32[2,2,257]{2,1,0:T(2,128)S(1)} %copy-done.2), custom_call_target="tpu_custom_call" | custom-call | flops 1000000000 | bytes 659476 | tf_op jit(solution)/shard_map/pallas_call | solution.py:247
  143.2 2.9 %all-gather.3 = bf16[1024,128]{1,0:T(8,128)(2,1)S(1)} all-gather(bf16[512,128]{1,0:T(8,128)(2,1)S(1)} %shard_map.77), channel_id=5, replica_groups=mesh['sp'=32,'y'=8,'c'=2] {'c'}, dimensions={0}, use_global_device_ids=true | all-gather | bytes 393216 | tf_op jit(solution)/shard_map/all_gather | solution.py:36
  146.1 3.1 %collective-permute-start.18 = (bf16[2,512,128]{2,1,0:T(8,128)(2,1)S(1)}, bf16[2,512,128]{2,1,0:T(8,128)(2,1)S(1)}, u32[]{:S(2)}, u32[]{:S(2)}) collective-permute-start(bf16[2,512,128]{2,1,0:T(8,128)(2,1)S(1)} %bitcast.50), channel_id=1, source_target_pairs={{0,4},{1,13},{2,6},{3,15},{4,8},{5,1},{6,10},{7,3},{8,12},{9,5},{1... | collective-permute-start | bytes 786440 | tf_op jit(solution)/shard_map/ppermute | solution.py:38
  149.2 5.7 %collective-permute-start.17 = (bf16[2,512,128]{2,1,0:T(8,128)(2,1)S(1)}, bf16[2,512,128]{2,1,0:T(8,128)(2,1)S(1)}, u32[]{:S(2)}, u32[]{:S(2)}) collective-permute-start(bf16[2,512,128]{2,1,0:T(8,128)(2,1)S(1)} %bitcast.51), channel_id=1, source_target_pairs={{0,2},{1,15},{2,4},{3,1},{4,6},{5,3},{6,8},{7,5},{8,10},{9,7},{10,... | collective-permute-start | bytes 786440 | tf_op jit(solution)/shard_map/ppermute | solution.py:37
  154.9 0.0 collective-permute-done.18
  154.9 6.4 %collective-permute-start.19 = (bf16[2,512,128]{2,1,0:T(8,128)(2,1)S(1)}, bf16[2,512,128]{2,1,0:T(8,128)(2,1)S(1)}, u32[]{:S(2)}, u32[]{:S(2)}) collective-permute-start(bf16[2,512,128]{2,1,0:T(8,128)(2,1)S(1)} %collective-permute-done.18), channel_id=1, source_target_pairs={{0,2},{1,15},{2,4},{3,1},{4,6},{5,3},{6,8},{7,5},{8,10},{9,7},{10,... | collective-permute-start | bytes 786440 | tf_op jit(solution)/shard_map/ppermute | solution.py:39
  161.3 3.4 %collective-permute-start.20 = (bf16[1,512,128]{2,1,0:T(8,128)(2,1)S(1)}, bf16[1,512,128]{2,1,0:T(8,128)(2,1)S(1)}, u32[]{:S(2)}, u32[]{:S(2)}) collective-permute-start(bf16[1,512,128]{2,1,0:T(8,128)(2,1)S(1)} %constant_dynamic-slice_fusion.1), channel_id=1, source_target_pairs={{0,4},{1,13},{2,6},{3,15},{4,8},{5,1},{6,10},{7,3},{8,12},{9,5},{1... | collective-permute-start | bytes 393224 | tf_op jit(solution)/shard_map/ppermute | solution.py:41
  164.8 4.2 %collective-permute-done.20 = bf16[1,512,128]{2,1,0:T(8,128)(2,1)S(1)} collective-permute-done((bf16[1,512,128]{2,1,0:T(8,128)(2,1)S(1)}, bf16[1,512,128]{2,1,0:T(8,128)(2,1)S(1)}, u32[]{:S(2)}, u32[]{:S(2)}) %collective-permute-start.20) | collective-permute-done | bytes 131104 | tf_op jit(solution)/shard_map/ppermute | solution.py:41
  169.0 5.7 %collective-permute-start.21 = (bf16[7,512,128]{2,1,0:T(8,128)(2,1)S(1)}, bf16[7,512,128]{2,1,0:T(8,128)(2,1)S(1)}, u32[]{:S(2)}, u32[]{:S(2)}) collective-permute-start(bf16[7,512,128]{2,1,0:T(8,128)(2,1)S(1)} %constant_dynamic-update-slice_fusion.12.received), channel_id=1, source_target_pairs={{0,1},{1,0},{2,3},{3,2},{4,5},{5,4},{6,7},{7,6},{8,9},{9,8},{10,11... | collective-permute-start | bytes 2752520 | tf_op jit(solution)/shard_map/ppermute | solution.py:43
  174.7 2.1 %collective-permute-done.21.other = bf16[7,512,128]{2,1,0:T(8,128)(2,1)S(1)} collective-permute-done((bf16[7,512,128]{2,1,0:T(8,128)(2,1)S(1)}, bf16[7,512,128]{2,1,0:T(8,128)(2,1)S(1)}, u32[]{:S(2)}, u32[]{:S(2)}) %collective-permute-start.21) | collective-permute-done | bytes 917536 | tf_op jit(solution)/shard_map/ppermute | solution.py:43
  176.8 1.3 shard_map.78
  178.1 0.6 broadcast_in_dim.3
  178.8 6.3 %all-to-all-start = ((f32[16,4,128]{2,1,0:T(4,128)}), f32[16,4,128]{2,1,0:T(4,128)S(1)}, u32[]{:S(2)}, u32[]{:S(2)}) async-start(f32[16,4,128]{2,1,0:T(4,128)} %broadcast_in_dim.3), calls=%async_computation | async-start | bytes 65536 | tf_op jit(solution)/shard_map/all_to_all | solution.py:305
  185.0 7.4 %all-to-all-done.squares = f32[16,4,128]{2,1,0:T(4,128)S(1)} async-done(((f32[16,4,128]{2,1,0:T(4,128)}), f32[16,4,128]{2,1,0:T(4,128)S(1)}, u32[]{:S(2)}, u32[]{:S(2)}) %all-to-all-start) | async-done | bytes 32800 | tf_op jit(solution)/shard_map/all_to_all | solution.py:305
  192.4 0.8 shard_map.79
  (41 shorter events, 0.6 us)
Async XLA Ops:
  2.5 12.0 %collective-permute-start.1 = (bf16[2,512,128]{2,1,0:T(8,128)(2,1)S(1)}, bf16[2,512,128]{2,1,0:T(8,128)(2,1)S(1)}, u32[]{:S(2)}, u32[]{:S(2)}) collective-permute-start(bf16[2,512,128]{2,1,0:T(8,128)(2,1)S(1)} %bitcast.46), channel_id=1, source_target_pairs={{0,4},{1,13},{2,6},{3,15},{4,8},{5,1},{6,10},{7,3},{8,12},{9,5},{1... | collective-permute-start | bytes 786440 | tf_op jit(solution)/shard_map/ppermute | solution.py:38
  8.4 14.1 %collective-permute-start = (bf16[2,512,128]{2,1,0:T(8,128)(2,1)S(1)}, bf16[2,512,128]{2,1,0:T(8,128)(2,1)S(1)}, u32[]{:S(2)}, u32[]{:S(2)}) collective-permute-start(bf16[2,512,128]{2,1,0:T(8,128)(2,1)S(1)} %bitcast.47), channel_id=1, source_target_pairs={{0,2},{1,15},{2,4},{3,1},{4,6},{5,3},{6,8},{7,5},{8,10},{9,7},{10,... | collective-permute-start | bytes 786440 | tf_op jit(solution)/shard_map/ppermute | solution.py:37
  11.5 0.8 copy-start.9
  12.4 18.8 %copy-start.5 = (bf16[2,2048,128]{2,1,0:T(8,128)(2,1)S(1)}, bf16[2,2048,128]{2,1,0:T(8,128)(2,1)}, u32[]{:S(2)}) copy-start(bf16[2,2048,128]{2,1,0:T(8,128)(2,1)} %param.9) | copy-start | bytes 3145732
  14.5 8.1 %collective-permute-start.2 = (bf16[2,512,128]{2,1,0:T(8,128)(2,1)S(1)}, bf16[2,512,128]{2,1,0:T(8,128)(2,1)S(1)}, u32[]{:S(2)}, u32[]{:S(2)}) collective-permute-start(bf16[2,512,128]{2,1,0:T(8,128)(2,1)S(1)} %collective-permute-done.1), channel_id=1, source_target_pairs={{0,2},{1,15},{2,4},{3,1},{4,6},{5,3},{6,8},{7,5},{8,10},{9,7},{10,... | collective-permute-start | bytes 786440 | tf_op jit(solution)/shard_map/ppermute | solution.py:39
  18.6 7.9 %collective-permute-start.3 = (bf16[1,512,128]{2,1,0:T(8,128)(2,1)S(1)}, bf16[1,512,128]{2,1,0:T(8,128)(2,1)S(1)}, u32[]{:S(2)}, u32[]{:S(2)}) collective-permute-start(bf16[1,512,128]{2,1,0:T(8,128)(2,1)S(1)} %constant_dynamic-slice_fusion.4), channel_id=1, source_target_pairs={{0,4},{1,13},{2,6},{3,15},{4,8},{5,1},{6,10},{7,3},{8,12},{9,5},{1... | collective-permute-start | bytes 393224 | tf_op jit(solution)/shard_map/ppermute | solution.py:41
  26.5 4.7 %copy-start.7 = (bf16[2,2048,128]{2,1,0:T(8,128)(2,1)S(1)}, bf16[2,2048,128]{2,1,0:T(8,128)(2,1)}, u32[]{:S(2)}) copy-start(bf16[2,2048,128]{2,1,0:T(8,128)(2,1)} %param.11) | copy-start | bytes 3145732
  26.6 4.7 %copy-start.8 = (bf16[2,2048,128]{2,1,0:T(8,128)(2,1)S(1)}, bf16[2,2048,128]{2,1,0:T(8,128)(2,1)}, u32[]{:S(2)}) copy-start(bf16[2,2048,128]{2,1,0:T(8,128)(2,1)} %param.10) | copy-start | bytes 3145732
  26.6 6.7 %collective-permute-start.4 = (bf16[7,512,128]{2,1,0:T(8,128)(2,1)S(1)}, bf16[7,512,128]{2,1,0:T(8,128)(2,1)S(1)}, u32[]{:S(2)}, u32[]{:S(2)}) collective-permute-start(bf16[7,512,128]{2,1,0:T(8,128)(2,1)S(1)} %constant_dynamic-update-slice_fusion.received), channel_id=1, source_target_pairs={{0,1},{1,0},{2,3},{3,2},{4,5},{5,4},{6,7},{7,6},{8,9},{9,8},{10,11... | collective-permute-start | bytes 2752520 | tf_op jit(solution)/shard_map/ppermute | solution.py:43
  33.2 4.6 %copy-start = (bf16[7,512,128]{2,1,0:T(8,128)(2,1)}, bf16[7,512,128]{2,1,0:T(8,128)(2,1)S(1)}, u32[]{:S(2)}) copy-start(bf16[7,512,128]{2,1,0:T(8,128)(2,1)S(1)} %collective-permute-done.4.other) | copy-start | bytes 2752516
  37.8 0.7 copy-start.3
  38.4 12.9 %collective-permute-start.5 = (bf16[512,256]{1,0:T(8,128)(2,1)}, bf16[512,256]{1,0:T(8,128)(2,1)S(1)}, u32[]{:S(2)}, u32[]{:S(2)}) collective-permute-start(bf16[512,256]{1,0:T(8,128)(2,1)} %get-tuple-element.13.kv), channel_id=1, source_target_pairs={{0,16},{16,32},{32,48},{48,64},{64,80},{80,96},{96,112},{112,128},... | collective-permute-start | bytes 786440 | tf_op jit(solution)/shard_map/ppermute | solution.py:275
  41.5 9.8 %copy-start.2 = (f32[2,2,257]{2,1,0:T(2,128)S(1)}, f32[2,2,257]{2,1,0:T(2,128)}, u32[]{:S(2)}) copy-start(f32[2,2,257]{2,1,0:T(2,128)} %bias.3) | copy-start | bytes 12340
  51.3 0.9 copy-start.4
  59.4 28.9 %copy-start.6 = (bf16[2,2048,128]{2,1,0:T(8,128)(2,1)S(1)}, bf16[2,2048,128]{2,1,0:T(8,128)(2,1)}, u32[]{:S(2)}) copy-start(bf16[2,2048,128]{2,1,0:T(8,128)(2,1)} %param.12) | copy-start | bytes 3145732
  59.4 9.1 %collective-permute-start.7 = (bf16[2,512,128]{2,1,0:T(8,128)(2,1)S(1)}, bf16[2,512,128]{2,1,0:T(8,128)(2,1)S(1)}, u32[]{:S(2)}, u32[]{:S(2)}) collective-permute-start(bf16[2,512,128]{2,1,0:T(8,128)(2,1)S(1)} %bitcast.56), channel_id=1, source_target_pairs={{0,4},{1,13},{2,6},{3,15},{4,8},{5,1},{6,10},{7,3},{8,12},{9,5},{1... | collective-permute-start | bytes 786440 | tf_op jit(solution)/shard_map/ppermute | solution.py:38
  62.2 15.5 %collective-permute-start.6 = (bf16[2,512,128]{2,1,0:T(8,128)(2,1)S(1)}, bf16[2,512,128]{2,1,0:T(8,128)(2,1)S(1)}, u32[]{:S(2)}, u32[]{:S(2)}) collective-permute-start(bf16[2,512,128]{2,1,0:T(8,128)(2,1)S(1)} %bitcast.57), channel_id=1, source_target_pairs={{0,2},{1,15},{2,4},{3,1},{4,6},{5,3},{6,8},{7,5},{8,10},{9,7},{10,... | collective-permute-start | bytes 786440 | tf_op jit(solution)/shard_map/ppermute | solution.py:37
  68.5 9.5 %collective-permute-start.8 = (bf16[2,512,128]{2,1,0:T(8,128)(2,1)S(1)}, bf16[2,512,128]{2,1,0:T(8,128)(2,1)S(1)}, u32[]{:S(2)}, u32[]{:S(2)}) collective-permute-start(bf16[2,512,128]{2,1,0:T(8,128)(2,1)S(1)} %collective-permute-done.7), channel_id=1, source_target_pairs={{0,2},{1,15},{2,4},{3,1},{4,6},{5,3},{6,8},{7,5},{8,10},{9,7},{10,... | collective-permute-start | bytes 786440 | tf_op jit(solution)/shard_map/ppermute | solution.py:39
  74.7 7.6 %collective-permute-start.9 = (bf16[1,512,128]{2,1,0:T(8,128)(2,1)S(1)}, bf16[1,512,128]{2,1,0:T(8,128)(2,1)S(1)}, u32[]{:S(2)}, u32[]{:S(2)}) collective-permute-start(bf16[1,512,128]{2,1,0:T(8,128)(2,1)S(1)} %constant_dynamic-slice_fusion.3), channel_id=1, source_target_pairs={{0,4},{1,13},{2,6},{3,15},{4,8},{5,1},{6,10},{7,3},{8,12},{9,5},{1... | collective-permute-start | bytes 393224 | tf_op jit(solution)/shard_map/ppermute | solution.py:41
  82.4 8.0 %collective-permute-start.10 = (bf16[7,512,128]{2,1,0:T(8,128)(2,1)S(1)}, bf16[7,512,128]{2,1,0:T(8,128)(2,1)S(1)}, u32[]{:S(2)}, u32[]{:S(2)}) collective-permute-start(bf16[7,512,128]{2,1,0:T(8,128)(2,1)S(1)} %constant_dynamic-update-slice_fusion.4.received), channel_id=1, source_target_pairs={{0,1},{1,0},{2,3},{3,2},{4,5},{5,4},{6,7},{7,6},{8,9},{9,8},{10,11... | collective-permute-start | bytes 2752520 | tf_op jit(solution)/shard_map/ppermute | solution.py:43
  93.6 10.1 %collective-permute-start.12 = (bf16[2,512,128]{2,1,0:T(8,128)(2,1)S(1)}, bf16[2,512,128]{2,1,0:T(8,128)(2,1)S(1)}, u32[]{:S(2)}, u32[]{:S(2)}) collective-permute-start(bf16[2,512,128]{2,1,0:T(8,128)(2,1)S(1)} %bitcast.53), channel_id=1, source_target_pairs={{0,4},{1,13},{2,6},{3,15},{4,8},{5,1},{6,10},{7,3},{8,12},{9,5},{1... | collective-permute-start | bytes 786440 | tf_op jit(solution)/shard_map/ppermute | solution.py:38
  97.5 13.4 %collective-permute-start.11 = (bf16[2,512,128]{2,1,0:T(8,128)(2,1)S(1)}, bf16[2,512,128]{2,1,0:T(8,128)(2,1)S(1)}, u32[]{:S(2)}, u32[]{:S(2)}) collective-permute-start(bf16[2,512,128]{2,1,0:T(8,128)(2,1)S(1)} %bitcast.54), channel_id=1, source_target_pairs={{0,2},{1,15},{2,4},{3,1},{4,6},{5,3},{6,8},{7,5},{8,10},{9,7},{10,... | collective-permute-start | bytes 786440 | tf_op jit(solution)/shard_map/ppermute | solution.py:37
  103.7 8.0 %collective-permute-start.13 = (bf16[2,512,128]{2,1,0:T(8,128)(2,1)S(1)}, bf16[2,512,128]{2,1,0:T(8,128)(2,1)S(1)}, u32[]{:S(2)}, u32[]{:S(2)}) collective-permute-start(bf16[2,512,128]{2,1,0:T(8,128)(2,1)S(1)} %collective-permute-done.12), channel_id=1, source_target_pairs={{0,2},{1,15},{2,4},{3,1},{4,6},{5,3},{6,8},{7,5},{8,10},{9,7},{10,... | collective-permute-start | bytes 786440 | tf_op jit(solution)/shard_map/ppermute | solution.py:39
  108.5 13.3 %copy-start.1 = (bf16[7,512,128]{2,1,0:T(8,128)(2,1)S(1)}, bf16[7,512,128]{2,1,0:T(8,128)(2,1)}, u32[]{:S(2)}) copy-start(bf16[7,512,128]{2,1,0:T(8,128)(2,1)} %copy-done) | copy-start | bytes 2752516
  108.5 7.9 %collective-permute-start.14 = (bf16[1,512,128]{2,1,0:T(8,128)(2,1)S(1)}, bf16[1,512,128]{2,1,0:T(8,128)(2,1)S(1)}, u32[]{:S(2)}, u32[]{:S(2)}) collective-permute-start(bf16[1,512,128]{2,1,0:T(8,128)(2,1)S(1)} %constant_dynamic-slice_fusion.2), channel_id=1, source_target_pairs={{0,4},{1,13},{2,6},{3,15},{4,8},{5,1},{6,10},{7,3},{8,12},{9,5},{1... | collective-permute-start | bytes 393224 | tf_op jit(solution)/shard_map/ppermute | solution.py:41
  116.5 5.3 %collective-permute-start.15 = (bf16[7,512,128]{2,1,0:T(8,128)(2,1)S(1)}, bf16[7,512,128]{2,1,0:T(8,128)(2,1)S(1)}, u32[]{:S(2)}, u32[]{:S(2)}) collective-permute-start(bf16[7,512,128]{2,1,0:T(8,128)(2,1)S(1)} %constant_dynamic-update-slice_fusion.8.b_received), channel_id=1, source_target_pairs={{0,1},{1,0},{2,3},{3,2},{4,5},{5,4},{6,7},{7,6},{8,9},{9,8},{10,11... | collective-permute-start | bytes 2752520 | tf_op jit(solution)/shard_map/ppermute | solution.py:43
  127.1 12.7 %collective-permute-start.16 = (bf16[512,256]{1,0:T(8,128)(2,1)S(1)}, bf16[512,256]{1,0:T(8,128)(2,1)S(1)}, u32[]{:S(2)}, u32[]{:S(2)}) collective-permute-start(bf16[512,256]{1,0:T(8,128)(2,1)S(1)} %get-tuple-element.15.kv), channel_id=1, source_target_pairs={{0,16},{16,32},{32,48},{48,64},{64,80},{80,96},{96,112},{112,128},... | collective-permute-start | bytes 786440 | tf_op jit(solution)/shard_map/ppermute | solution.py:275
  146.1 8.8 %collective-permute-start.18 = (bf16[2,512,128]{2,1,0:T(8,128)(2,1)S(1)}, bf16[2,512,128]{2,1,0:T(8,128)(2,1)S(1)}, u32[]{:S(2)}, u32[]{:S(2)}) collective-permute-start(bf16[2,512,128]{2,1,0:T(8,128)(2,1)S(1)} %bitcast.50), channel_id=1, source_target_pairs={{0,4},{1,13},{2,6},{3,15},{4,8},{5,1},{6,10},{7,3},{8,12},{9,5},{1... | collective-permute-start | bytes 786440 | tf_op jit(solution)/shard_map/ppermute | solution.py:38
  149.2 15.5 %collective-permute-start.17 = (bf16[2,512,128]{2,1,0:T(8,128)(2,1)S(1)}, bf16[2,512,128]{2,1,0:T(8,128)(2,1)S(1)}, u32[]{:S(2)}, u32[]{:S(2)}) collective-permute-start(bf16[2,512,128]{2,1,0:T(8,128)(2,1)S(1)} %bitcast.51), channel_id=1, source_target_pairs={{0,2},{1,15},{2,4},{3,1},{4,6},{5,3},{6,8},{7,5},{8,10},{9,7},{10,... | collective-permute-start | bytes 786440 | tf_op jit(solution)/shard_map/ppermute | solution.py:37
  154.9 9.9 %collective-permute-start.19 = (bf16[2,512,128]{2,1,0:T(8,128)(2,1)S(1)}, bf16[2,512,128]{2,1,0:T(8,128)(2,1)S(1)}, u32[]{:S(2)}, u32[]{:S(2)}) collective-permute-start(bf16[2,512,128]{2,1,0:T(8,128)(2,1)S(1)} %collective-permute-done.18), channel_id=1, source_target_pairs={{0,2},{1,15},{2,4},{3,1},{4,6},{5,3},{6,8},{7,5},{8,10},{9,7},{10,... | collective-permute-start | bytes 786440 | tf_op jit(solution)/shard_map/ppermute | solution.py:39
  161.3 7.7 %collective-permute-start.20 = (bf16[1,512,128]{2,1,0:T(8,128)(2,1)S(1)}, bf16[1,512,128]{2,1,0:T(8,128)(2,1)S(1)}, u32[]{:S(2)}, u32[]{:S(2)}) collective-permute-start(bf16[1,512,128]{2,1,0:T(8,128)(2,1)S(1)} %constant_dynamic-slice_fusion.1), channel_id=1, source_target_pairs={{0,4},{1,13},{2,6},{3,15},{4,8},{5,1},{6,10},{7,3},{8,12},{9,5},{1... | collective-permute-start | bytes 393224 | tf_op jit(solution)/shard_map/ppermute | solution.py:41
  169.0 7.7 %collective-permute-start.21 = (bf16[7,512,128]{2,1,0:T(8,128)(2,1)S(1)}, bf16[7,512,128]{2,1,0:T(8,128)(2,1)S(1)}, u32[]{:S(2)}, u32[]{:S(2)}) collective-permute-start(bf16[7,512,128]{2,1,0:T(8,128)(2,1)S(1)} %constant_dynamic-update-slice_fusion.12.received), channel_id=1, source_target_pairs={{0,1},{1,0},{2,3},{3,2},{4,5},{5,4},{6,7},{7,6},{8,9},{9,8},{10,11... | collective-permute-start | bytes 2752520 | tf_op jit(solution)/shard_map/ppermute | solution.py:43
  178.8 13.6 %all-to-all-start = ((f32[16,4,128]{2,1,0:T(4,128)}), f32[16,4,128]{2,1,0:T(4,128)S(1)}, u32[]{:S(2)}, u32[]{:S(2)}) async-start(f32[16,4,128]{2,1,0:T(4,128)} %broadcast_in_dim.3), calls=%async_computation | async-start | bytes 65536 | tf_op jit(solution)/shard_map/all_to_all | solution.py:305

commit v2 on v1

v2 whole, which is shorter than its diff:
```python
import functools

import jax
import jax.numpy as jnp
from jax import lax
from jax.experimental import pallas as pl
from jax.experimental.pallas import tpu as pltpu
from jax.sharding import Mesh
from jax.sharding import PartitionSpec as P


D = 2048
HEAD = 64
BLK = 128
NB = 16
EPS = 1e-06
BIG = 60
NEG = -1e30
VMEM = pl.BlockSpec(memory_space=pltpu.VMEM)
SMEM = pl.BlockSpec(memory_space=pltpu.SMEM)
HBM = pl.BlockSpec(memory_space=pltpu.HBM)


def params(mib):
    return pltpu.CompilerParams(vmem_limit_bytes=mib * 1024 * 1024)


def core_pairs(step):
    pairs = []
    for y in range(8):
        for c in range(2):
            target = (y + (step if c == 0 else -step)) % 8
            pairs.append((2 * y + c, 2 * target + c))
    return pairs


def gather_blocks(x):
    core = lax.axis_index("c")

    own = lax.all_gather(x, "c", axis=0)
    two = lax.ppermute(own, ("y", "c"), core_pairs(2))
    one = lax.ppermute(own, ("y", "c"), core_pairs(1))
    half = lax.dynamic_index_in_dim(two, core, 0, keepdims=True)
    three = lax.ppermute(two, ("y", "c"), core_pairs(1))
    four = lax.ppermute(half, ("y", "c"), core_pairs(2))
    received = jnp.concatenate([one, two, three, four], axis=0)
    other = lax.ppermute(received, "c", [(0, 1), (1, 0)])
    return own, received, other


def block_ids():
    y = lax.axis_index("y")
    c = lax.axis_index("c")
    sign = 1 - 2 * c
    near = [(y - sign * d) % 8 for d in (1, 2, 3)]
    far = [(y + sign * d) % 8 for d in (1, 2, 3)]
    across = (y + 4) % 8
    ids = [2 * y, 2 * y + 1]
    for chip in near:
        ids += [2 * chip, 2 * chip + 1]
    ids.append(2 * across + c)
    for chip in far:
        ids += [2 * chip, 2 * chip + 1]
    ids.append(2 * across + 1 - c)
    return jnp.stack(ids).astype(jnp.int32)


def part(refs, k):
    own, received, other = refs
    if k < 2:
        return own, k
    if k < 9:
        return received, k - 2
    return other, k - 9


def scale_kernel(layer, count, ids, gain, *refs):
    weights, (out, *held, sems) = refs[:count], refs[count:]
    copies = [
        pltpu.make_async_copy(w.at[layer], dst, sems.at[n])
        for n, (w, dst) in enumerate(zip(weights, held))
    ]
    for copy in copies:
        copy.start()
    for copy in copies:
        copy.wait()
    for k in range(NB):
        t = ids[k]
        rows = pl.ds(pl.multiple_of(t * BLK, BLK), BLK)
        factor = jnp.broadcast_to(gain_row(gain, layer, 0, t), (BLK, BLK)).T
        for n, w in enumerate(held):
            scaled = w[rows, :].astype(jnp.float32) * factor
            out[k, :, n * BLK : (n + 1) * BLK] = scaled.astype(jnp.bfloat16)


def gain_row(gain, layer, kind, t):
    return gain[layer, kind : kind + 1, pl.ds(pl.multiple_of(t * BLK, BLK), BLK)]


def product(blocks, w):
    left = jnp.concatenate(blocks, axis=1)
    return jnp.dot(left, w[...].reshape(D, w.shape[2]), preferred_element_type=jnp.float32)


def blocks_of(refs):
    if len(refs) == 1:
        return [refs[0][k] for k in range(NB)]
    pairs = [part(refs, k) for k in range(NB)]
    return [ref[j] for ref, j in pairs]


def wide_inverse(total):
    inv = lax.rsqrt(jnp.sum(total, axis=1, keepdims=True) / D + EPS)
    return jnp.broadcast_to(inv, total.shape)


def first_kernel(own, received, other, w, kv_out, inv_out):
    refs = (own, received, other)

    def tile(i, carry):
        rows = pl.ds(pl.multiple_of(i * 64, 64), 64)
        total = jnp.zeros((64, BLK), jnp.float32)
        for k in range(NB):
            ref, j = part(refs, k)
            x = ref[j, rows, :].astype(jnp.float32)
            total += x * x
        inv_out[rows, :] = wide_inverse(total)
        return carry

    lax.fori_loop(0, own.shape[1] // 64, tile, 0)
    inv = inv_out[...]
    kv = product(blocks_of(refs), w)
    kv_out[...] = (kv * jnp.concatenate([inv, inv], axis=1)).astype(jnp.bfloat16)


def next_kernel(
    ids, mine, own, received, other, b_own, b_received, b_other, gain, w,
    kv_out, inv_out, stream, carried,
):
    refs = (own, received, other)
    b_refs = (b_own, b_received, b_other)

    def tile(i, carry):
        rows = pl.ds(pl.multiple_of(i * 64, 64), 64)

        def load(group, k):
            ref, j = part(group, k)
            return ref[j, rows, :].astype(jnp.float32)

        total = jnp.zeros((64, BLK), jnp.float32)
        for k in range(NB):
            x = load(b_refs, k)
            total += x * x
        inv_post = wide_inverse(total)
        total = jnp.zeros((64, BLK), jnp.float32)
        for k in range(NB):
            x = load(refs, k) + load(b_refs, k) * inv_post * gain_row(gain, 0, 1, ids[k])
            x = x.astype(jnp.bfloat16)
            stream[k, rows, :] = x
            x = x.astype(jnp.float32)
            total += x * x
        inv_out[rows, :] = wide_inverse(total)
        carried[rows, :] = stream[mine[0], rows, :]
        return carry

    lax.fori_loop(0, own.shape[1] // 64, tile, 0)
    inv = inv_out[...]
    kv = product(blocks_of((stream,)), w)
    kv_out[...] = (kv * jnp.concatenate([inv, inv], axis=1)).astype(jnp.bfloat16)


def grids():
    lane = lax.broadcasted_iota(jnp.int32, (BLK, BLK), 1)
    row = lax.broadcasted_iota(jnp.int32, (BLK, BLK), 0)
    return lane, row


def split_bias(bias, layer, h):
    low = bias[layer, h : h + 1, 0:BLK]
    high = bias[layer, h : h + 1, BLK : 2 * BLK]
    last = bias[layer, h : h + 1, 2 * BLK : 2 * BLK + 1]
    return low, high, last


def skewed(left, right):
    full = jnp.broadcast_to(jnp.concatenate([left, right], axis=1), (BLK, 2 * BLK))
    return pltpu.roll(full, 0, 1, stride=1, stride_axis=0)[:, :BLK].T


def head_scores(qh, keys):
    dims = (((1,), (1,)), ((), ()))
    return lax.dot_general(qh, keys, dims, preferred_element_type=jnp.float32)


def local_kernel(layer, x_count, *refs):
    xs, rest = refs[:x_count], refs[x_count:]
    w, inv, kv, bias, q_out, acc_out, top_out, sum_out, near_out = rest
    q = product(blocks_of(xs), w)
    q_out[...] = (q * inv[...] * HEAD ** (-0.5)).astype(jnp.bfloat16)
    lane, row = grids()
    tables = []
    for h in range(2):
        low, high, last = split_bias(bias, layer, h)
        last_row = jnp.broadcast_to(last, (1, BLK))
        diag = jnp.where((lane >= 64) & (row < 64), NEG, skewed(high, low))
        near_out[h] = skewed(last_row, high)
        tables.append((diag, near_out[h], jnp.broadcast_to(last, (BLK, BLK))))
    for i in range(4):
        rows = slice(i * BLK, (i + 1) * BLK)
        found = []
        for h in range(2):
            qh = q_out[rows, :]
            qh = jnp.where((lane < HEAD) == (h == 0), qh, jnp.zeros_like(qh))
            raw = head_scores(qh, kv[: (i + 1) * BLK, :BLK])
            scores = [
                raw[:, j * BLK : (j + 1) * BLK] + tables[h][min(i - j, 2)] for j in range(i + 1)
            ]
            top = jnp.max(functools.reduce(jnp.maximum, scores), axis=1, keepdims=True)
            weights = [jnp.exp(s - top) for s in scores]
            norm = jnp.sum(functools.reduce(jnp.add, weights), axis=1, keepdims=True)
            probs = jnp.concatenate([x.astype(jnp.bfloat16) for x in weights], axis=1)
            acc = jnp.dot(probs, kv[: (i + 1) * BLK, BLK:], preferred_element_type=jnp.float32)
            found.append((acc, top, norm))
        for n, out in enumerate((acc_out, top_out, sum_out)):
            out[rows, :] = jnp.where(lane < HEAD, found[0][n], found[1][n])


def merge_kernel(layer, first, q, kv, acc, top, total, nears, bias, out):
    lane, row = grids()
    hidden = jnp.where(first[0] == 1, NEG, 0.0)
    tables = []
    for h in range(2):
        last = split_bias(bias, layer, h)[2]
        full = jnp.broadcast_to(last, (BLK, BLK)) + hidden
        edge = jnp.where((lane < 64) & (row >= 64), NEG, full)
        tables.append((nears[h] + hidden, full, edge))
    for i in range(4):
        rows = slice(i * BLK, (i + 1) * BLK)
        found = []
        for h in range(2):
            near, full, edge = tables[h]
            qh = q[rows, :]
            qh = jnp.where((lane < HEAD) == (h == 0), qh, jnp.zeros_like(qh))
            raw = head_scores(qh, kv[i * BLK :, :BLK])
            scores = []
            for j in range(4 - i):
                term = edge if j == 0 else near if j == 3 else full
                scores.append(raw[:, j * BLK : (j + 1) * BLK] + term)
            old = top[rows, h * HEAD : h * HEAD + 1]
            peak = jnp.max(functools.reduce(jnp.maximum, scores), axis=1, keepdims=True)
            peak = jnp.maximum(peak, old)
            weights = [jnp.exp(s - peak) for s in scores]
            norm = jnp.sum(functools.reduce(jnp.add, weights), axis=1, keepdims=True)
            probs = jnp.concatenate([x.astype(jnp.bfloat16) for x in weights], axis=1)
            part_acc = jnp.dot(probs, kv[i * BLK :, BLK:], preferred_element_type=jnp.float32)
            found.append((part_acc, jnp.exp(old - peak), norm))
        more, fade, norm = (jnp.where(lane < HEAD, found[0][n], found[1][n]) for n in range(3))
        result = (acc[rows, :] * fade + more) / (total[rows, :] * fade + norm)
        out[rows, :] = result.astype(jnp.bfloat16)


def branch_of(ids, refs, w, acc):
    acc[...] = jnp.zeros_like(acc)
    for k in (0, 2, 4, 6, 9, 11, 13):
        ref, j = part(refs, k)
        pair = jnp.concatenate([ref[j], ref[j + 1]], axis=1)
        rows = pl.ds(pl.multiple_of(ids[k] * BLK, 2 * BLK), 2 * BLK)
        acc[...] += jnp.dot(pair, w[rows, :], preferred_element_type=jnp.float32)
    for k in (8, 15):
        ref, j = part(refs, k)
        rows = pl.ds(pl.multiple_of(ids[k] * BLK, BLK), BLK)
        acc[...] += jnp.dot(ref[j], w[rows, :], preferred_element_type=jnp.float32)


def out_kernel(ids, own, received, other, w, out, acc):
    branch_of(ids, (own, received, other), w, acc)
    out[...] = acc[...].astype(jnp.bfloat16)


def last_kernel(ids, own, received, other, w, out, squares):
    branch_of(ids, (own, received, other), w, out)
    for i in range(4):
        x = out[i * BLK : (i + 1) * BLK, :]
        sums = jnp.sum((x * x).T, axis=0, keepdims=True)
        for n in range(NB):
            squares[n, i : i + 1, :] = sums


def finish_kernel(ids, mine, squares, branch, stream, gain, out):
    total = jnp.sum(squares[...], axis=0)
    inv = lax.rsqrt(total / D + EPS)
    own_gain = gain_row(gain, 1, 1, ids[mine[0]])
    for i in range(4):
        rows = slice(i * BLK, (i + 1) * BLK)
        scale = jnp.broadcast_to(inv[i : i + 1, :], (BLK, BLK)).T
        x = stream[rows, :].astype(jnp.float32)
        out[rows, :] = (x + branch[rows, :] * scale * own_gain).astype(jnp.bfloat16)


def call(kernel, ins, outs, scratch, mib, flops, args):
    size = sum(a.size * a.dtype.itemsize for a in args)
    return pl.pallas_call(
        kernel,
        out_shape=outs,
        in_specs=ins,
        out_specs=jax.tree.map(lambda _: VMEM, outs),
        scratch_shapes=scratch,
        compiler_params=params(mib),
        cost_estimate=pl.CostEstimate(flops=flops, bytes_accessed=size, transcendentals=0),
    )(*args)


def on_device(residual, gains, w_query, w_key, w_value, w_out, rel_bias):
    tokens = residual.shape[0]
    half = jnp.bfloat16
    ids = block_ids()
    core = lax.axis_index("c")
    mine = core.reshape(1).astype(jnp.int32)
    first = (lax.axis_index("sp") == 0).reshape(1).astype(jnp.int32)
    block = jax.ShapeDtypeStruct((tokens, BLK), half)
    pair = jax.ShapeDtypeStruct((tokens, 2 * BLK), half)
    wide = jax.ShapeDtypeStruct((tokens, BLK), jnp.float32)
    stack = jax.ShapeDtypeStruct((NB, tokens, BLK), half)
    tiles = jax.ShapeDtypeStruct((2, BLK, BLK), jnp.float32)
    flow = lax.axis_size("sp")
    shift = [(i, i + 1) for i in range(flow - 1)]

    def scaled(layer, weights, mib):
        count = len(weights)
        shape = jax.ShapeDtypeStruct((NB, BLK, count * BLK), half)
        scratch = [pltpu.VMEM((D, BLK), half)] * count + [pltpu.SemaphoreType.DMA((count,))]
        return call(
            functools.partial(scale_kernel, layer, count), [SMEM, VMEM] + [HBM] * count,
            shape, scratch, mib, 10**9, (ids, gains, *weights),
        )

    def attention(layer, xs, wq, kv, inv):
        previous = lax.ppermute(kv, "sp", shift)
        local = call(
            functools.partial(local_kernel, layer, len(xs)), [VMEM] * (len(xs) + 4),
            (block, wide, wide, wide, tiles), [], 4, 2 * 10**9, (*xs, wq, inv, kv, rel_bias),
        )
        return call(
            functools.partial(merge_kernel, layer), [SMEM] + [VMEM] * 7, block, [], 4,
            10**9, (first, local[0], previous, *local[1:], rel_bias),
        )

    wkv = scaled(0, (w_key, w_value), BIG)
    wq = scaled(0, (w_query,), 4)
    stream = gather_blocks(residual)
    kv, inv = call(
        first_kernel, [VMEM] * 4, (pair, wide), [], 4, 2 * 10**9, (*stream, wkv),
    )
    attended = gather_blocks(attention(0, stream, wq, kv, inv))
    branch = call(
        out_kernel, [SMEM] + [VMEM] * 4, block, [pltpu.VMEM((tokens, BLK), jnp.float32)], 4,
        10**9, (ids, *attended, w_out[0]),
    )
    branch = gather_blocks(branch)
    wkv = scaled(1, (w_key, w_value), 4)
    wq = scaled(1, (w_query,), 4)
    kv, inv, full, carried = call(
        next_kernel, [SMEM] * 2 + [VMEM] * 8, (pair, wide, stack, block), [], 4, 2 * 10**9,
        (ids, mine, *stream, *branch, gains, wkv),
    )
    attended = gather_blocks(attention(1, (full,), wq, kv, inv))
    branch, squares = call(
        last_kernel, [SMEM] + [VMEM] * 4,
        (wide, jax.ShapeDtypeStruct((NB, tokens // BLK, BLK), jnp.float32)), [], 4, 10**9,
        (ids, *attended, w_out[1]),
    )
    everything = lax.all_to_all(squares, ("y", "c"), split_axis=0, concat_axis=0, tiled=True)
    return call(
        finish_kernel, [SMEM] * 2 + [VMEM] * 4, block, [], 4, 10**7,
        (ids, mine, everything, branch, carried, gains),
    )


def solution(mesh):
    finer = Mesh(mesh.devices.reshape(mesh.shape["sp"], 8, 2), ("sp", "y", "c"))
    tp = ("y", "c")
    in_specs = (
        P("sp", tp),
        P(),
        P(None, None, tp),
        P(None, None, tp),
        P(None, None, tp),
        P(None, None, tp),
        P(None, tp, None),
    )

    return jax.shard_map(
        on_device, mesh=finer, in_specs=in_specs, out_specs=P("sp", tp), check_vma=False
    )
```

time: 194 us -> 188 us (0.969)
  waiting for transfers between devices: 60.2 us -> 42.1 us
  blocking collectives: 10.2 us -> 23.5 us
  starting transfers between devices: 97.3 us -> 91.2 us
  Pallas kernels: 21 us -> 26.5 us
    all_to_all x0 -> x1, blocking collectives: none -> 13.4 us  [on_device(): lax.all_to_all(squares, ('y', 'c'), split_axis=0, concat_axis=0, tiled=True)]
    ppermute x2, waiting for transfers between devices: 20.5 us -> 11.9 us  [attention(): previous = lax.ppermute(kv, 'sp', shift)]
    all_to_all x1 -> x0, waiting for transfers between devices: 7.38 us -> none  [on_device(): lax.all_to_all(copies, ('y', 'c'), split_axis=0, concat_axis=0, tiled=True)]
    all_to_all x1 -> x0, starting transfers between devices: 6.25 us -> none  [on_device(): lax.all_to_all(copies, ('y', 'c'), split_axis=0, concat_axis=0, tiled=True)]
    pallas_call x7 -> x13, Pallas kernels: 21 us -> 26.5 us  [call(): pl.pallas_call(kernel, out_shape=outs, in_specs=ins, out_specs=jax.tree.m...]
    ppermute x4, waiting for transfers between devices: 7.97 us -> 5.14 us  [gather_blocks(): other = lax.ppermute(received, 'c', [(0, 1), (1, 0)])]
  transfers between devices with their start and end apart: 23 -> 22, of which waited for: 15 -> 12; matrix products, arithmetic and copies ran while one was open for 0% -> 1% of each run, Pallas kernels for 0% -> 7%
where the time goes in v2:
time: 188 us; the launch traced here: 187 us
  starting transfers between devices  91.2 us (49%)
  waiting for transfers between devices  42.1 us (22%)
  Pallas kernels  26.5 us (14%)
  blocking collectives  23.5 us (12%)
  local copies, waits for them, and re-layouts  2.56 us (1%)
    pallas_call x13, Pallas kernels, call(): pl.pallas_call(kernel, out_shape=outs, in_specs=ins, out_specs=jax.tree.m...  26.5 us
    ppermute x4, starting transfers between devices, gather_blocks(): three = lax.ppermute(two, ('y', 'c'), core_pairs(1))  21 us
    ppermute x4, starting transfers between devices, gather_blocks(): other = lax.ppermute(received, 'c', [(0, 1), (1, 0)])  19.1 us
    ppermute x4, starting transfers between devices, gather_blocks(): one = lax.ppermute(own, ('y', 'c'), core_pairs(1))  17 us
    ppermute x4, waiting for transfers between devices, gather_blocks(): four = lax.ppermute(half, ('y', 'c'), core_pairs(2))  16.8 us
    ppermute x4, starting transfers between devices, gather_blocks(): two = lax.ppermute(own, ('y', 'c'), core_pairs(2))  15.6 us
    all_to_all x1, blocking collectives, on_device(): lax.all_to_all(squares, ('y', 'c'), split_axis=0, concat_axis=0, tiled=True)  13.4 us
    ppermute x4, starting transfers between devices, gather_blocks(): four = lax.ppermute(half, ('y', 'c'), core_pairs(2))  13.2 us
  transfers between devices with their start and end apart: 22, of which 12 were waited for; matrix products, arithmetic and copies ran while one was open for 1% of the time, Pallas kernels for 7%

profile of v2, /device:TPU:257, one launch (start us, length us, event | category | flops | bytes accessed | tf_op | source)
XLA Modules:
  0.0 186.6 jit_solution(3861548971846450412)
XLA Ops:
  0.0 2.5 %all-gather = bf16[1024,128]{1,0:T(8,128)(2,1)S(1)} all-gather(bf16[512,128]{1,0:T(8,128)(2,1)} %param.7), channel_id=2, replica_groups=mesh['sp'=32,'y'=8,'c'=2] {'c'}, dimensions={0}, use_global_device_ids=true | all-gather | bytes 393216 | tf_op jit(solution)/shard_map/all_gather | solution.py:40
  2.5 5.9 %collective-permute-start.1 = (bf16[2,512,128]{2,1,0:T(8,128)(2,1)S(1)}, bf16[2,512,128]{2,1,0:T(8,128)(2,1)S(1)}, u32[]{:S(2)}, u32[]{:S(2)}) collective-permute-start(bf16[2,512,128]{2,1,0:T(8,128)(2,1)S(1)} %bitcast.26), channel_id=1, source_target_pairs={{0,4},{1,13},{2,6},{3,15},{4,8},{5,1},{6,10},{7,3},{8,12},{9,5},{1... | collective-permute-start | bytes 786440 | tf_op jit(solution)/shard_map/ppermute | solution.py:41
  8.4 3.0 %collective-permute-start = (bf16[2,512,128]{2,1,0:T(8,128)(2,1)S(1)}, bf16[2,512,128]{2,1,0:T(8,128)(2,1)S(1)}, u32[]{:S(2)}, u32[]{:S(2)}) collective-permute-start(bf16[2,512,128]{2,1,0:T(8,128)(2,1)S(1)} %bitcast.27), channel_id=1, source_target_pairs={{0,2},{1,15},{2,4},{3,1},{4,6},{5,3},{6,8},{7,5},{8,10},{9,7},{10,... | collective-permute-start | bytes 786440 | tf_op jit(solution)/shard_map/ppermute | solution.py:42
  11.4 3.1 %collective-permute-done.1 = bf16[2,512,128]{2,1,0:T(8,128)(2,1)S(1)} collective-permute-done((bf16[2,512,128]{2,1,0:T(8,128)(2,1)S(1)}, bf16[2,512,128]{2,1,0:T(8,128)(2,1)S(1)}, u32[]{:S(2)}, u32[]{:S(2)}) %collective-permute-start.1) | collective-permute-done | bytes 262176 | tf_op jit(solution)/shard_map/ppermute | solution.py:41
  14.5 4.1 %collective-permute-start.2 = (bf16[2,512,128]{2,1,0:T(8,128)(2,1)S(1)}, bf16[2,512,128]{2,1,0:T(8,128)(2,1)S(1)}, u32[]{:S(2)}, u32[]{:S(2)}) collective-permute-start(bf16[2,512,128]{2,1,0:T(8,128)(2,1)S(1)} %collective-permute-done.1), channel_id=1, source_target_pairs={{0,2},{1,15},{2,4},{3,1},{4,6},{5,3},{6,8},{7,5},{8,10},{9,7},{10,... | collective-permute-start | bytes 786440 | tf_op jit(solution)/shard_map/ppermute | solution.py:44
  18.6 3.9 %collective-permute-start.3 = (bf16[1,512,128]{2,1,0:T(8,128)(2,1)S(1)}, bf16[1,512,128]{2,1,0:T(8,128)(2,1)S(1)}, u32[]{:S(2)}, u32[]{:S(2)}) collective-permute-start(bf16[1,512,128]{2,1,0:T(8,128)(2,1)S(1)} %constant_dynamic-slice_fusion.3), channel_id=1, source_target_pairs={{0,4},{1,13},{2,6},{3,15},{4,8},{5,1},{6,10},{7,3},{8,12},{9,5},{1... | collective-permute-start | bytes 393224 | tf_op jit(solution)/shard_map/ppermute | solution.py:45
  22.5 0.0 collective-permute-done
  22.5 0.0 collective-permute-done.2
  22.6 3.9 %collective-permute-done.3 = bf16[1,512,128]{2,1,0:T(8,128)(2,1)S(1)} collective-permute-done((bf16[1,512,128]{2,1,0:T(8,128)(2,1)S(1)}, bf16[1,512,128]{2,1,0:T(8,128)(2,1)S(1)}, u32[]{:S(2)}, u32[]{:S(2)}) %collective-permute-start.3) | collective-permute-done | bytes 131104 | tf_op jit(solution)/shard_map/ppermute | solution.py:45
  26.5 4.4 %collective-permute-start.4 = (bf16[7,512,128]{2,1,0:T(8,128)(2,1)S(1)}, bf16[7,512,128]{2,1,0:T(8,128)(2,1)S(1)}, u32[]{:S(2)}, u32[]{:S(2)}) collective-permute-start(bf16[7,512,128]{2,1,0:T(8,128)(2,1)S(1)} %constant_dynamic-update-slice_fusion.received.refs_1_), channel_id=1, source_target_pairs={{0,1},{1,0},{2,3},{3,2},{4,5},{5,4},{6,7},{7,6},{8,9},{9,8},{10,11... | collective-permute-start | bytes 2752520 | tf_op jit(solution)/shard_map/ppermute | solution.py:47
  31.1 0.6 stack.67.ids
  31.7 3.3 %shard_map.74.w = bf16[16,128,256]{2,1,0:T(8,128)(2,1)} custom-call(s32[16]{0:T(128)} %stack.67.ids, f32[2,2,2048]{2,1,0:T(2,128)} %gain.11, bf16[2,2048,128]{2,1,0:T(8,128)(2,1)} %refs_0_.6, bf16[2,2048,128]{2,1,0:T(8,128)(2,1)} %refs_1_.3), custom_call_target="tpu_custom_call" | custom-call | flops 1000000000 | bytes 2129984 | tf_op jit(solution)/shard_map/pallas_call | solution.py:302
  35.1 0.0 copy-start
  35.1 0.0 copy-start.4
  35.1 0.0 collective-permute-done.4.other.refs_2_
  35.1 1.3 copy-done.6
  36.4 1.5 shard_map.75
  37.9 0.0 copy-start.5
  38.0 3.1 %collective-permute-start.5 = (bf16[512,256]{1,0:T(8,128)(2,1)S(1)}, bf16[512,256]{1,0:T(8,128)(2,1)S(1)}, u32[]{:S(2)}, u32[]{:S(2)}) collective-permute-start(bf16[512,256]{1,0:T(8,128)(2,1)S(1)} %get-tuple-element.24.refs_5_), channel_id=1, source_target_pairs={{0,16},{16,32},{32,48},{48,64},{64,80},{80,96},{96,112},{112,128},... | collective-permute-start | bytes 786440 | tf_op jit(solution)/shard_map/ppermute | solution.py:338
  41.1 0.9 shard_map.73.refs_3_
  42.1 3.3 %shard_map.76 = (bf16[512,128]{1,0:T(8,128)(2,1)S(1)}, f32[512,128]{1,0:T(8,128)S(1)}, f32[512,128]{1,0:T(8,128)S(1)}, f32[512,128]{1,0:T(8,128)S(1)}, f32[2,128,128]{2,1,0:T(8,128)S(1)}) custom-call(bf16[2,512,128]{2,1,0:T(8,128)(2,1)S(1)} %bitcast.29, bf16[7,512,128]{2,1,0:T(8,128)(2,1)S(1)} %constant_dynamic-update-slice_fusion.received.refs_1_, ...), custom_call_target="tpu_custom_call" | custom-call | flops 2000000000 | bytes 3149840 | tf_op jit(solution)/shard_map/pallas_call | solution.py:302
  45.4 5.6 %collective-permute-done.5.kv = bf16[512,256]{1,0:T(8,128)(2,1)S(1)} collective-permute-done((bf16[512,256]{1,0:T(8,128)(2,1)S(1)}, bf16[512,256]{1,0:T(8,128)(2,1)S(1)}, u32[]{:S(2)}, u32[]{:S(2)}) %collective-permute-start.5) | collective-permute-done | bytes 262176 | tf_op jit(solution)/shard_map/ppermute | solution.py:338
  51.0 2.3 %shard_map.77 = bf16[512,128]{1,0:T(8,128)(2,1)S(1)} custom-call(s32[1]{0:T(128)} %bitcast.17.first, bf16[512,128]{1,0:T(8,128)(2,1)S(1)} %get-tuple-element.25.q, bf16[512,256]{1,0:T(8,128)(2,1)S(1)} %collective-permute-done.5.kv, f32[512,128]{1,0:T(8,128)S(1)} %get-tuple-element.26.acc, f32[512,128]{1,0:T(8,128)S(1)} %get-tuple-element.27.top, ...), custom_call_target="tpu_custom_call" | custom-call | flops 1000000000 | bytes 1314836 | tf_op jit(solution)/shard_map/pallas_call | solution.py:302
  53.3 0.0 copy-start.7
  53.3 2.6 %all-gather.1 = bf16[1024,128]{1,0:T(8,128)(2,1)S(1)} all-gather(bf16[512,128]{1,0:T(8,128)(2,1)S(1)} %shard_map.77), channel_id=3, replica_groups=mesh['sp'=32,'y'=8,'c'=2] {'c'}, dimensions={0}, use_global_device_ids=true | all-gather | bytes 393216 | tf_op jit(solution)/shard_map/all_gather | solution.py:40
  56.0 2.7 %collective-permute-start.7 = (bf16[2,512,128]{2,1,0:T(8,128)(2,1)S(1)}, bf16[2,512,128]{2,1,0:T(8,128)(2,1)S(1)}, u32[]{:S(2)}, u32[]{:S(2)}) collective-permute-start(bf16[2,512,128]{2,1,0:T(8,128)(2,1)S(1)} %bitcast.37), channel_id=1, source_target_pairs={{0,4},{1,13},{2,6},{3,15},{4,8},{5,1},{6,10},{7,3},{8,12},{9,5},{1... | collective-permute-start | bytes 786440 | tf_op jit(solution)/shard_map/ppermute | solution.py:41
  58.6 6.3 %collective-permute-start.6 = (bf16[2,512,128]{2,1,0:T(8,128)(2,1)S(1)}, bf16[2,512,128]{2,1,0:T(8,128)(2,1)S(1)}, u32[]{:S(2)}, u32[]{:S(2)}) collective-permute-start(bf16[2,512,128]{2,1,0:T(8,128)(2,1)S(1)} %bitcast.38), channel_id=1, source_target_pairs={{0,2},{1,15},{2,4},{3,1},{4,6},{5,3},{6,8},{7,5},{8,10},{9,7},{10,... | collective-permute-start | bytes 786440 | tf_op jit(solution)/shard_map/ppermute | solution.py:42
  64.9 5.9 %collective-permute-start.8 = (bf16[2,512,128]{2,1,0:T(8,128)(2,1)S(1)}, bf16[2,512,128]{2,1,0:T(8,128)(2,1)S(1)}, u32[]{:S(2)}, u32[]{:S(2)}) collective-permute-start(bf16[2,512,128]{2,1,0:T(8,128)(2,1)S(1)} %collective-permute-done.7), channel_id=1, source_target_pairs={{0,2},{1,15},{2,4},{3,1},{4,6},{5,3},{6,8},{7,5},{8,10},{9,7},{10,... | collective-permute-start | bytes 786440 | tf_op jit(solution)/shard_map/ppermute | solution.py:44
  70.9 3.6 %collective-permute-start.9 = (bf16[1,512,128]{2,1,0:T(8,128)(2,1)S(1)}, bf16[1,512,128]{2,1,0:T(8,128)(2,1)S(1)}, u32[]{:S(2)}, u32[]{:S(2)}) collective-permute-start(bf16[1,512,128]{2,1,0:T(8,128)(2,1)S(1)} %constant_dynamic-slice_fusion.2), channel_id=1, source_target_pairs={{0,4},{1,13},{2,6},{3,15},{4,8},{5,1},{6,10},{7,3},{8,12},{9,5},{1... | collective-permute-start | bytes 393224 | tf_op jit(solution)/shard_map/ppermute | solution.py:45
  74.6 4.2 %collective-permute-done.9 = bf16[1,512,128]{2,1,0:T(8,128)(2,1)S(1)} collective-permute-done((bf16[1,512,128]{2,1,0:T(8,128)(2,1)S(1)}, bf16[1,512,128]{2,1,0:T(8,128)(2,1)S(1)}, u32[]{:S(2)}, u32[]{:S(2)}) %collective-permute-start.9) | collective-permute-done | bytes 131104 | tf_op jit(solution)/shard_map/ppermute | solution.py:45
  78.9 5.8 %collective-permute-start.10 = (bf16[7,512,128]{2,1,0:T(8,128)(2,1)S(1)}, bf16[7,512,128]{2,1,0:T(8,128)(2,1)S(1)}, u32[]{:S(2)}, u32[]{:S(2)}) collective-permute-start(bf16[7,512,128]{2,1,0:T(8,128)(2,1)S(1)} %constant_dynamic-update-slice_fusion.4.received), channel_id=1, source_target_pairs={{0,1},{1,0},{2,3},{3,2},{4,5},{5,4},{6,7},{7,6},{8,9},{9,8},{10,11... | collective-permute-start | bytes 2752520 | tf_op jit(solution)/shard_map/ppermute | solution.py:47
  84.8 0.1 slice_bitcast_fusion
  84.8 2.0 %collective-permute-done.10.other = bf16[7,512,128]{2,1,0:T(8,128)(2,1)S(1)} collective-permute-done((bf16[7,512,128]{2,1,0:T(8,128)(2,1)S(1)}, bf16[7,512,128]{2,1,0:T(8,128)(2,1)S(1)}, u32[]{:S(2)}, u32[]{:S(2)}) %collective-permute-start.10) | collective-permute-done | bytes 917536 | tf_op jit(solution)/shard_map/ppermute | solution.py:47
  86.8 1.3 shard_map.78
  88.1 0.0 copy-start.2
  88.1 0.0 copy-start.3
  88.1 2.1 %all-gather.2 = bf16[1024,128]{1,0:T(8,128)(2,1)S(1)} all-gather(bf16[512,128]{1,0:T(8,128)(2,1)S(1)} %shard_map.78), channel_id=4, replica_groups=mesh['sp'=32,'y'=8,'c'=2] {'c'}, dimensions={0}, use_global_device_ids=true | all-gather | bytes 393216 | tf_op jit(solution)/shard_map/all_gather | solution.py:40
  90.3 3.8 %collective-permute-start.12 = (bf16[2,512,128]{2,1,0:T(8,128)(2,1)S(1)}, bf16[2,512,128]{2,1,0:T(8,128)(2,1)S(1)}, u32[]{:S(2)}, u32[]{:S(2)}) collective-permute-start(bf16[2,512,128]{2,1,0:T(8,128)(2,1)S(1)} %bitcast.31), channel_id=1, source_target_pairs={{0,4},{1,13},{2,6},{3,15},{4,8},{5,1},{6,10},{7,3},{8,12},{9,5},{1... | collective-permute-start | bytes 786440 | tf_op jit(solution)/shard_map/ppermute | solution.py:41
  94.1 2.1 %collective-permute-start.11 = (bf16[2,512,128]{2,1,0:T(8,128)(2,1)S(1)}, bf16[2,512,128]{2,1,0:T(8,128)(2,1)S(1)}, u32[]{:S(2)}, u32[]{:S(2)}) collective-permute-start(bf16[2,512,128]{2,1,0:T(8,128)(2,1)S(1)} %bitcast.32), channel_id=1, source_target_pairs={{0,2},{1,15},{2,4},{3,1},{4,6},{5,3},{6,8},{7,5},{8,10},{9,7},{10,... | collective-permute-start | bytes 786440 | tf_op jit(solution)/shard_map/ppermute | solution.py:42
  96.2 4.1 %collective-permute-done.12 = bf16[2,512,128]{2,1,0:T(8,128)(2,1)S(1)} collective-permute-done((bf16[2,512,128]{2,1,0:T(8,128)(2,1)S(1)}, bf16[2,512,128]{2,1,0:T(8,128)(2,1)S(1)}, u32[]{:S(2)}, u32[]{:S(2)}) %collective-permute-start.12) | collective-permute-done | bytes 262176 | tf_op jit(solution)/shard_map/ppermute | solution.py:41
  100.3 4.8 %collective-permute-start.13 = (bf16[2,512,128]{2,1,0:T(8,128)(2,1)S(1)}, bf16[2,512,128]{2,1,0:T(8,128)(2,1)S(1)}, u32[]{:S(2)}, u32[]{:S(2)}) collective-permute-start(bf16[2,512,128]{2,1,0:T(8,128)(2,1)S(1)} %collective-permute-done.12), channel_id=1, source_target_pairs={{0,2},{1,15},{2,4},{3,1},{4,6},{5,3},{6,8},{7,5},{8,10},{9,7},{10,... | collective-permute-start | bytes 786440 | tf_op jit(solution)/shard_map/ppermute | solution.py:44
  105.1 2.2 %collective-permute-start.14 = (bf16[1,512,128]{2,1,0:T(8,128)(2,1)S(1)}, bf16[1,512,128]{2,1,0:T(8,128)(2,1)S(1)}, u32[]{:S(2)}, u32[]{:S(2)}) collective-permute-start(bf16[1,512,128]{2,1,0:T(8,128)(2,1)S(1)} %constant_dynamic-slice_fusion.1), channel_id=1, source_target_pairs={{0,4},{1,13},{2,6},{3,15},{4,8},{5,1},{6,10},{7,3},{8,12},{9,5},{1... | collective-permute-start | bytes 393224 | tf_op jit(solution)/shard_map/ppermute | solution.py:45
  107.4 1.0 collective-permute-done.13
  108.4 4.6 %collective-permute-done.14 = bf16[1,512,128]{2,1,0:T(8,128)(2,1)S(1)} collective-permute-done((bf16[1,512,128]{2,1,0:T(8,128)(2,1)S(1)}, bf16[1,512,128]{2,1,0:T(8,128)(2,1)S(1)}, u32[]{:S(2)}, u32[]{:S(2)}) %collective-permute-start.14) | collective-permute-done | bytes 131104 | tf_op jit(solution)/shard_map/ppermute | solution.py:45
  113.0 3.1 %collective-permute-start.15 = (bf16[7,512,128]{2,1,0:T(8,128)(2,1)S(1)}, bf16[7,512,128]{2,1,0:T(8,128)(2,1)S(1)}, u32[]{:S(2)}, u32[]{:S(2)}) collective-permute-start(bf16[7,512,128]{2,1,0:T(8,128)(2,1)S(1)} %constant_dynamic-update-slice_fusion.8.b_received), channel_id=1, source_target_pairs={{0,1},{1,0},{2,3},{3,2},{4,5},{5,4},{6,7},{7,6},{8,9},{9,8},{10,11... | collective-permute-start | bytes 2752520 | tf_op jit(solution)/shard_map/ppermute | solution.py:47
  116.2 1.0 shard_map.79.w
  117.1 1.1 collective-permute-done.15.b_other
  118.2 3.6 %shard_map.80 = (bf16[512,256]{1,0:T(8,128)(2,1)S(1)}, f32[512,128]{1,0:T(8,128)S(1)}, bf16[16,512,128]{2,1,0:T(8,128)(2,1)S(1)}, bf16[512,128]{1,0:T(8,128)(2,1)S(1)}) custom-call(s32[16]{0:T(128)S(1)} %copy-done.1, s32[1]{0:T(128)} %bitcast.16.mine, bf16[2,512,128]{2,1,0:T(8,128)(2,1)S(1)} %bitcast.30, ...), custom_call_target="tpu_custom_call" | custom-call | flops 2000000000 | bytes 5275716 | tf_op jit(solution)/shard_map/pallas_call | solution.py:302
  121.8 2.1 %collective-permute-start.16 = (bf16[512,256]{1,0:T(8,128)(2,1)S(1)}, bf16[512,256]{1,0:T(8,128)(2,1)S(1)}, u32[]{:S(2)}, u32[]{:S(2)}) collective-permute-start(bf16[512,256]{1,0:T(8,128)(2,1)S(1)} %get-tuple-element.32.refs_3_), channel_id=1, source_target_pairs={{0,16},{16,32},{32,48},{48,64},{64,80},{80,96},{96,112},{112,128},... | collective-permute-start | bytes 786440 | tf_op jit(solution)/shard_map/ppermute | solution.py:338
  124.0 0.9 shard_map.81.refs_1_
  124.9 3.3 %shard_map.82 = (bf16[512,128]{1,0:T(8,128)(2,1)S(1)}, f32[512,128]{1,0:T(8,128)S(1)}, f32[512,128]{1,0:T(8,128)S(1)}, f32[512,128]{1,0:T(8,128)S(1)}, f32[2,128,128]{2,1,0:T(8,128)S(1)}) custom-call(bf16[16,512,128]{2,1,0:T(8,128)(2,1)S(1)} %get-tuple-element.30.refs_0_, bf16[16,128,128]{2,1,0:T(8,128)(2,1)S(1)} %shard_map.81.refs_1_, ...), custom_call_target="tpu_custom_call" | custom-call | flops 2000000000 | bytes 3149840 | tf_op jit(solution)/shard_map/pallas_call | solution.py:302
  128.2 6.3 %collective-permute-done.16.kv = bf16[512,256]{1,0:T(8,128)(2,1)S(1)} collective-permute-done((bf16[512,256]{1,0:T(8,128)(2,1)S(1)}, bf16[512,256]{1,0:T(8,128)(2,1)S(1)}, u32[]{:S(2)}, u32[]{:S(2)}) %collective-permute-start.16) | collective-permute-done | bytes 262176 | tf_op jit(solution)/shard_map/ppermute | solution.py:338
  134.6 2.3 %shard_map.83 = bf16[512,128]{1,0:T(8,128)(2,1)S(1)} custom-call(s32[1]{0:T(128)} %bitcast.17.first, bf16[512,128]{1,0:T(8,128)(2,1)S(1)} %get-tuple-element.33.q, bf16[512,256]{1,0:T(8,128)(2,1)S(1)} %collective-permute-done.16.kv, f32[512,128]{1,0:T(8,128)S(1)} %get-tuple-element.34.acc, f32[512,128]{1,0:T(8,128)S(1)} %get-tuple-element.35.top, ...), custom_call_target="tpu_custom_call" | custom-call | flops 1000000000 | bytes 1314836 | tf_op jit(solution)/shard_map/pallas_call | solution.py:302
  136.9 2.8 %all-gather.3 = bf16[1024,128]{1,0:T(8,128)(2,1)S(1)} all-gather(bf16[512,128]{1,0:T(8,128)(2,1)S(1)} %shard_map.83), channel_id=5, replica_groups=mesh['sp'=32,'y'=8,'c'=2] {'c'}, dimensions={0}, use_global_device_ids=true | all-gather | bytes 393216 | tf_op jit(solution)/shard_map/all_gather | solution.py:40
  139.7 3.2 %collective-permute-start.18 = (bf16[2,512,128]{2,1,0:T(8,128)(2,1)S(1)}, bf16[2,512,128]{2,1,0:T(8,128)(2,1)S(1)}, u32[]{:S(2)}, u32[]{:S(2)}) collective-permute-start(bf16[2,512,128]{2,1,0:T(8,128)(2,1)S(1)} %bitcast.34), channel_id=1, source_target_pairs={{0,4},{1,13},{2,6},{3,15},{4,8},{5,1},{6,10},{7,3},{8,12},{9,5},{1... | collective-permute-start | bytes 786440 | tf_op jit(solution)/shard_map/ppermute | solution.py:41
  142.9 5.7 %collective-permute-start.17 = (bf16[2,512,128]{2,1,0:T(8,128)(2,1)S(1)}, bf16[2,512,128]{2,1,0:T(8,128)(2,1)S(1)}, u32[]{:S(2)}, u32[]{:S(2)}) collective-permute-start(bf16[2,512,128]{2,1,0:T(8,128)(2,1)S(1)} %bitcast.35), channel_id=1, source_target_pairs={{0,2},{1,15},{2,4},{3,1},{4,6},{5,3},{6,8},{7,5},{8,10},{9,7},{10,... | collective-permute-start | bytes 786440 | tf_op jit(solution)/shard_map/ppermute | solution.py:42
  148.6 6.3 %collective-permute-start.19 = (bf16[2,512,128]{2,1,0:T(8,128)(2,1)S(1)}, bf16[2,512,128]{2,1,0:T(8,128)(2,1)S(1)}, u32[]{:S(2)}, u32[]{:S(2)}) collective-permute-start(bf16[2,512,128]{2,1,0:T(8,128)(2,1)S(1)} %collective-permute-done.18), channel_id=1, source_target_pairs={{0,2},{1,15},{2,4},{3,1},{4,6},{5,3},{6,8},{7,5},{8,10},{9,7},{10,... | collective-permute-start | bytes 786440 | tf_op jit(solution)/shard_map/ppermute | solution.py:44
  154.9 3.5 %collective-permute-start.20 = (bf16[1,512,128]{2,1,0:T(8,128)(2,1)S(1)}, bf16[1,512,128]{2,1,0:T(8,128)(2,1)S(1)}, u32[]{:S(2)}, u32[]{:S(2)}) collective-permute-start(bf16[1,512,128]{2,1,0:T(8,128)(2,1)S(1)} %constant_dynamic-slice_fusion), channel_id=1, source_target_pairs={{0,4},{1,13},{2,6},{3,15},{4,8},{5,1},{6,10},{7,3},{8,12},{9,5},{1... | collective-permute-start | bytes 393224 | tf_op jit(solution)/shard_map/ppermute | solution.py:45
  158.6 4.1 %collective-permute-done.20 = bf16[1,512,128]{2,1,0:T(8,128)(2,1)S(1)} collective-permute-done((bf16[1,512,128]{2,1,0:T(8,128)(2,1)S(1)}, bf16[1,512,128]{2,1,0:T(8,128)(2,1)S(1)}, u32[]{:S(2)}, u32[]{:S(2)}) %collective-permute-start.20) | collective-permute-done | bytes 131104 | tf_op jit(solution)/shard_map/ppermute | solution.py:45
  162.6 5.8 %collective-permute-start.21 = (bf16[7,512,128]{2,1,0:T(8,128)(2,1)S(1)}, bf16[7,512,128]{2,1,0:T(8,128)(2,1)S(1)}, u32[]{:S(2)}, u32[]{:S(2)}) collective-permute-start(bf16[7,512,128]{2,1,0:T(8,128)(2,1)S(1)} %constant_dynamic-update-slice_fusion.12.received), channel_id=1, source_target_pairs={{0,1},{1,0},{2,3},{3,2},{4,5},{5,4},{6,7},{7,6},{8,9},{9,8},{10,11... | collective-permute-start | bytes 2752520 | tf_op jit(solution)/shard_map/ppermute | solution.py:47
  168.4 2.1 %collective-permute-done.21.other = bf16[7,512,128]{2,1,0:T(8,128)(2,1)S(1)} collective-permute-done((bf16[7,512,128]{2,1,0:T(8,128)(2,1)S(1)}, bf16[7,512,128]{2,1,0:T(8,128)(2,1)S(1)}, u32[]{:S(2)}, u32[]{:S(2)}) %collective-permute-start.21) | collective-permute-done | bytes 917536 | tf_op jit(solution)/shard_map/ppermute | solution.py:47
  170.5 1.4 shard_map.84
  171.9 13.4 %all_to_all.5.squares = f32[16,4,128]{2,1,0:T(4,128)S(1)} all-to-all(f32[16,4,128]{2,1,0:T(4,128)S(1)} %get-tuple-element.38), channel_id=1, replica_groups=mesh['sp'=32,'y'=8,'c'=2] {'y','c'}, dimensions={0} | all-to-all | bytes 65536 | tf_op jit(solution)/shard_map/all_to_all | solution.py:372
  185.3 1.4 shard_map.85
  (36 shorter events, 0.5 us)
Async XLA Ops:
  2.5 12.0 %collective-permute-start.1 = (bf16[2,512,128]{2,1,0:T(8,128)(2,1)S(1)}, bf16[2,512,128]{2,1,0:T(8,128)(2,1)S(1)}, u32[]{:S(2)}, u32[]{:S(2)}) collective-permute-start(bf16[2,512,128]{2,1,0:T(8,128)(2,1)S(1)} %bitcast.26), channel_id=1, source_target_pairs={{0,4},{1,13},{2,6},{3,15},{4,8},{5,1},{6,10},{7,3},{8,12},{9,5},{1... | collective-permute-start | bytes 786440 | tf_op jit(solution)/shard_map/ppermute | solution.py:41
  8.4 14.1 %collective-permute-start = (bf16[2,512,128]{2,1,0:T(8,128)(2,1)S(1)}, bf16[2,512,128]{2,1,0:T(8,128)(2,1)S(1)}, u32[]{:S(2)}, u32[]{:S(2)}) collective-permute-start(bf16[2,512,128]{2,1,0:T(8,128)(2,1)S(1)} %bitcast.27), channel_id=1, source_target_pairs={{0,2},{1,15},{2,4},{3,1},{4,6},{5,3},{6,8},{7,5},{8,10},{9,7},{10,... | collective-permute-start | bytes 786440 | tf_op jit(solution)/shard_map/ppermute | solution.py:42
  14.5 8.1 %collective-permute-start.2 = (bf16[2,512,128]{2,1,0:T(8,128)(2,1)S(1)}, bf16[2,512,128]{2,1,0:T(8,128)(2,1)S(1)}, u32[]{:S(2)}, u32[]{:S(2)}) collective-permute-start(bf16[2,512,128]{2,1,0:T(8,128)(2,1)S(1)} %collective-permute-done.1), channel_id=1, source_target_pairs={{0,2},{1,15},{2,4},{3,1},{4,6},{5,3},{6,8},{7,5},{8,10},{9,7},{10,... | collective-permute-start | bytes 786440 | tf_op jit(solution)/shard_map/ppermute | solution.py:44
  18.6 7.9 %collective-permute-start.3 = (bf16[1,512,128]{2,1,0:T(8,128)(2,1)S(1)}, bf16[1,512,128]{2,1,0:T(8,128)(2,1)S(1)}, u32[]{:S(2)}, u32[]{:S(2)}) collective-permute-start(bf16[1,512,128]{2,1,0:T(8,128)(2,1)S(1)} %constant_dynamic-slice_fusion.3), channel_id=1, source_target_pairs={{0,4},{1,13},{2,6},{3,15},{4,8},{5,1},{6,10},{7,3},{8,12},{9,5},{1... | collective-permute-start | bytes 393224 | tf_op jit(solution)/shard_map/ppermute | solution.py:45
  26.5 8.5 %collective-permute-start.4 = (bf16[7,512,128]{2,1,0:T(8,128)(2,1)S(1)}, bf16[7,512,128]{2,1,0:T(8,128)(2,1)S(1)}, u32[]{:S(2)}, u32[]{:S(2)}) collective-permute-start(bf16[7,512,128]{2,1,0:T(8,128)(2,1)S(1)} %constant_dynamic-update-slice_fusion.received.refs_1_), channel_id=1, source_target_pairs={{0,1},{1,0},{2,3},{3,2},{4,5},{5,4},{6,7},{7,6},{8,9},{9,8},{10,11... | collective-permute-start | bytes 2752520 | tf_op jit(solution)/shard_map/ppermute | solution.py:47
  35.1 6.0 %copy-start = (f32[2,2,2048]{2,1,0:T(2,128)S(1)}, f32[2,2,2048]{2,1,0:T(2,128)}, u32[]{:S(2)}) copy-start(f32[2,2,2048]{2,1,0:T(2,128)} %gain.11) | copy-start | bytes 98308
  35.1 6.0 %copy-start.1 = (s32[16]{0:T(128)S(1)}, s32[16]{0:T(128)}, u32[]{:S(2)}) copy-start(s32[16]{0:T(128)} %stack.67.ids) | copy-start | bytes 196
  35.1 6.0 %copy-start.4 = (bf16[2,2048,128]{2,1,0:T(8,128)(2,1)S(1)}, bf16[2,2048,128]{2,1,0:T(8,128)(2,1)}, u32[]{:S(2)}) copy-start(bf16[2,2048,128]{2,1,0:T(8,128)(2,1)} %refs_0_.7) | copy-start | bytes 3145732
  35.1 1.3 copy-start.6
  37.9 4.1 %copy-start.5 = (f32[2,2,257]{2,1,0:T(2,128)S(1)}, f32[2,2,257]{2,1,0:T(2,128)}, u32[]{:S(2)}) copy-start(f32[2,2,257]{2,1,0:T(2,128)} %bias.3) | copy-start | bytes 12340
  38.0 13.1 %collective-permute-start.5 = (bf16[512,256]{1,0:T(8,128)(2,1)S(1)}, bf16[512,256]{1,0:T(8,128)(2,1)S(1)}, u32[]{:S(2)}, u32[]{:S(2)}) collective-permute-start(bf16[512,256]{1,0:T(8,128)(2,1)S(1)} %get-tuple-element.24.refs_5_), channel_id=1, source_target_pairs={{0,16},{16,32},{32,48},{48,64},{64,80},{80,96},{96,112},{112,128},... | collective-permute-start | bytes 786440 | tf_op jit(solution)/shard_map/ppermute | solution.py:338
  53.3 31.4 %copy-start.7 = (bf16[2,2048,128]{2,1,0:T(8,128)(2,1)S(1)}, bf16[2,2048,128]{2,1,0:T(8,128)(2,1)}, u32[]{:S(2)}) copy-start(bf16[2,2048,128]{2,1,0:T(8,128)(2,1)} %param.12) | copy-start | bytes 3145732
  56.0 8.9 %collective-permute-start.7 = (bf16[2,512,128]{2,1,0:T(8,128)(2,1)S(1)}, bf16[2,512,128]{2,1,0:T(8,128)(2,1)S(1)}, u32[]{:S(2)}, u32[]{:S(2)}) collective-permute-start(bf16[2,512,128]{2,1,0:T(8,128)(2,1)S(1)} %bitcast.37), channel_id=1, source_target_pairs={{0,4},{1,13},{2,6},{3,15},{4,8},{5,1},{6,10},{7,3},{8,12},{9,5},{1... | collective-permute-start | bytes 786440 | tf_op jit(solution)/shard_map/ppermute | solution.py:41
  58.6 15.9 %collective-permute-start.6 = (bf16[2,512,128]{2,1,0:T(8,128)(2,1)S(1)}, bf16[2,512,128]{2,1,0:T(8,128)(2,1)S(1)}, u32[]{:S(2)}, u32[]{:S(2)}) collective-permute-start(bf16[2,512,128]{2,1,0:T(8,128)(2,1)S(1)} %bitcast.38), channel_id=1, source_target_pairs={{0,2},{1,15},{2,4},{3,1},{4,6},{5,3},{6,8},{7,5},{8,10},{9,7},{10,... | collective-permute-start | bytes 786440 | tf_op jit(solution)/shard_map/ppermute | solution.py:42
  64.9 9.7 %collective-permute-start.8 = (bf16[2,512,128]{2,1,0:T(8,128)(2,1)S(1)}, bf16[2,512,128]{2,1,0:T(8,128)(2,1)S(1)}, u32[]{:S(2)}, u32[]{:S(2)}) collective-permute-start(bf16[2,512,128]{2,1,0:T(8,128)(2,1)S(1)} %collective-permute-done.7), channel_id=1, source_target_pairs={{0,2},{1,15},{2,4},{3,1},{4,6},{5,3},{6,8},{7,5},{8,10},{9,7},{10,... | collective-permute-start | bytes 786440 | tf_op jit(solution)/shard_map/ppermute | solution.py:44
  70.9 8.0 %collective-permute-start.9 = (bf16[1,512,128]{2,1,0:T(8,128)(2,1)S(1)}, bf16[1,512,128]{2,1,0:T(8,128)(2,1)S(1)}, u32[]{:S(2)}, u32[]{:S(2)}) collective-permute-start(bf16[1,512,128]{2,1,0:T(8,128)(2,1)S(1)} %constant_dynamic-slice_fusion.2), channel_id=1, source_target_pairs={{0,4},{1,13},{2,6},{3,15},{4,8},{5,1},{6,10},{7,3},{8,12},{9,5},{1... | collective-permute-start | bytes 393224 | tf_op jit(solution)/shard_map/ppermute | solution.py:45
  78.9 7.9 %collective-permute-start.10 = (bf16[7,512,128]{2,1,0:T(8,128)(2,1)S(1)}, bf16[7,512,128]{2,1,0:T(8,128)(2,1)S(1)}, u32[]{:S(2)}, u32[]{:S(2)}) collective-permute-start(bf16[7,512,128]{2,1,0:T(8,128)(2,1)S(1)} %constant_dynamic-update-slice_fusion.4.received), channel_id=1, source_target_pairs={{0,1},{1,0},{2,3},{3,2},{4,5},{5,4},{6,7},{7,6},{8,9},{9,8},{10,11... | collective-permute-start | bytes 2752520 | tf_op jit(solution)/shard_map/ppermute | solution.py:47
  88.1 28.0 %copy-start.2 = (bf16[2,2048,128]{2,1,0:T(8,128)(2,1)S(1)}, bf16[2,2048,128]{2,1,0:T(8,128)(2,1)}, u32[]{:S(2)}) copy-start(bf16[2,2048,128]{2,1,0:T(8,128)(2,1)} %refs_0_.6) | copy-start | bytes 3145732
  88.1 28.0 %copy-start.3 = (bf16[2,2048,128]{2,1,0:T(8,128)(2,1)S(1)}, bf16[2,2048,128]{2,1,0:T(8,128)(2,1)}, u32[]{:S(2)}) copy-start(bf16[2,2048,128]{2,1,0:T(8,128)(2,1)} %refs_1_.3) | copy-start | bytes 3145732
  90.3 10.1 %collective-permute-start.12 = (bf16[2,512,128]{2,1,0:T(8,128)(2,1)S(1)}, bf16[2,512,128]{2,1,0:T(8,128)(2,1)S(1)}, u32[]{:S(2)}, u32[]{:S(2)}) collective-permute-start(bf16[2,512,128]{2,1,0:T(8,128)(2,1)S(1)} %bitcast.31), channel_id=1, source_target_pairs={{0,4},{1,13},{2,6},{3,15},{4,8},{5,1},{6,10},{7,3},{8,12},{9,5},{1... | collective-permute-start | bytes 786440 | tf_op jit(solution)/shard_map/ppermute | solution.py:41
  94.1 13.2 %collective-permute-start.11 = (bf16[2,512,128]{2,1,0:T(8,128)(2,1)S(1)}, bf16[2,512,128]{2,1,0:T(8,128)(2,1)S(1)}, u32[]{:S(2)}, u32[]{:S(2)}) collective-permute-start(bf16[2,512,128]{2,1,0:T(8,128)(2,1)S(1)} %bitcast.32), channel_id=1, source_target_pairs={{0,2},{1,15},{2,4},{3,1},{4,6},{5,3},{6,8},{7,5},{8,10},{9,7},{10,... | collective-permute-start | bytes 786440 | tf_op jit(solution)/shard_map/ppermute | solution.py:42
  100.3 8.1 %collective-permute-start.13 = (bf16[2,512,128]{2,1,0:T(8,128)(2,1)S(1)}, bf16[2,512,128]{2,1,0:T(8,128)(2,1)S(1)}, u32[]{:S(2)}, u32[]{:S(2)}) collective-permute-start(bf16[2,512,128]{2,1,0:T(8,128)(2,1)S(1)} %collective-permute-done.12), channel_id=1, source_target_pairs={{0,2},{1,15},{2,4},{3,1},{4,6},{5,3},{6,8},{7,5},{8,10},{9,7},{10,... | collective-permute-start | bytes 786440 | tf_op jit(solution)/shard_map/ppermute | solution.py:44
  105.1 7.9 %collective-permute-start.14 = (bf16[1,512,128]{2,1,0:T(8,128)(2,1)S(1)}, bf16[1,512,128]{2,1,0:T(8,128)(2,1)S(1)}, u32[]{:S(2)}, u32[]{:S(2)}) collective-permute-start(bf16[1,512,128]{2,1,0:T(8,128)(2,1)S(1)} %constant_dynamic-slice_fusion.1), channel_id=1, source_target_pairs={{0,4},{1,13},{2,6},{3,15},{4,8},{5,1},{6,10},{7,3},{8,12},{9,5},{1... | collective-permute-start | bytes 393224 | tf_op jit(solution)/shard_map/ppermute | solution.py:45
  113.0 5.2 %collective-permute-start.15 = (bf16[7,512,128]{2,1,0:T(8,128)(2,1)S(1)}, bf16[7,512,128]{2,1,0:T(8,128)(2,1)S(1)}, u32[]{:S(2)}, u32[]{:S(2)}) collective-permute-start(bf16[7,512,128]{2,1,0:T(8,128)(2,1)S(1)} %constant_dynamic-update-slice_fusion.8.b_received), channel_id=1, source_target_pairs={{0,1},{1,0},{2,3},{3,2},{4,5},{5,4},{6,7},{7,6},{8,9},{9,8},{10,11... | collective-permute-start | bytes 2752520 | tf_op jit(solution)/shard_map/ppermute | solution.py:47
  121.8 12.7 %collective-permute-start.16 = (bf16[512,256]{1,0:T(8,128)(2,1)S(1)}, bf16[512,256]{1,0:T(8,128)(2,1)S(1)}, u32[]{:S(2)}, u32[]{:S(2)}) collective-permute-start(bf16[512,256]{1,0:T(8,128)(2,1)S(1)} %get-tuple-element.32.refs_3_), channel_id=1, source_target_pairs={{0,16},{16,32},{32,48},{48,64},{64,80},{80,96},{96,112},{112,128},... | collective-permute-start | bytes 786440 | tf_op jit(solution)/shard_map/ppermute | solution.py:338
  139.7 8.9 %collective-permute-start.18 = (bf16[2,512,128]{2,1,0:T(8,128)(2,1)S(1)}, bf16[2,512,128]{2,1,0:T(8,128)(2,1)S(1)}, u32[]{:S(2)}, u32[]{:S(2)}) collective-permute-start(bf16[2,512,128]{2,1,0:T(8,128)(2,1)S(1)} %bitcast.34), channel_id=1, source_target_pairs={{0,4},{1,13},{2,6},{3,15},{4,8},{5,1},{6,10},{7,3},{8,12},{9,5},{1... | collective-permute-start | bytes 786440 | tf_op jit(solution)/shard_map/ppermute | solution.py:41
  142.9 15.5 %collective-permute-start.17 = (bf16[2,512,128]{2,1,0:T(8,128)(2,1)S(1)}, bf16[2,512,128]{2,1,0:T(8,128)(2,1)S(1)}, u32[]{:S(2)}, u32[]{:S(2)}) collective-permute-start(bf16[2,512,128]{2,1,0:T(8,128)(2,1)S(1)} %bitcast.35), channel_id=1, source_target_pairs={{0,2},{1,15},{2,4},{3,1},{4,6},{5,3},{6,8},{7,5},{8,10},{9,7},{10,... | collective-permute-start | bytes 786440 | tf_op jit(solution)/shard_map/ppermute | solution.py:42
  148.6 9.9 %collective-permute-start.19 = (bf16[2,512,128]{2,1,0:T(8,128)(2,1)S(1)}, bf16[2,512,128]{2,1,0:T(8,128)(2,1)S(1)}, u32[]{:S(2)}, u32[]{:S(2)}) collective-permute-start(bf16[2,512,128]{2,1,0:T(8,128)(2,1)S(1)} %collective-permute-done.18), channel_id=1, source_target_pairs={{0,2},{1,15},{2,4},{3,1},{4,6},{5,3},{6,8},{7,5},{8,10},{9,7},{10,... | collective-permute-start | bytes 786440 | tf_op jit(solution)/shard_map/ppermute | solution.py:44
  154.9 7.7 %collective-permute-start.20 = (bf16[1,512,128]{2,1,0:T(8,128)(2,1)S(1)}, bf16[1,512,128]{2,1,0:T(8,128)(2,1)S(1)}, u32[]{:S(2)}, u32[]{:S(2)}) collective-permute-start(bf16[1,512,128]{2,1,0:T(8,128)(2,1)S(1)} %constant_dynamic-slice_fusion), channel_id=1, source_target_pairs={{0,4},{1,13},{2,6},{3,15},{4,8},{5,1},{6,10},{7,3},{8,12},{9,5},{1... | collective-permute-start | bytes 393224 | tf_op jit(solution)/shard_map/ppermute | solution.py:45
  162.6 7.9 %collective-permute-start.21 = (bf16[7,512,128]{2,1,0:T(8,128)(2,1)S(1)}, bf16[7,512,128]{2,1,0:T(8,128)(2,1)S(1)}, u32[]{:S(2)}, u32[]{:S(2)}) collective-permute-start(bf16[7,512,128]{2,1,0:T(8,128)(2,1)S(1)} %constant_dynamic-update-slice_fusion.12.received), channel_id=1, source_target_pairs={{0,1},{1,0},{2,3},{3,2},{4,5},{5,4},{6,7},{7,6},{8,9},{9,8},{10,11... | collective-permute-start | bytes 2752520 | tf_op jit(solution)/shard_map/ppermute | solution.py:47

commit v3 on v2

v3 whole, which is shorter than its diff:
```python
import functools

import jax
import jax.numpy as jnp
from jax import lax
from jax.experimental import pallas as pl
from jax.experimental.pallas import tpu as pltpu
from jax.sharding import Mesh
from jax.sharding import PartitionSpec as P


D = 2048
HEAD = 64
BLK = 128
NB = 16
EPS = 1e-06
BIG = 60
CUTS = 4
NEG = -1e30
VMEM = pl.BlockSpec(memory_space=pltpu.VMEM)
SMEM = pl.BlockSpec(memory_space=pltpu.SMEM)
HBM = pl.BlockSpec(memory_space=pltpu.HBM)


def params(mib):
    return pltpu.CompilerParams(vmem_limit_bytes=mib * 1024 * 1024)


def core_pairs(step):
    pairs = []
    for y in range(8):
        for c in range(2):
            target = (y + (step if c == 0 else -step)) % 8
            pairs.append((2 * y + c, 2 * target + c))
    return pairs


def gather_blocks(x):
    core = lax.axis_index("c")

    own = lax.all_gather(x, "c", axis=0)
    two = lax.ppermute(own, ("y", "c"), core_pairs(2))
    one = lax.ppermute(own, ("y", "c"), core_pairs(1))
    half = lax.dynamic_index_in_dim(two, core, 0, keepdims=True)
    three = lax.ppermute(two, ("y", "c"), core_pairs(1))
    four = lax.ppermute(half, ("y", "c"), core_pairs(2))
    received = jnp.concatenate([one, two, three, four], axis=0)
    other = lax.ppermute(received, "c", [(0, 1), (1, 0)])
    return own, received, other


def block_ids(place):
    y, c = place[0] // 2, place[0] % 2
    sign = 1 - 2 * c
    across = 2 * ((y + 4) % 8)
    ids = [2 * y, 2 * y + 1]
    for way, last in ((-sign, c), (sign, 1 - c)):
        for d in (1, 2, 3):
            chip = (y + way * d + 8) % 8
            ids += [2 * chip, 2 * chip + 1]
        ids.append(across + last)
    return ids


def part(refs, k):
    own, received, other = refs
    if k < 2:
        return own, k
    if k < 9:
        return received, k - 2
    return other, k - 9


def scale_kernel(layer, count, place, gain, *refs):
    weights, (out, *held, sems) = refs[:count], refs[count:]
    ids = block_ids(place)
    copies = []
    for n, (w, dst) in enumerate(zip(weights, held)):
        for m in range(CUTS):
            rows = pl.ds(m * (D // CUTS), D // CUTS)
            copies.append(
                pltpu.make_async_copy(w.at[layer, rows, :], dst.at[rows, :], sems.at[n, m])
            )
    for copy in copies:
        copy.start()
    for copy in copies:
        copy.wait()
    for k in range(NB):
        t = ids[k]
        rows = pl.ds(pl.multiple_of(t * BLK, BLK), BLK)
        factor = jnp.broadcast_to(gain_row(gain, layer, 0, t), (BLK, BLK)).T
        for n, w in enumerate(held):
            scaled = w[rows, :].astype(jnp.float32) * factor
            out[k, :, n * BLK : (n + 1) * BLK] = scaled.astype(jnp.bfloat16)


def gain_row(gain, layer, kind, t):
    return gain[layer, kind : kind + 1, pl.ds(pl.multiple_of(t * BLK, BLK), BLK)]


def product(blocks, weights):
    left = jnp.concatenate(blocks, axis=1)
    right = jnp.concatenate(
        [jnp.concatenate([w[k] for w in weights], axis=1) for k in range(len(blocks))], axis=0
    )
    return jnp.dot(left, right, preferred_element_type=jnp.float32)


def blocks_of(refs):
    return [ref[k] for ref in refs for k in range(ref.shape[0])]


def row_squares(refs, rows):
    total = jnp.zeros((rows.size, BLK), jnp.float32)
    for ref in refs:
        for k in range(ref.shape[0]):
            x = ref[k, rows, :].astype(jnp.float32)
            total += x * x
    return total


def tiled(count, body):
    def tile(i, carry):
        body(pl.ds(pl.multiple_of(i * 64, 64), 64))
        return carry

    lax.fori_loop(0, count // 64, tile, 0)


def wide_inverse(total):
    inv = lax.rsqrt(jnp.sum(total, axis=1, keepdims=True) / D + EPS)
    return jnp.broadcast_to(inv, total.shape)


def first_part_kernel(own, received, w, total_out, kv_out):
    refs = (own, received)

    def body(rows):
        total_out[rows, :] = row_squares(refs, rows)

    tiled(own.shape[1], body)
    kv_out[...] = product(blocks_of(refs), (w.at[:9],))


def first_kernel(other, w, total, kv_part, kv_out, inv_out):
    def body(rows):
        inv_out[rows, :] = wide_inverse(total[rows, :] + row_squares((other,), rows))

    tiled(other.shape[1], body)
    inv = inv_out[...]
    kv = kv_part[...] + product(blocks_of((other,)), (w.at[9:],))
    kv_out[...] = (kv * jnp.concatenate([inv, inv], axis=1)).astype(jnp.bfloat16)


def squares_kernel(own, received, total_out):
    def body(rows):
        total_out[rows, :] = row_squares((own, received), rows)

    tiled(own.shape[1], body)


def next_kernel(
    place, own, received, other, b_own, b_received, b_other, b_total, gain, w,
    kv_out, inv_out, stream, carried,
):
    ids = block_ids(place)
    mine = place[0] % 2
    refs = (own, received, other)
    b_refs = (b_own, b_received, b_other)

    def body(rows):
        def load(group, k):
            ref, j = part(group, k)
            return ref[j, rows, :].astype(jnp.float32)

        inv_post = wide_inverse(b_total[rows, :] + row_squares((b_other,), rows))
        total = jnp.zeros((64, BLK), jnp.float32)
        for k in range(NB):
            x = load(refs, k) + load(b_refs, k) * inv_post * gain_row(gain, 0, 1, ids[k])
            x = x.astype(jnp.bfloat16)
            stream[k, rows, :] = x
            x = x.astype(jnp.float32)
            total += x * x
        inv_out[rows, :] = wide_inverse(total)
        carried[rows, :] = stream[mine, rows, :]

    tiled(own.shape[1], body)
    inv = inv_out[...]
    kv = product(blocks_of((stream,)), (w,))
    kv_out[...] = (kv * jnp.concatenate([inv, inv], axis=1)).astype(jnp.bfloat16)


def grids():
    lane = lax.broadcasted_iota(jnp.int32, (BLK, BLK), 1)
    row = lax.broadcasted_iota(jnp.int32, (BLK, BLK), 0)
    return lane, row


def split_bias(bias, layer, h):
    low = bias[layer, h : h + 1, 0:BLK]
    high = bias[layer, h : h + 1, BLK : 2 * BLK]
    last = bias[layer, h : h + 1, 2 * BLK : 2 * BLK + 1]
    return low, high, last


def skewed(left, right):
    full = jnp.broadcast_to(jnp.concatenate([left, right], axis=1), (BLK, 2 * BLK))
    return pltpu.roll(full, 0, 1, stride=1, stride_axis=0)[:, :BLK].T


def padded_values(kv):
    values = kv[:, BLK:]
    lane = lax.broadcasted_iota(jnp.int32, values.shape, 1)
    one = jnp.ones_like(values)
    return jnp.where(lane < HEAD, values, one), jnp.where(lane < HEAD, one, values)


def head_scores(qh, keys):
    dims = (((1,), (1,)), ((), ()))
    return lax.dot_general(qh, keys, dims, preferred_element_type=jnp.float32)


def local_kernel(layer, x_count, *refs):
    xs, rest = refs[:x_count], refs[x_count:]
    w, inv, kv, bias, q_out, acc_out, top_out, sum_out, near_out = rest
    q = product(blocks_of(xs), (w,))
    q_out[...] = (q * inv[...] * HEAD ** (-0.5)).astype(jnp.bfloat16)
    lane, row = grids()
    values = padded_values(kv)
    tables = []
    for h in range(2):
        low, high, last = split_bias(bias, layer, h)
        last_row = jnp.broadcast_to(last, (1, BLK))
        diag = jnp.where((lane >= 64) & (row < 64), NEG, skewed(high, low))
        near_out[h] = skewed(last_row, high)
        tables.append((diag, near_out[h], jnp.broadcast_to(last, (BLK, BLK))))
    for i in range(4):
        rows = slice(i * BLK, (i + 1) * BLK)
        found = []
        for h in range(2):
            qh = q_out[rows, :]
            qh = jnp.where((lane < HEAD) == (h == 0), qh, jnp.zeros_like(qh))
            raw = head_scores(qh, kv[: (i + 1) * BLK, :BLK])
            scores = [
                raw[:, j * BLK : (j + 1) * BLK] + tables[h][min(i - j, 2)] for j in range(i + 1)
            ]
            top = jnp.max(functools.reduce(jnp.maximum, scores), axis=1, keepdims=True)
            weights = [jnp.exp(s - top).astype(jnp.bfloat16) for s in scores]
            probs = jnp.concatenate(weights, axis=1)
            acc = jnp.dot(probs, values[h][: (i + 1) * BLK], preferred_element_type=jnp.float32)
            found.append((acc, top))
        for n, out in enumerate((acc_out, top_out)):
            out[rows, :] = jnp.where(lane < HEAD, found[0][n], found[1][n])
        sum_out[rows, :] = jnp.where(lane < HEAD, found[1][0], found[0][0])


def merge_kernel(layer, first, q, kv, acc, top, total, nears, bias, out):
    lane, row = grids()
    values = padded_values(kv)
    hidden = jnp.where(first[0] == 1, NEG, 0.0)
    tables = []
    for h in range(2):
        last = split_bias(bias, layer, h)[2]
        full = jnp.broadcast_to(last, (BLK, BLK)) + hidden
        edge = jnp.where((lane < 64) & (row >= 64), NEG, full)
        tables.append((nears[h] + hidden, full, edge))
    where = [(i, h) for i in range(4) for h in range(2)]
    raw, peaks, olds, found = {}, {}, {}, {}
    for i, h in where:
        qh = q[i * BLK : (i + 1) * BLK, :]
        qh = jnp.where((lane < HEAD) == (h == 0), qh, jnp.zeros_like(qh))
        raw[i, h] = head_scores(qh, kv[i * BLK :, :BLK])
    for i, h in where:
        near, full, edge = tables[h]
        scores = []
        for j in range(4 - i):
            term = edge if j == 0 else near if j == 3 else full
            scores.append(raw[i, h][:, j * BLK : (j + 1) * BLK] + term)
        raw[i, h] = scores
        olds[i, h] = top[i * BLK : (i + 1) * BLK, h * HEAD : h * HEAD + 1]
        peak = jnp.max(functools.reduce(jnp.maximum, scores), axis=1, keepdims=True)
        peaks[i, h] = jnp.maximum(peak, olds[i, h])
    for i, h in where:
        weights = [jnp.exp(s - peaks[i, h]).astype(jnp.bfloat16) for s in raw[i, h]]
        probs = jnp.concatenate(weights, axis=1)
        found[i, h] = jnp.dot(probs, values[h][i * BLK :], preferred_element_type=jnp.float32)
    for i in range(4):
        rows = slice(i * BLK, (i + 1) * BLK)
        fades = [jnp.exp(olds[i, h] - peaks[i, h]) for h in range(2)]
        more, fade = (jnp.where(lane < HEAD, x, z) for x, z in ((found[i, 0], found[i, 1]), fades))
        sums = jnp.where(lane < HEAD, found[i, 1], found[i, 0])
        sums_fade = jnp.where(lane < HEAD, fades[1], fades[0])
        norm = pltpu.roll(total[rows, :] * sums_fade + sums, HEAD, 1)
        out[rows, :] = ((acc[rows, :] * fade + more) / norm).astype(jnp.bfloat16)


def rows_product(ids, offset, refs, w):
    rows = [
        w[pl.ds(pl.multiple_of(ids[offset + k] * BLK, BLK), BLK), :]
        for k in range(sum(ref.shape[0] for ref in refs))
    ]
    left = jnp.concatenate(blocks_of(refs), axis=1)
    return jnp.dot(left, jnp.concatenate(rows, axis=0), preferred_element_type=jnp.float32)


def out_part_kernel(place, own, received, w, acc):
    acc[...] = rows_product(block_ids(place), 0, (own, received), w)


def out_kernel(place, other, w, acc, out):
    out[...] = (acc[...] + rows_product(block_ids(place), 9, (other,), w)).astype(jnp.bfloat16)


def last_kernel(place, own, received, other, w, out, squares):
    out[...] = rows_product(block_ids(place), 0, (own, received, other), w)
    for i in range(4):
        x = out[i * BLK : (i + 1) * BLK, :]
        sums = jnp.sum((x * x).T, axis=0, keepdims=True)
        for n in range(NB):
            squares[n, i : i + 1, :] = sums


def finish_kernel(squares, branch, stream, gain, out):
    total = jnp.sum(squares[...], axis=0)
    inv = lax.rsqrt(total / D + EPS)
    for i in range(4):
        rows = slice(i * BLK, (i + 1) * BLK)
        scale = jnp.broadcast_to(inv[i : i + 1, :], (BLK, BLK)).T
        x = stream[rows, :].astype(jnp.float32)
        out[rows, :] = (x + branch[rows, :] * scale * gain[...]).astype(jnp.bfloat16)


def call(kernel, ins, outs, scratch, mib, flops, args):
    size = sum(a.size * a.dtype.itemsize for a in args)
    return pl.pallas_call(
        kernel,
        out_shape=outs,
        in_specs=ins,
        out_specs=jax.tree.map(lambda _: VMEM, outs),
        scratch_shapes=scratch,
        compiler_params=params(mib),
        cost_estimate=pl.CostEstimate(flops=flops, bytes_accessed=size, transcendentals=0),
    )(*args)


def on_device(residual, gains, w_query, w_key, w_value, w_out, rel_bias):
    tokens = residual.shape[0]
    half = jnp.bfloat16
    place = lax.axis_index(("y", "c")).reshape(1).astype(jnp.int32)
    first = (lax.axis_index("sp") == 0).reshape(1).astype(jnp.int32)
    block = jax.ShapeDtypeStruct((tokens, BLK), half)
    pair = jax.ShapeDtypeStruct((tokens, 2 * BLK), half)
    wide = jax.ShapeDtypeStruct((tokens, BLK), jnp.float32)
    stack = jax.ShapeDtypeStruct((NB, tokens, BLK), half)
    tiles = jax.ShapeDtypeStruct((2, BLK, BLK), jnp.float32)
    flow = lax.axis_size("sp")
    shift = [(i, i + 1) for i in range(flow - 1)]

    def scaled(layer, weights, mib):
        count = len(weights)
        shape = jax.ShapeDtypeStruct((NB, BLK, count * BLK), half)
        scratch = [pltpu.VMEM((D, BLK), half)] * count + [pltpu.SemaphoreType.DMA((count, CUTS))]
        return call(
            functools.partial(scale_kernel, layer, count), [SMEM, VMEM] + [HBM] * count,
            shape, scratch, mib, 10**9, (place, gains, *weights),
        )

    def attention(layer, xs, wq, kv, inv):
        previous = lax.ppermute(kv, "sp", shift)
        local = call(
            functools.partial(local_kernel, layer, len(xs)), [VMEM] * (len(xs) + 4),
            (block, wide, wide, wide, tiles), [], 4, 2 * 10**9, (*xs, wq, inv, kv, rel_bias),
        )
        return call(
            functools.partial(merge_kernel, layer), [SMEM] + [VMEM] * 7, block, [], 4,
            10**9, (first, local[0], previous, *local[1:], rel_bias),
        )

    def projected(attended, w):
        own, received, other = attended
        acc = call(
            out_part_kernel, [SMEM] + [VMEM] * 3, wide, [], 4, 10**9, (place, own, received, w)
        )
        return other, w, acc

    wkv = scaled(0, (w_key, w_value), BIG)
    wq = scaled(0, (w_query,), 4)
    stream = gather_blocks(residual)
    parts = call(
        first_part_kernel, [VMEM] * 3,
        (wide, jax.ShapeDtypeStruct((tokens, 2 * BLK), jnp.float32)), [], 4, 10**9,
        (*stream[:2], wkv),
    )
    kv, inv = call(
        first_kernel, [VMEM] * 4, (pair, wide), [], 4, 10**9, (stream[2], wkv, *parts),
    )
    attended = gather_blocks(attention(0, stream, wq, kv, inv))
    branch = call(
        out_kernel, [SMEM] + [VMEM] * 3, block, [], 4, 10**9,
        (place, *projected(attended, w_out[0])),
    )
    branch = gather_blocks(branch)
    total = call(squares_kernel, [VMEM] * 2, wide, [], 4, 10**9, branch[:2])
    wkv = scaled(1, (w_key, w_value), 4)
    wq = scaled(1, (w_query,), 4)
    kv, inv, full, carried = call(
        next_kernel, [SMEM] + [VMEM] * 9, (pair, wide, stack, block), [], 4, 2 * 10**9,
        (place, *stream, *branch, total, gains, wkv),
    )
    attended = gather_blocks(attention(1, (full,), wq, kv, inv))
    branch, squares = call(
        last_kernel, [SMEM] + [VMEM] * 4,
        (wide, jax.ShapeDtypeStruct((NB, tokens // BLK, BLK), jnp.float32)), [], 4, 10**9,
        (place, *attended, w_out[1]),
    )
    own_gain = lax.dynamic_slice_in_dim(
        gains[1, 1].reshape(1, D), lax.axis_index(("y", "c")) * BLK, BLK, 1
    )
    everything = lax.all_to_all(squares, ("y", "c"), split_axis=0, concat_axis=0, tiled=True)
    return call(
        finish_kernel, [VMEM] * 4, block, [], 4, 10**7, (everything, branch, carried, own_gain)
    )


def solution(mesh):
    finer = Mesh(mesh.devices.reshape(mesh.shape["sp"], 8, 2), ("sp", "y", "c"))
    tp = ("y", "c")
    in_specs = (
        P("sp", tp),
        P(),
        P(None, None, tp),
        P(None, None, tp),
        P(None, None, tp),
        P(None, None, tp),
        P(None, tp, None),
    )

    return jax.shard_map(
        on_device, mesh=finer, in_specs=in_specs, out_specs=P("sp", tp), check_vma=False
    )
```

time: 188 us -> 184 us (0.979)
  blocking collectives: 23.5 us -> 10.1 us
  starting transfers between devices: 91.2 us -> 97.4 us
  waiting for transfers between devices: 42.1 us -> 47.8 us
    all_to_all x1 -> x0, blocking collectives: 13.4 us -> none  [on_device(): lax.all_to_all(squares, ('y', 'c'), split_axis=0, concat_axis=0, tiled=True)]
    all_to_all x0 -> x1, waiting for transfers between devices: none -> 7.39 us  [on_device(): lax.all_to_all(squares, ('y', 'c'), split_axis=0, concat_axis=0, tiled=True)]
    all_to_all x0 -> x1, starting transfers between devices: none -> 6.23 us  [on_device(): lax.all_to_all(squares, ('y', 'c'), split_axis=0, concat_axis=0, tiled=True)]
    pallas_call x13 -> x16, Pallas kernels: 26.5 us -> 25.3 us  [call(): pl.pallas_call(kernel, out_shape=outs, in_specs=ins, out_specs=jax.tree.m...]
  transfers between devices with their start and end apart: 22 -> 23, of which waited for: 12 -> 13; matrix products, arithmetic and copies ran while one was open for 1% -> 0% of each run, Pallas kernels for 7% -> 8%
where the time goes in v3:
time: 184 us; the launch traced here: 183 us
  starting transfers between devices  97.4 us (53%)
  waiting for transfers between devices  47.8 us (26%)
  Pallas kernels  25.3 us (14%)
  blocking collectives  10.1 us (5%)
  local copies, waits for them, and re-layouts  1.85 us (1%)
    pallas_call x16, Pallas kernels, call(): pl.pallas_call(kernel, out_shape=outs, in_specs=ins, out_specs=jax.tree.m...  25.3 us
    ppermute x4, starting transfers between devices, gather_blocks(): three = lax.ppermute(two, ('y', 'c'), core_pairs(1))  21 us
    ppermute x4, starting transfers between devices, gather_blocks(): other = lax.ppermute(received, 'c', [(0, 1), (1, 0)])  19.2 us
    ppermute x4, starting transfers between devices, gather_blocks(): one = lax.ppermute(own, ('y', 'c'), core_pairs(1))  17 us
    ppermute x4, waiting for transfers between devices, gather_blocks(): four = lax.ppermute(half, ('y', 'c'), core_pairs(2))  16.9 us
    ppermute x4, starting transfers between devices, gather_blocks(): two = lax.ppermute(own, ('y', 'c'), core_pairs(2))  15.6 us
    ppermute x4, starting transfers between devices, gather_blocks(): four = lax.ppermute(half, ('y', 'c'), core_pairs(2))  13.2 us
    ppermute x2, waiting for transfers between devices, attention(): previous = lax.ppermute(kv, 'sp', shift)  11.6 us
  transfers between devices with their start and end apart: 23, of which 13 were waited for; matrix products, arithmetic and copies ran while one was open for 0% of the time, Pallas kernels for 8%

profile of v3, /device:TPU:257, one launch (start us, length us, event | category | flops | bytes accessed | tf_op | source)
XLA Modules:
  0.0 183.1 jit_solution(9198948223376781070)
XLA Ops:
  0.0 2.5 %all-gather = bf16[1024,128]{1,0:T(8,128)(2,1)S(1)} all-gather(bf16[512,128]{1,0:T(8,128)(2,1)} %param.7), channel_id=2, replica_groups=mesh['sp'=32,'y'=8,'c'=2] {'c'}, dimensions={0}, use_global_device_ids=true | all-gather | bytes 393216 | tf_op jit(solution)/shard_map/all_gather | solution.py:41
  2.5 5.9 %collective-permute-start.1 = (bf16[2,512,128]{2,1,0:T(8,128)(2,1)S(1)}, bf16[2,512,128]{2,1,0:T(8,128)(2,1)S(1)}, u32[]{:S(2)}, u32[]{:S(2)}) collective-permute-start(bf16[2,512,128]{2,1,0:T(8,128)(2,1)S(1)} %bitcast.12), channel_id=1, source_target_pairs={{0,4},{1,13},{2,6},{3,15},{4,8},{5,1},{6,10},{7,3},{8,12},{9,5},{1... | collective-permute-start | bytes 786440 | tf_op jit(solution)/shard_map/ppermute | solution.py:42
  8.4 3.0 %collective-permute-start = (bf16[2,512,128]{2,1,0:T(8,128)(2,1)S(1)}, bf16[2,512,128]{2,1,0:T(8,128)(2,1)S(1)}, u32[]{:S(2)}, u32[]{:S(2)}) collective-permute-start(bf16[2,512,128]{2,1,0:T(8,128)(2,1)S(1)} %bitcast.13), channel_id=1, source_target_pairs={{0,2},{1,15},{2,4},{3,1},{4,6},{5,3},{6,8},{7,5},{8,10},{9,7},{10,... | collective-permute-start | bytes 786440 | tf_op jit(solution)/shard_map/ppermute | solution.py:43
  11.4 3.1 %collective-permute-done.1 = bf16[2,512,128]{2,1,0:T(8,128)(2,1)S(1)} collective-permute-done((bf16[2,512,128]{2,1,0:T(8,128)(2,1)S(1)}, bf16[2,512,128]{2,1,0:T(8,128)(2,1)S(1)}, u32[]{:S(2)}, u32[]{:S(2)}) %collective-permute-start.1) | collective-permute-done | bytes 262176 | tf_op jit(solution)/shard_map/ppermute | solution.py:42
  14.5 4.1 %collective-permute-start.2 = (bf16[2,512,128]{2,1,0:T(8,128)(2,1)S(1)}, bf16[2,512,128]{2,1,0:T(8,128)(2,1)S(1)}, u32[]{:S(2)}, u32[]{:S(2)}) collective-permute-start(bf16[2,512,128]{2,1,0:T(8,128)(2,1)S(1)} %collective-permute-done.1), channel_id=1, source_target_pairs={{0,2},{1,15},{2,4},{3,1},{4,6},{5,3},{6,8},{7,5},{8,10},{9,7},{10,... | collective-permute-start | bytes 786440 | tf_op jit(solution)/shard_map/ppermute | solution.py:45
  18.6 3.9 %collective-permute-start.3 = (bf16[1,512,128]{2,1,0:T(8,128)(2,1)S(1)}, bf16[1,512,128]{2,1,0:T(8,128)(2,1)S(1)}, u32[]{:S(2)}, u32[]{:S(2)}) collective-permute-start(bf16[1,512,128]{2,1,0:T(8,128)(2,1)S(1)} %constant_dynamic-slice_fusion.4), channel_id=1, source_target_pairs={{0,4},{1,13},{2,6},{3,15},{4,8},{5,1},{6,10},{7,3},{8,12},{9,5},{1... | collective-permute-start | bytes 393224 | tf_op jit(solution)/shard_map/ppermute | solution.py:46
  22.6 3.9 %collective-permute-done.3 = bf16[1,512,128]{2,1,0:T(8,128)(2,1)S(1)} collective-permute-done((bf16[1,512,128]{2,1,0:T(8,128)(2,1)S(1)}, bf16[1,512,128]{2,1,0:T(8,128)(2,1)S(1)}, u32[]{:S(2)}, u32[]{:S(2)}) %collective-permute-start.3) | collective-permute-done | bytes 131104 | tf_op jit(solution)/shard_map/ppermute | solution.py:46
  26.5 4.4 %collective-permute-start.4 = (bf16[7,512,128]{2,1,0:T(8,128)(2,1)S(1)}, bf16[7,512,128]{2,1,0:T(8,128)(2,1)S(1)}, u32[]{:S(2)}, u32[]{:S(2)}) collective-permute-start(bf16[7,512,128]{2,1,0:T(8,128)(2,1)S(1)} %constant_dynamic-update-slice_fusion.received.refs_1_), channel_id=1, source_target_pairs={{0,1},{1,0},{2,3},{3,2},{4,5},{5,4},{6,7},{7,6},{8,9},{9,8},{10,11... | collective-permute-start | bytes 2752520 | tf_op jit(solution)/shard_map/ppermute | solution.py:48
  31.0 3.4 %shard_map.74.w = bf16[16,128,256]{2,1,0:T(8,128)(2,1)} custom-call(s32[1]{0:T(128)} %bitcast.place, f32[2,2,2048]{2,1,0:T(2,128)} %gain.9, bf16[2,2048,128]{2,1,0:T(8,128)(2,1)} %refs_0_.6, bf16[2,2048,128]{2,1,0:T(8,128)(2,1)} %refs_1_.3), custom_call_target="tpu_custom_call" | custom-call | flops 1000000000 | bytes 2129924 | tf_op jit(solution)/shard_map/pallas_call | solution.py:335
  34.4 1.2 copy-done.5
  35.7 0.6 shard_map.75
  36.3 0.0 copy-start
  36.3 0.0 copy-start.3
  36.3 1.2 shard_map.76
  37.5 0.0 copy-start.4
  37.5 3.1 %collective-permute-start.5 = (bf16[512,256]{1,0:T(8,128)(2,1)S(1)}, bf16[512,256]{1,0:T(8,128)(2,1)S(1)}, u32[]{:S(2)}, u32[]{:S(2)}) collective-permute-start(bf16[512,256]{1,0:T(8,128)(2,1)S(1)} %get-tuple-element.28.refs_5_), channel_id=1, source_target_pairs={{0,16},{16,32},{32,48},{48,64},{64,80},{80,96},{96,112},{112,128},... | collective-permute-start | bytes 786440 | tf_op jit(solution)/shard_map/ppermute | solution.py:369
  40.7 1.1 shard_map.73.refs_3_
  41.8 3.3 %shard_map.77 = (bf16[512,128]{1,0:T(8,128)(2,1)S(1)}, f32[512,128]{1,0:T(8,128)S(1)}, f32[512,128]{1,0:T(8,128)S(1)}, f32[512,128]{1,0:T(8,128)S(1)}, f32[2,128,128]{2,1,0:T(8,128)S(1)}) custom-call(bf16[2,512,128]{2,1,0:T(8,128)(2,1)S(1)} %bitcast.15, bf16[7,512,128]{2,1,0:T(8,128)(2,1)S(1)} %constant_dynamic-update-slice_fusion.received.refs_1_, ...), custom_call_target="tpu_custom_call" | custom-call | flops 2000000000 | bytes 3149840 | tf_op jit(solution)/shard_map/pallas_call | solution.py:335
  45.1 5.5 %collective-permute-done.5.kv = bf16[512,256]{1,0:T(8,128)(2,1)S(1)} collective-permute-done((bf16[512,256]{1,0:T(8,128)(2,1)S(1)}, bf16[512,256]{1,0:T(8,128)(2,1)S(1)}, u32[]{:S(2)}, u32[]{:S(2)}) %collective-permute-start.5) | collective-permute-done | bytes 262176 | tf_op jit(solution)/shard_map/ppermute | solution.py:369
  50.6 1.6 shard_map.78
  52.2 0.0 copy-start.6
  52.2 2.6 %all-gather.1 = bf16[1024,128]{1,0:T(8,128)(2,1)S(1)} all-gather(bf16[512,128]{1,0:T(8,128)(2,1)S(1)} %shard_map.78), channel_id=3, replica_groups=mesh['sp'=32,'y'=8,'c'=2] {'c'}, dimensions={0}, use_global_device_ids=true | all-gather | bytes 393216 | tf_op jit(solution)/shard_map/all_gather | solution.py:41
  54.8 2.7 %collective-permute-start.7 = (bf16[2,512,128]{2,1,0:T(8,128)(2,1)S(1)}, bf16[2,512,128]{2,1,0:T(8,128)(2,1)S(1)}, u32[]{:S(2)}, u32[]{:S(2)}) collective-permute-start(bf16[2,512,128]{2,1,0:T(8,128)(2,1)S(1)} %bitcast.24), channel_id=1, source_target_pairs={{0,4},{1,13},{2,6},{3,15},{4,8},{5,1},{6,10},{7,3},{8,12},{9,5},{1... | collective-permute-start | bytes 786440 | tf_op jit(solution)/shard_map/ppermute | solution.py:42
  57.5 6.3 %collective-permute-start.6 = (bf16[2,512,128]{2,1,0:T(8,128)(2,1)S(1)}, bf16[2,512,128]{2,1,0:T(8,128)(2,1)S(1)}, u32[]{:S(2)}, u32[]{:S(2)}) collective-permute-start(bf16[2,512,128]{2,1,0:T(8,128)(2,1)S(1)} %bitcast.25), channel_id=1, source_target_pairs={{0,2},{1,15},{2,4},{3,1},{4,6},{5,3},{6,8},{7,5},{8,10},{9,7},{10,... | collective-permute-start | bytes 786440 | tf_op jit(solution)/shard_map/ppermute | solution.py:43
  63.8 5.9 %collective-permute-start.8 = (bf16[2,512,128]{2,1,0:T(8,128)(2,1)S(1)}, bf16[2,512,128]{2,1,0:T(8,128)(2,1)S(1)}, u32[]{:S(2)}, u32[]{:S(2)}) collective-permute-start(bf16[2,512,128]{2,1,0:T(8,128)(2,1)S(1)} %collective-permute-done.7), channel_id=1, source_target_pairs={{0,2},{1,15},{2,4},{3,1},{4,6},{5,3},{6,8},{7,5},{8,10},{9,7},{10,... | collective-permute-start | bytes 786440 | tf_op jit(solution)/shard_map/ppermute | solution.py:45
  69.7 3.6 %collective-permute-start.9 = (bf16[1,512,128]{2,1,0:T(8,128)(2,1)S(1)}, bf16[1,512,128]{2,1,0:T(8,128)(2,1)S(1)}, u32[]{:S(2)}, u32[]{:S(2)}) collective-permute-start(bf16[1,512,128]{2,1,0:T(8,128)(2,1)S(1)} %constant_dynamic-slice_fusion.3), channel_id=1, source_target_pairs={{0,4},{1,13},{2,6},{3,15},{4,8},{5,1},{6,10},{7,3},{8,12},{9,5},{1... | collective-permute-start | bytes 393224 | tf_op jit(solution)/shard_map/ppermute | solution.py:46
  73.5 4.2 %collective-permute-done.9 = bf16[1,512,128]{2,1,0:T(8,128)(2,1)S(1)} collective-permute-done((bf16[1,512,128]{2,1,0:T(8,128)(2,1)S(1)}, bf16[1,512,128]{2,1,0:T(8,128)(2,1)S(1)}, u32[]{:S(2)}, u32[]{:S(2)}) %collective-permute-start.9) | collective-permute-done | bytes 131104 | tf_op jit(solution)/shard_map/ppermute | solution.py:46
  77.8 5.9 %collective-permute-start.10 = (bf16[7,512,128]{2,1,0:T(8,128)(2,1)S(1)}, bf16[7,512,128]{2,1,0:T(8,128)(2,1)S(1)}, u32[]{:S(2)}, u32[]{:S(2)}) collective-permute-start(bf16[7,512,128]{2,1,0:T(8,128)(2,1)S(1)} %constant_dynamic-update-slice_fusion.4.received), channel_id=1, source_target_pairs={{0,1},{1,0},{2,3},{3,2},{4,5},{5,4},{6,7},{7,6},{8,9},{9,8},{10,11... | collective-permute-start | bytes 2752520 | tf_op jit(solution)/shard_map/ppermute | solution.py:48
  83.6 0.1 slice_bitcast_fusion
  83.7 0.5 shard_map.79.acc
  84.2 1.5 collective-permute-done.10.other
  85.7 0.4 shard_map.80
  86.1 0.0 copy-start.1
  86.1 0.0 copy-start.2
  86.1 2.1 %all-gather.2 = bf16[1024,128]{1,0:T(8,128)(2,1)S(1)} all-gather(bf16[512,128]{1,0:T(8,128)(2,1)S(1)} %shard_map.80), channel_id=4, replica_groups=mesh['sp'=32,'y'=8,'c'=2] {'c'}, dimensions={0}, use_global_device_ids=true | all-gather | bytes 393216 | tf_op jit(solution)/shard_map/all_gather | solution.py:41
  88.3 3.8 %collective-permute-start.12 = (bf16[2,512,128]{2,1,0:T(8,128)(2,1)S(1)}, bf16[2,512,128]{2,1,0:T(8,128)(2,1)S(1)}, u32[]{:S(2)}, u32[]{:S(2)}) collective-permute-start(bf16[2,512,128]{2,1,0:T(8,128)(2,1)S(1)} %bitcast.20), channel_id=1, source_target_pairs={{0,4},{1,13},{2,6},{3,15},{4,8},{5,1},{6,10},{7,3},{8,12},{9,5},{1... | collective-permute-start | bytes 786440 | tf_op jit(solution)/shard_map/ppermute | solution.py:42
  92.1 2.1 %collective-permute-start.11 = (bf16[2,512,128]{2,1,0:T(8,128)(2,1)S(1)}, bf16[2,512,128]{2,1,0:T(8,128)(2,1)S(1)}, u32[]{:S(2)}, u32[]{:S(2)}) collective-permute-start(bf16[2,512,128]{2,1,0:T(8,128)(2,1)S(1)} %bitcast.21), channel_id=1, source_target_pairs={{0,2},{1,15},{2,4},{3,1},{4,6},{5,3},{6,8},{7,5},{8,10},{9,7},{10,... | collective-permute-start | bytes 786440 | tf_op jit(solution)/shard_map/ppermute | solution.py:43
  94.2 4.1 %collective-permute-done.12 = bf16[2,512,128]{2,1,0:T(8,128)(2,1)S(1)} collective-permute-done((bf16[2,512,128]{2,1,0:T(8,128)(2,1)S(1)}, bf16[2,512,128]{2,1,0:T(8,128)(2,1)S(1)}, u32[]{:S(2)}, u32[]{:S(2)}) %collective-permute-start.12) | collective-permute-done | bytes 262176 | tf_op jit(solution)/shard_map/ppermute | solution.py:42
  98.3 4.8 %collective-permute-start.13 = (bf16[2,512,128]{2,1,0:T(8,128)(2,1)S(1)}, bf16[2,512,128]{2,1,0:T(8,128)(2,1)S(1)}, u32[]{:S(2)}, u32[]{:S(2)}) collective-permute-start(bf16[2,512,128]{2,1,0:T(8,128)(2,1)S(1)} %collective-permute-done.12), channel_id=1, source_target_pairs={{0,2},{1,15},{2,4},{3,1},{4,6},{5,3},{6,8},{7,5},{8,10},{9,7},{10,... | collective-permute-start | bytes 786440 | tf_op jit(solution)/shard_map/ppermute | solution.py:45
  103.1 2.2 %collective-permute-start.14 = (bf16[1,512,128]{2,1,0:T(8,128)(2,1)S(1)}, bf16[1,512,128]{2,1,0:T(8,128)(2,1)S(1)}, u32[]{:S(2)}, u32[]{:S(2)}) collective-permute-start(bf16[1,512,128]{2,1,0:T(8,128)(2,1)S(1)} %constant_dynamic-slice_fusion.2), channel_id=1, source_target_pairs={{0,4},{1,13},{2,6},{3,15},{4,8},{5,1},{6,10},{7,3},{8,12},{9,5},{1... | collective-permute-start | bytes 393224 | tf_op jit(solution)/shard_map/ppermute | solution.py:46
  105.4 1.0 collective-permute-done.13
  106.4 4.6 %collective-permute-done.14 = bf16[1,512,128]{2,1,0:T(8,128)(2,1)S(1)} collective-permute-done((bf16[1,512,128]{2,1,0:T(8,128)(2,1)S(1)}, bf16[1,512,128]{2,1,0:T(8,128)(2,1)S(1)}, u32[]{:S(2)}, u32[]{:S(2)}) %collective-permute-start.14) | collective-permute-done | bytes 131104 | tf_op jit(solution)/shard_map/ppermute | solution.py:46
  111.1 3.1 %collective-permute-start.15 = (bf16[7,512,128]{2,1,0:T(8,128)(2,1)S(1)}, bf16[7,512,128]{2,1,0:T(8,128)(2,1)S(1)}, u32[]{:S(2)}, u32[]{:S(2)}) collective-permute-start(bf16[7,512,128]{2,1,0:T(8,128)(2,1)S(1)} %constant_dynamic-update-slice_fusion.8.received.b_received), channel_id=1, source_target_pairs={{0,1},{1,0},{2,3},{3,2},{4,5},{5,4},{6,7},{7,6},{8,9},{9,8},{10,11... | collective-permute-start | bytes 2752520 | tf_op jit(solution)/shard_map/ppermute | solution.py:48
  114.2 1.8 shard_map.82.w
  116.0 0.1 shard_map.81.b_total
  116.1 0.1 collective-permute-done.15.b_other
  116.2 3.0 %shard_map.83 = (bf16[512,256]{1,0:T(8,128)(2,1)S(1)}, f32[512,128]{1,0:T(8,128)S(1)}, bf16[16,512,128]{2,1,0:T(8,128)(2,1)S(1)}, bf16[512,128]{1,0:T(8,128)(2,1)S(1)}) custom-call(s32[1]{0:T(128)} %bitcast.place, bf16[2,512,128]{2,1,0:T(8,128)(2,1)S(1)} %bitcast.16, bf16[7,512,128]{2,1,0:T(8,128)(2,1)S(1)} %constant_dynamic-update-slice_fusion.received.refs_1_, ...), custom_call_target="tpu_custom_call" | custom-call | flops 2000000000 | bytes 5537796 | tf_op jit(solution)/shard_map/pallas_call | solution.py:335
  119.3 2.1 %collective-permute-start.16 = (bf16[512,256]{1,0:T(8,128)(2,1)S(1)}, bf16[512,256]{1,0:T(8,128)(2,1)S(1)}, u32[]{:S(2)}, u32[]{:S(2)}) collective-permute-start(bf16[512,256]{1,0:T(8,128)(2,1)S(1)} %get-tuple-element.36.refs_3_), channel_id=1, source_target_pairs={{0,16},{16,32},{32,48},{48,64},{64,80},{80,96},{96,112},{112,128},... | collective-permute-start | bytes 786440 | tf_op jit(solution)/shard_map/ppermute | solution.py:369
  121.4 1.1 shard_map.84.refs_1_
  122.5 3.3 %shard_map.85 = (bf16[512,128]{1,0:T(8,128)(2,1)S(1)}, f32[512,128]{1,0:T(8,128)S(1)}, f32[512,128]{1,0:T(8,128)S(1)}, f32[512,128]{1,0:T(8,128)S(1)}, f32[2,128,128]{2,1,0:T(8,128)S(1)}) custom-call(bf16[16,512,128]{2,1,0:T(8,128)(2,1)S(1)} %get-tuple-element.34.refs_0_, bf16[16,128,128]{2,1,0:T(8,128)(2,1)S(1)} %shard_map.84.refs_1_, ...), custom_call_target="tpu_custom_call" | custom-call | flops 2000000000 | bytes 3149840 | tf_op jit(solution)/shard_map/pallas_call | solution.py:335
  125.8 6.2 %collective-permute-done.16.kv = bf16[512,256]{1,0:T(8,128)(2,1)S(1)} collective-permute-done((bf16[512,256]{1,0:T(8,128)(2,1)S(1)}, bf16[512,256]{1,0:T(8,128)(2,1)S(1)}, u32[]{:S(2)}, u32[]{:S(2)}) %collective-permute-start.16) | collective-permute-done | bytes 262176 | tf_op jit(solution)/shard_map/ppermute | solution.py:369
  132.0 1.5 shard_map.86
  133.5 2.9 %all-gather.3 = bf16[1024,128]{1,0:T(8,128)(2,1)S(1)} all-gather(bf16[512,128]{1,0:T(8,128)(2,1)S(1)} %shard_map.86), channel_id=5, replica_groups=mesh['sp'=32,'y'=8,'c'=2] {'c'}, dimensions={0}, use_global_device_ids=true | all-gather | bytes 393216 | tf_op jit(solution)/shard_map/all_gather | solution.py:41
  136.4 3.2 %collective-permute-start.18 = (bf16[2,512,128]{2,1,0:T(8,128)(2,1)S(1)}, bf16[2,512,128]{2,1,0:T(8,128)(2,1)S(1)}, u32[]{:S(2)}, u32[]{:S(2)}) collective-permute-start(bf16[2,512,128]{2,1,0:T(8,128)(2,1)S(1)} %bitcast.17), channel_id=1, source_target_pairs={{0,4},{1,13},{2,6},{3,15},{4,8},{5,1},{6,10},{7,3},{8,12},{9,5},{1... | collective-permute-start | bytes 786440 | tf_op jit(solution)/shard_map/ppermute | solution.py:42
  139.6 5.7 %collective-permute-start.17 = (bf16[2,512,128]{2,1,0:T(8,128)(2,1)S(1)}, bf16[2,512,128]{2,1,0:T(8,128)(2,1)S(1)}, u32[]{:S(2)}, u32[]{:S(2)}) collective-permute-start(bf16[2,512,128]{2,1,0:T(8,128)(2,1)S(1)} %bitcast.18), channel_id=1, source_target_pairs={{0,2},{1,15},{2,4},{3,1},{4,6},{5,3},{6,8},{7,5},{8,10},{9,7},{10,... | collective-permute-start | bytes 786440 | tf_op jit(solution)/shard_map/ppermute | solution.py:43
  145.3 6.2 %collective-permute-start.19 = (bf16[2,512,128]{2,1,0:T(8,128)(2,1)S(1)}, bf16[2,512,128]{2,1,0:T(8,128)(2,1)S(1)}, u32[]{:S(2)}, u32[]{:S(2)}) collective-permute-start(bf16[2,512,128]{2,1,0:T(8,128)(2,1)S(1)} %collective-permute-done.18), channel_id=1, source_target_pairs={{0,2},{1,15},{2,4},{3,1},{4,6},{5,3},{6,8},{7,5},{8,10},{9,7},{10,... | collective-permute-start | bytes 786440 | tf_op jit(solution)/shard_map/ppermute | solution.py:45
  151.6 3.5 %collective-permute-start.20 = (bf16[1,512,128]{2,1,0:T(8,128)(2,1)S(1)}, bf16[1,512,128]{2,1,0:T(8,128)(2,1)S(1)}, u32[]{:S(2)}, u32[]{:S(2)}) collective-permute-start(bf16[1,512,128]{2,1,0:T(8,128)(2,1)S(1)} %constant_dynamic-slice_fusion.1), channel_id=1, source_target_pairs={{0,4},{1,13},{2,6},{3,15},{4,8},{5,1},{6,10},{7,3},{8,12},{9,5},{1... | collective-permute-start | bytes 393224 | tf_op jit(solution)/shard_map/ppermute | solution.py:46
  155.3 4.1 %collective-permute-done.20 = bf16[1,512,128]{2,1,0:T(8,128)(2,1)S(1)} collective-permute-done((bf16[1,512,128]{2,1,0:T(8,128)(2,1)S(1)}, bf16[1,512,128]{2,1,0:T(8,128)(2,1)S(1)}, u32[]{:S(2)}, u32[]{:S(2)}) %collective-permute-start.20) | collective-permute-done | bytes 131104 | tf_op jit(solution)/shard_map/ppermute | solution.py:46
  159.3 5.8 %collective-permute-start.21 = (bf16[7,512,128]{2,1,0:T(8,128)(2,1)S(1)}, bf16[7,512,128]{2,1,0:T(8,128)(2,1)S(1)}, u32[]{:S(2)}, u32[]{:S(2)}) collective-permute-start(bf16[7,512,128]{2,1,0:T(8,128)(2,1)S(1)} %constant_dynamic-update-slice_fusion.12.received), channel_id=1, source_target_pairs={{0,1},{1,0},{2,3},{3,2},{4,5},{5,4},{6,7},{7,6},{8,9},{9,8},{10,11... | collective-permute-start | bytes 2752520 | tf_op jit(solution)/shard_map/ppermute | solution.py:48
  165.2 2.1 %collective-permute-done.21.other = bf16[7,512,128]{2,1,0:T(8,128)(2,1)S(1)} collective-permute-done((bf16[7,512,128]{2,1,0:T(8,128)(2,1)S(1)}, bf16[7,512,128]{2,1,0:T(8,128)(2,1)S(1)}, u32[]{:S(2)}, u32[]{:S(2)}) %collective-permute-start.21) | collective-permute-done | bytes 917536 | tf_op jit(solution)/shard_map/ppermute | solution.py:48
  167.2 1.4 shard_map.87
  168.6 6.2 %all-to-all-start = ((f32[16,4,128]{2,1,0:T(4,128)}), f32[16,4,128]{2,1,0:T(4,128)S(1)}, u32[]{:S(2)}, u32[]{:S(2)}) async-start(f32[16,4,128]{2,1,0:T(4,128)} %get-tuple-element.42), calls=%async_computation | async-start | bytes 65536 | tf_op jit(solution)/shard_map/all_to_all | solution.py:419
  174.9 7.4 %all-to-all-done.squares = f32[16,4,128]{2,1,0:T(4,128)S(1)} async-done(((f32[16,4,128]{2,1,0:T(4,128)}), f32[16,4,128]{2,1,0:T(4,128)S(1)}, u32[]{:S(2)}, u32[]{:S(2)}) %all-to-all-start) | async-done | bytes 32800 | tf_op jit(solution)/shard_map/all_to_all | solution.py:419
  182.3 0.8 shard_map.88
  (39 shorter events, 0.6 us)
Async XLA Ops:
  2.5 12.0 %collective-permute-start.1 = (bf16[2,512,128]{2,1,0:T(8,128)(2,1)S(1)}, bf16[2,512,128]{2,1,0:T(8,128)(2,1)S(1)}, u32[]{:S(2)}, u32[]{:S(2)}) collective-permute-start(bf16[2,512,128]{2,1,0:T(8,128)(2,1)S(1)} %bitcast.12), channel_id=1, source_target_pairs={{0,4},{1,13},{2,6},{3,15},{4,8},{5,1},{6,10},{7,3},{8,12},{9,5},{1... | collective-permute-start | bytes 786440 | tf_op jit(solution)/shard_map/ppermute | solution.py:42
  8.4 14.1 %collective-permute-start = (bf16[2,512,128]{2,1,0:T(8,128)(2,1)S(1)}, bf16[2,512,128]{2,1,0:T(8,128)(2,1)S(1)}, u32[]{:S(2)}, u32[]{:S(2)}) collective-permute-start(bf16[2,512,128]{2,1,0:T(8,128)(2,1)S(1)} %bitcast.13), channel_id=1, source_target_pairs={{0,2},{1,15},{2,4},{3,1},{4,6},{5,3},{6,8},{7,5},{8,10},{9,7},{10,... | collective-permute-start | bytes 786440 | tf_op jit(solution)/shard_map/ppermute | solution.py:43
  14.5 8.1 %collective-permute-start.2 = (bf16[2,512,128]{2,1,0:T(8,128)(2,1)S(1)}, bf16[2,512,128]{2,1,0:T(8,128)(2,1)S(1)}, u32[]{:S(2)}, u32[]{:S(2)}) collective-permute-start(bf16[2,512,128]{2,1,0:T(8,128)(2,1)S(1)} %collective-permute-done.1), channel_id=1, source_target_pairs={{0,2},{1,15},{2,4},{3,1},{4,6},{5,3},{6,8},{7,5},{8,10},{9,7},{10,... | collective-permute-start | bytes 786440 | tf_op jit(solution)/shard_map/ppermute | solution.py:45
  18.6 7.9 %collective-permute-start.3 = (bf16[1,512,128]{2,1,0:T(8,128)(2,1)S(1)}, bf16[1,512,128]{2,1,0:T(8,128)(2,1)S(1)}, u32[]{:S(2)}, u32[]{:S(2)}) collective-permute-start(bf16[1,512,128]{2,1,0:T(8,128)(2,1)S(1)} %constant_dynamic-slice_fusion.4), channel_id=1, source_target_pairs={{0,4},{1,13},{2,6},{3,15},{4,8},{5,1},{6,10},{7,3},{8,12},{9,5},{1... | collective-permute-start | bytes 393224 | tf_op jit(solution)/shard_map/ppermute | solution.py:46
  26.5 9.7 %collective-permute-start.4 = (bf16[7,512,128]{2,1,0:T(8,128)(2,1)S(1)}, bf16[7,512,128]{2,1,0:T(8,128)(2,1)S(1)}, u32[]{:S(2)}, u32[]{:S(2)}) collective-permute-start(bf16[7,512,128]{2,1,0:T(8,128)(2,1)S(1)} %constant_dynamic-update-slice_fusion.received.refs_1_), channel_id=1, source_target_pairs={{0,1},{1,0},{2,3},{3,2},{4,5},{5,4},{6,7},{7,6},{8,9},{9,8},{10,11... | collective-permute-start | bytes 2752520 | tf_op jit(solution)/shard_map/ppermute | solution.py:48
  34.4 1.2 copy-start.5
  36.3 4.4 %copy-start = (f32[2,2,2048]{2,1,0:T(2,128)S(1)}, f32[2,2,2048]{2,1,0:T(2,128)}, u32[]{:S(2)}) copy-start(f32[2,2,2048]{2,1,0:T(2,128)} %gain.9) | copy-start | bytes 98308
  36.3 4.4 %copy-start.3 = (bf16[2,2048,128]{2,1,0:T(8,128)(2,1)S(1)}, bf16[2,2048,128]{2,1,0:T(8,128)(2,1)}, u32[]{:S(2)}) copy-start(bf16[2,2048,128]{2,1,0:T(8,128)(2,1)} %refs_0_.7) | copy-start | bytes 3145732
  37.5 4.3 %copy-start.4 = (f32[2,2,257]{2,1,0:T(2,128)S(1)}, f32[2,2,257]{2,1,0:T(2,128)}, u32[]{:S(2)}) copy-start(f32[2,2,257]{2,1,0:T(2,128)} %bias.3) | copy-start | bytes 12340
  37.5 13.1 %collective-permute-start.5 = (bf16[512,256]{1,0:T(8,128)(2,1)S(1)}, bf16[512,256]{1,0:T(8,128)(2,1)S(1)}, u32[]{:S(2)}, u32[]{:S(2)}) collective-permute-start(bf16[512,256]{1,0:T(8,128)(2,1)S(1)} %get-tuple-element.28.refs_5_), channel_id=1, source_target_pairs={{0,16},{16,32},{32,48},{48,64},{64,80},{80,96},{96,112},{112,128},... | collective-permute-start | bytes 786440 | tf_op jit(solution)/shard_map/ppermute | solution.py:369
  52.2 31.4 %copy-start.6 = (bf16[2,2048,128]{2,1,0:T(8,128)(2,1)S(1)}, bf16[2,2048,128]{2,1,0:T(8,128)(2,1)}, u32[]{:S(2)}) copy-start(bf16[2,2048,128]{2,1,0:T(8,128)(2,1)} %param.12) | copy-start | bytes 3145732
  54.8 8.9 %collective-permute-start.7 = (bf16[2,512,128]{2,1,0:T(8,128)(2,1)S(1)}, bf16[2,512,128]{2,1,0:T(8,128)(2,1)S(1)}, u32[]{:S(2)}, u32[]{:S(2)}) collective-permute-start(bf16[2,512,128]{2,1,0:T(8,128)(2,1)S(1)} %bitcast.24), channel_id=1, source_target_pairs={{0,4},{1,13},{2,6},{3,15},{4,8},{5,1},{6,10},{7,3},{8,12},{9,5},{1... | collective-permute-start | bytes 786440 | tf_op jit(solution)/shard_map/ppermute | solution.py:42
  57.5 15.9 %collective-permute-start.6 = (bf16[2,512,128]{2,1,0:T(8,128)(2,1)S(1)}, bf16[2,512,128]{2,1,0:T(8,128)(2,1)S(1)}, u32[]{:S(2)}, u32[]{:S(2)}) collective-permute-start(bf16[2,512,128]{2,1,0:T(8,128)(2,1)S(1)} %bitcast.25), channel_id=1, source_target_pairs={{0,2},{1,15},{2,4},{3,1},{4,6},{5,3},{6,8},{7,5},{8,10},{9,7},{10,... | collective-permute-start | bytes 786440 | tf_op jit(solution)/shard_map/ppermute | solution.py:43
  63.8 9.7 %collective-permute-start.8 = (bf16[2,512,128]{2,1,0:T(8,128)(2,1)S(1)}, bf16[2,512,128]{2,1,0:T(8,128)(2,1)S(1)}, u32[]{:S(2)}, u32[]{:S(2)}) collective-permute-start(bf16[2,512,128]{2,1,0:T(8,128)(2,1)S(1)} %collective-permute-done.7), channel_id=1, source_target_pairs={{0,2},{1,15},{2,4},{3,1},{4,6},{5,3},{6,8},{7,5},{8,10},{9,7},{10,... | collective-permute-start | bytes 786440 | tf_op jit(solution)/shard_map/ppermute | solution.py:45
  69.7 8.0 %collective-permute-start.9 = (bf16[1,512,128]{2,1,0:T(8,128)(2,1)S(1)}, bf16[1,512,128]{2,1,0:T(8,128)(2,1)S(1)}, u32[]{:S(2)}, u32[]{:S(2)}) collective-permute-start(bf16[1,512,128]{2,1,0:T(8,128)(2,1)S(1)} %constant_dynamic-slice_fusion.3), channel_id=1, source_target_pairs={{0,4},{1,13},{2,6},{3,15},{4,8},{5,1},{6,10},{7,3},{8,12},{9,5},{1... | collective-permute-start | bytes 393224 | tf_op jit(solution)/shard_map/ppermute | solution.py:46
  77.8 7.9 %collective-permute-start.10 = (bf16[7,512,128]{2,1,0:T(8,128)(2,1)S(1)}, bf16[7,512,128]{2,1,0:T(8,128)(2,1)S(1)}, u32[]{:S(2)}, u32[]{:S(2)}) collective-permute-start(bf16[7,512,128]{2,1,0:T(8,128)(2,1)S(1)} %constant_dynamic-update-slice_fusion.4.received), channel_id=1, source_target_pairs={{0,1},{1,0},{2,3},{3,2},{4,5},{5,4},{6,7},{7,6},{8,9},{9,8},{10,11... | collective-permute-start | bytes 2752520 | tf_op jit(solution)/shard_map/ppermute | solution.py:48
  86.1 28.0 %copy-start.1 = (bf16[2,2048,128]{2,1,0:T(8,128)(2,1)S(1)}, bf16[2,2048,128]{2,1,0:T(8,128)(2,1)}, u32[]{:S(2)}) copy-start(bf16[2,2048,128]{2,1,0:T(8,128)(2,1)} %refs_0_.6) | copy-start | bytes 3145732
  86.1 28.0 %copy-start.2 = (bf16[2,2048,128]{2,1,0:T(8,128)(2,1)S(1)}, bf16[2,2048,128]{2,1,0:T(8,128)(2,1)}, u32[]{:S(2)}) copy-start(bf16[2,2048,128]{2,1,0:T(8,128)(2,1)} %refs_1_.3) | copy-start | bytes 3145732
  88.3 10.0 %collective-permute-start.12 = (bf16[2,512,128]{2,1,0:T(8,128)(2,1)S(1)}, bf16[2,512,128]{2,1,0:T(8,128)(2,1)S(1)}, u32[]{:S(2)}, u32[]{:S(2)}) collective-permute-start(bf16[2,512,128]{2,1,0:T(8,128)(2,1)S(1)} %bitcast.20), channel_id=1, source_target_pairs={{0,4},{1,13},{2,6},{3,15},{4,8},{5,1},{6,10},{7,3},{8,12},{9,5},{1... | collective-permute-start | bytes 786440 | tf_op jit(solution)/shard_map/ppermute | solution.py:42
  92.1 13.2 %collective-permute-start.11 = (bf16[2,512,128]{2,1,0:T(8,128)(2,1)S(1)}, bf16[2,512,128]{2,1,0:T(8,128)(2,1)S(1)}, u32[]{:S(2)}, u32[]{:S(2)}) collective-permute-start(bf16[2,512,128]{2,1,0:T(8,128)(2,1)S(1)} %bitcast.21), channel_id=1, source_target_pairs={{0,2},{1,15},{2,4},{3,1},{4,6},{5,3},{6,8},{7,5},{8,10},{9,7},{10,... | collective-permute-start | bytes 786440 | tf_op jit(solution)/shard_map/ppermute | solution.py:43
  98.3 8.1 %collective-permute-start.13 = (bf16[2,512,128]{2,1,0:T(8,128)(2,1)S(1)}, bf16[2,512,128]{2,1,0:T(8,128)(2,1)S(1)}, u32[]{:S(2)}, u32[]{:S(2)}) collective-permute-start(bf16[2,512,128]{2,1,0:T(8,128)(2,1)S(1)} %collective-permute-done.12), channel_id=1, source_target_pairs={{0,2},{1,15},{2,4},{3,1},{4,6},{5,3},{6,8},{7,5},{8,10},{9,7},{10,... | collective-permute-start | bytes 786440 | tf_op jit(solution)/shard_map/ppermute | solution.py:45
  103.1 7.9 %collective-permute-start.14 = (bf16[1,512,128]{2,1,0:T(8,128)(2,1)S(1)}, bf16[1,512,128]{2,1,0:T(8,128)(2,1)S(1)}, u32[]{:S(2)}, u32[]{:S(2)}) collective-permute-start(bf16[1,512,128]{2,1,0:T(8,128)(2,1)S(1)} %constant_dynamic-slice_fusion.2), channel_id=1, source_target_pairs={{0,4},{1,13},{2,6},{3,15},{4,8},{5,1},{6,10},{7,3},{8,12},{9,5},{1... | collective-permute-start | bytes 393224 | tf_op jit(solution)/shard_map/ppermute | solution.py:46
  111.1 5.2 %collective-permute-start.15 = (bf16[7,512,128]{2,1,0:T(8,128)(2,1)S(1)}, bf16[7,512,128]{2,1,0:T(8,128)(2,1)S(1)}, u32[]{:S(2)}, u32[]{:S(2)}) collective-permute-start(bf16[7,512,128]{2,1,0:T(8,128)(2,1)S(1)} %constant_dynamic-update-slice_fusion.8.received.b_received), channel_id=1, source_target_pairs={{0,1},{1,0},{2,3},{3,2},{4,5},{5,4},{6,7},{7,6},{8,9},{9,8},{10,11... | collective-permute-start | bytes 2752520 | tf_op jit(solution)/shard_map/ppermute | solution.py:48
  119.3 12.7 %collective-permute-start.16 = (bf16[512,256]{1,0:T(8,128)(2,1)S(1)}, bf16[512,256]{1,0:T(8,128)(2,1)S(1)}, u32[]{:S(2)}, u32[]{:S(2)}) collective-permute-start(bf16[512,256]{1,0:T(8,128)(2,1)S(1)} %get-tuple-element.36.refs_3_), channel_id=1, source_target_pairs={{0,16},{16,32},{32,48},{48,64},{64,80},{80,96},{96,112},{112,128},... | collective-permute-start | bytes 786440 | tf_op jit(solution)/shard_map/ppermute | solution.py:369
  136.4 8.9 %collective-permute-start.18 = (bf16[2,512,128]{2,1,0:T(8,128)(2,1)S(1)}, bf16[2,512,128]{2,1,0:T(8,128)(2,1)S(1)}, u32[]{:S(2)}, u32[]{:S(2)}) collective-permute-start(bf16[2,512,128]{2,1,0:T(8,128)(2,1)S(1)} %bitcast.17), channel_id=1, source_target_pairs={{0,4},{1,13},{2,6},{3,15},{4,8},{5,1},{6,10},{7,3},{8,12},{9,5},{1... | collective-permute-start | bytes 786440 | tf_op jit(solution)/shard_map/ppermute | solution.py:42
  139.6 15.5 %collective-permute-start.17 = (bf16[2,512,128]{2,1,0:T(8,128)(2,1)S(1)}, bf16[2,512,128]{2,1,0:T(8,128)(2,1)S(1)}, u32[]{:S(2)}, u32[]{:S(2)}) collective-permute-start(bf16[2,512,128]{2,1,0:T(8,128)(2,1)S(1)} %bitcast.18), channel_id=1, source_target_pairs={{0,2},{1,15},{2,4},{3,1},{4,6},{5,3},{6,8},{7,5},{8,10},{9,7},{10,... | collective-permute-start | bytes 786440 | tf_op jit(solution)/shard_map/ppermute | solution.py:43
  145.3 9.9 %collective-permute-start.19 = (bf16[2,512,128]{2,1,0:T(8,128)(2,1)S(1)}, bf16[2,512,128]{2,1,0:T(8,128)(2,1)S(1)}, u32[]{:S(2)}, u32[]{:S(2)}) collective-permute-start(bf16[2,512,128]{2,1,0:T(8,128)(2,1)S(1)} %collective-permute-done.18), channel_id=1, source_target_pairs={{0,2},{1,15},{2,4},{3,1},{4,6},{5,3},{6,8},{7,5},{8,10},{9,7},{10,... | collective-permute-start | bytes 786440 | tf_op jit(solution)/shard_map/ppermute | solution.py:45
  151.6 7.7 %collective-permute-start.20 = (bf16[1,512,128]{2,1,0:T(8,128)(2,1)S(1)}, bf16[1,512,128]{2,1,0:T(8,128)(2,1)S(1)}, u32[]{:S(2)}, u32[]{:S(2)}) collective-permute-start(bf16[1,512,128]{2,1,0:T(8,128)(2,1)S(1)} %constant_dynamic-slice_fusion.1), channel_id=1, source_target_pairs={{0,4},{1,13},{2,6},{3,15},{4,8},{5,1},{6,10},{7,3},{8,12},{9,5},{1... | collective-permute-start | bytes 393224 | tf_op jit(solution)/shard_map/ppermute | solution.py:46
  159.3 7.9 %collective-permute-start.21 = (bf16[7,512,128]{2,1,0:T(8,128)(2,1)S(1)}, bf16[7,512,128]{2,1,0:T(8,128)(2,1)S(1)}, u32[]{:S(2)}, u32[]{:S(2)}) collective-permute-start(bf16[7,512,128]{2,1,0:T(8,128)(2,1)S(1)} %constant_dynamic-update-slice_fusion.12.received), channel_id=1, source_target_pairs={{0,1},{1,0},{2,3},{3,2},{4,5},{5,4},{6,7},{7,6},{8,9},{9,8},{10,11... | collective-permute-start | bytes 2752520 | tf_op jit(solution)/shard_map/ppermute | solution.py:48
  168.6 13.6 %all-to-all-start = ((f32[16,4,128]{2,1,0:T(4,128)}), f32[16,4,128]{2,1,0:T(4,128)S(1)}, u32[]{:S(2)}, u32[]{:S(2)}) async-start(f32[16,4,128]{2,1,0:T(4,128)} %get-tuple-element.42), calls=%async_computation | async-start | bytes 65536 | tf_op jit(solution)/shard_map/all_to_all | solution.py:419

commit v4 on v3

--- a/solution.py
+++ b/solution.py
@@ -35,10 +35,11 @@
     return pairs
 
 
-def gather_blocks(x):
+def gather_blocks(x, own=None):
     core = lax.axis_index("c")
 
-    own = lax.all_gather(x, "c", axis=0)
+    if own is None:
+        own = lax.all_gather(x, "c", axis=0)
     two = lax.ppermute(own, ("y", "c"), core_pairs(2))
     one = lax.ppermute(own, ("y", "c"), core_pairs(1))
     half = lax.dynamic_index_in_dim(two, core, 0, keepdims=True)
@@ -294,25 +295,31 @@
         out[rows, :] = ((acc[rows, :] * fade + more) / norm).astype(jnp.bfloat16)
 
 
-def rows_product(ids, offset, refs, w):
+def rows_product(layer, ids, offset, refs, weights):
+    count = sum(ref.shape[0] for ref in refs)
     rows = [
-        w[pl.ds(pl.multiple_of(ids[offset + k] * BLK, BLK), BLK), :]
-        for k in range(sum(ref.shape[0] for ref in refs))
+        pl.ds(pl.multiple_of(ids[offset + k] * BLK, BLK), BLK) for k in range(count)
     ]
+    right = jnp.concatenate(
+        [jnp.concatenate([w[layer, r, :] for w in weights], axis=1) for r in rows], axis=0
+    )
     left = jnp.concatenate(blocks_of(refs), axis=1)
-    return jnp.dot(left, jnp.concatenate(rows, axis=0), preferred_element_type=jnp.float32)
-
-
-def out_part_kernel(place, own, received, w, acc):
-    acc[...] = rows_product(block_ids(place), 0, (own, received), w)
-
-
-def out_kernel(place, other, w, acc, out):
-    out[...] = (acc[...] + rows_product(block_ids(place), 9, (other,), w)).astype(jnp.bfloat16)
+    return jnp.dot(left, right, preferred_element_type=jnp.float32)
+
+
+def out_part_kernel(place, own, received, w, w_other, acc):
+    acc[...] = rows_product(0, block_ids(place), 0, (own, received), (w, w_other))
+
+
+def out_kernel(place, other, w, w_other, acc, out):
+    core = place[0] % 2
+    total = acc[...] + rows_product(0, block_ids(place), 9, (other,), (w, w_other))
+    out[core] = total[:, :BLK].astype(jnp.bfloat16)
+    out[1 - core] = total[:, BLK:].astype(jnp.bfloat16)
 
 
 def last_kernel(place, own, received, other, w, out, squares):
-    out[...] = rows_product(block_ids(place), 0, (own, received, other), w)
+    out[...] = rows_product(1, block_ids(place), 0, (own, received, other), (w,))
     for i in range(4):
         x = out[i * BLK : (i + 1) * BLK, :]
         sums = jnp.sum((x * x).T, axis=0, keepdims=True)
@@ -376,13 +383,9 @@
             10**9, (first, local[0], previous, *local[1:], rel_bias),
         )
 
-    def projected(attended, w):
-        own, received, other = attended
-        acc = call(
-            out_part_kernel, [SMEM] + [VMEM] * 3, wide, [], 4, 10**9, (place, own, received, w)
-        )
-        return other, w, acc
-
+    w_other = lax.ppermute(w_out, "c", [(0, 1), (1, 0)])
+    both = jax.ShapeDtypeStruct((2, tokens, BLK), half)
+    double = jax.ShapeDtypeStruct((tokens, 2 * BLK), jnp.float32)
     wkv = scaled(0, (w_key, w_value), BIG)
     wq = scaled(0, (w_query,), 4)
     stream = gather_blocks(residual)
@@ -395,11 +398,15 @@
         first_kernel, [VMEM] * 4, (pair, wide), [], 4, 10**9, (stream[2], wkv, *parts),
     )
     attended = gather_blocks(attention(0, stream, wq, kv, inv))
+    acc = call(
+        out_part_kernel, [SMEM] + [VMEM] * 4, double, [], 4, 10**9,
+        (place, *attended[:2], w_out, w_other),
+    )
     branch = call(
-        out_kernel, [SMEM] + [VMEM] * 3, block, [], 4, 10**9,
-        (place, *projected(attended, w_out[0])),
-    )
-    branch = gather_blocks(branch)
+        out_kernel, [SMEM] + [VMEM] * 4, both, [], 4, 10**9,
+        (place, attended[2], w_out, w_other, acc),
+    )
+    branch = gather_blocks(None, branch)
     total = call(squares_kernel, [VMEM] * 2, wide, [], 4, 10**9, branch[:2])
     wkv = scaled(1, (w_key, w_value), 4)
     wq = scaled(1, (w_query,), 4)
@@ -411,7 +418,7 @@
     branch, squares = call(
         last_kernel, [SMEM] + [VMEM] * 4,
         (wide, jax.ShapeDtypeStruct((NB, tokens // BLK, BLK), jnp.float32)), [], 4, 10**9,
-        (place, *attended, w_out[1]),
+        (place, *attended, w_out),
     )
     own_gain = lax.dynamic_slice_in_dim(
         gains[1, 1].reshape(1, D), lax.axis_index(("y", "c")) * BLK, BLK, 1

time: 184 us -> 182 us (0.989)
  blocking collectives: 10.1 us -> 7.87 us
    all_gather x4 -> x3, blocking collectives: 10.1 us -> 7.87 us  [gather_blocks(): own = lax.all_gather(x, 'c', axis=0)]
    ppermute x4, starting transfers between devices: 21 us -> 19 us  [gather_blocks(): three = lax.ppermute(two, ('y', 'c'), core_pairs(1))]
    ppermute x0 -> x1, starting transfers between devices: none -> 1.92 us  [on_device(): w_other = lax.ppermute(w_out, 'c', [(0, 1), (1, 0)])]
  transfers between devices with their start and end apart: 23 -> 24, of which waited for: 13 -> 13; matrix products, arithmetic and copies ran while one was open for 0% -> 0% of each run, Pallas kernels for 8% -> 8%
where the time goes in v4:
time: 182 us; the launch traced here: 181 us
  starting transfers between devices  97.4 us (54%)
  waiting for transfers between devices  47.8 us (26%)
  Pallas kernels  25.3 us (14%)
  blocking collectives  7.87 us (4%)
    pallas_call x16, Pallas kernels, call(): pl.pallas_call(kernel, out_shape=outs, in_specs=ins, out_specs=jax.tree.m...  25.3 us
    ppermute x4, starting transfers between devices, gather_blocks(): other = lax.ppermute(received, 'c', [(0, 1), (1, 0)])  19.2 us
    ppermute x4, starting transfers between devices, gather_blocks(): three = lax.ppermute(two, ('y', 'c'), core_pairs(1))  19 us
    ppermute x4, starting transfers between devices, gather_blocks(): one = lax.ppermute(own, ('y', 'c'), core_pairs(1))  17 us
    ppermute x4, waiting for transfers between devices, gather_blocks(): four = lax.ppermute(half, ('y', 'c'), core_pairs(2))  16.8 us
    ppermute x4, starting transfers between devices, gather_blocks(): two = lax.ppermute(own, ('y', 'c'), core_pairs(2))  15.6 us
    ppermute x4, starting transfers between devices, gather_blocks(): four = lax.ppermute(half, ('y', 'c'), core_pairs(2))  13.2 us
    ppermute x2, waiting for transfers between devices, attention(): previous = lax.ppermute(kv, 'sp', shift)  11.6 us
  transfers between devices with their start and end apart: 24, of which 13 were waited for; matrix products, arithmetic and copies ran while one was open for 0% of the time, Pallas kernels for 8%

profile of v4, /device:TPU:257, one launch (start us, length us, event | category | flops | bytes accessed | tf_op | source)
XLA Modules:
  0.0 180.8 jit_solution(14598808741831812386)
XLA Ops:
  0.0 2.5 %all-gather = bf16[1024,128]{1,0:T(8,128)(2,1)S(1)} all-gather(bf16[512,128]{1,0:T(8,128)(2,1)} %param.7), channel_id=2, replica_groups=mesh['sp'=32,'y'=8,'c'=2] {'c'}, dimensions={0}, use_global_device_ids=true | all-gather | bytes 393216 | tf_op jit(solution)/shard_map/all_gather | solution.py:42
  2.5 5.9 %collective-permute-start.1 = (bf16[2,512,128]{2,1,0:T(8,128)(2,1)S(1)}, bf16[2,512,128]{2,1,0:T(8,128)(2,1)S(1)}, u32[]{:S(2)}, u32[]{:S(2)}) collective-permute-start(bf16[2,512,128]{2,1,0:T(8,128)(2,1)S(1)} %bitcast.10), channel_id=1, source_target_pairs={{0,4},{1,13},{2,6},{3,15},{4,8},{5,1},{6,10},{7,3},{8,12},{9,5},{1... | collective-permute-start | bytes 786440 | tf_op jit(solution)/shard_map/ppermute | solution.py:43
  8.4 3.0 %collective-permute-start = (bf16[2,512,128]{2,1,0:T(8,128)(2,1)S(1)}, bf16[2,512,128]{2,1,0:T(8,128)(2,1)S(1)}, u32[]{:S(2)}, u32[]{:S(2)}) collective-permute-start(bf16[2,512,128]{2,1,0:T(8,128)(2,1)S(1)} %bitcast.11), channel_id=1, source_target_pairs={{0,2},{1,15},{2,4},{3,1},{4,6},{5,3},{6,8},{7,5},{8,10},{9,7},{10,... | collective-permute-start | bytes 786440 | tf_op jit(solution)/shard_map/ppermute | solution.py:44
  11.4 3.1 %collective-permute-done.1 = bf16[2,512,128]{2,1,0:T(8,128)(2,1)S(1)} collective-permute-done((bf16[2,512,128]{2,1,0:T(8,128)(2,1)S(1)}, bf16[2,512,128]{2,1,0:T(8,128)(2,1)S(1)}, u32[]{:S(2)}, u32[]{:S(2)}) %collective-permute-start.1) | collective-permute-done | bytes 262176 | tf_op jit(solution)/shard_map/ppermute | solution.py:43
  14.5 4.1 %collective-permute-start.2 = (bf16[2,512,128]{2,1,0:T(8,128)(2,1)S(1)}, bf16[2,512,128]{2,1,0:T(8,128)(2,1)S(1)}, u32[]{:S(2)}, u32[]{:S(2)}) collective-permute-start(bf16[2,512,128]{2,1,0:T(8,128)(2,1)S(1)} %collective-permute-done.1), channel_id=1, source_target_pairs={{0,2},{1,15},{2,4},{3,1},{4,6},{5,3},{6,8},{7,5},{8,10},{9,7},{10,... | collective-permute-start | bytes 786440 | tf_op jit(solution)/shard_map/ppermute | solution.py:46
  18.6 3.9 %collective-permute-start.3 = (bf16[1,512,128]{2,1,0:T(8,128)(2,1)S(1)}, bf16[1,512,128]{2,1,0:T(8,128)(2,1)S(1)}, u32[]{:S(2)}, u32[]{:S(2)}) collective-permute-start(bf16[1,512,128]{2,1,0:T(8,128)(2,1)S(1)} %constant_dynamic-slice_fusion.4), channel_id=1, source_target_pairs={{0,4},{1,13},{2,6},{3,15},{4,8},{5,1},{6,10},{7,3},{8,12},{9,5},{1... | collective-permute-start | bytes 393224 | tf_op jit(solution)/shard_map/ppermute | solution.py:47
  22.5 0.0 collective-permute-done
  22.6 3.9 %collective-permute-done.3 = bf16[1,512,128]{2,1,0:T(8,128)(2,1)S(1)} collective-permute-done((bf16[1,512,128]{2,1,0:T(8,128)(2,1)S(1)}, bf16[1,512,128]{2,1,0:T(8,128)(2,1)S(1)}, u32[]{:S(2)}, u32[]{:S(2)}) %collective-permute-start.3) | collective-permute-done | bytes 131104 | tf_op jit(solution)/shard_map/ppermute | solution.py:47
  26.5 4.4 %collective-permute-start.4 = (bf16[7,512,128]{2,1,0:T(8,128)(2,1)S(1)}, bf16[7,512,128]{2,1,0:T(8,128)(2,1)S(1)}, u32[]{:S(2)}, u32[]{:S(2)}) collective-permute-start(bf16[7,512,128]{2,1,0:T(8,128)(2,1)S(1)} %constant_dynamic-update-slice_fusion.received.refs_1_), channel_id=1, source_target_pairs={{0,1},{1,0},{2,3},{3,2},{4,5},{5,4},{6,7},{7,6},{8,9},{9,8},{10,11... | collective-permute-start | bytes 2752520 | tf_op jit(solution)/shard_map/ppermute | solution.py:49
  31.0 3.4 %shard_map.74.w = bf16[16,128,256]{2,1,0:T(8,128)(2,1)} custom-call(s32[1]{0:T(128)} %bitcast.place, f32[2,2,2048]{2,1,0:T(2,128)} %gain.9, bf16[2,2048,128]{2,1,0:T(8,128)(2,1)} %refs_0_.6, bf16[2,2048,128]{2,1,0:T(8,128)(2,1)} %refs_1_.3), custom_call_target="tpu_custom_call" | custom-call | flops 1000000000 | bytes 2129924 | tf_op jit(solution)/shard_map/pallas_call | solution.py:342
  34.4 1.2 copy-done.6
  35.7 0.6 shard_map.75
  36.3 0.0 copy-start.1
  36.3 0.0 copy-start.4
  36.3 1.2 shard_map.76
  37.5 0.0 copy-start.5
  37.5 3.1 %collective-permute-start.5 = (bf16[512,256]{1,0:T(8,128)(2,1)S(1)}, bf16[512,256]{1,0:T(8,128)(2,1)S(1)}, u32[]{:S(2)}, u32[]{:S(2)}) collective-permute-start(bf16[512,256]{1,0:T(8,128)(2,1)S(1)} %get-tuple-element.28.refs_5_), channel_id=1, source_target_pairs={{0,16},{16,32},{32,48},{48,64},{64,80},{80,96},{96,112},{112,128},... | collective-permute-start | bytes 786440 | tf_op jit(solution)/shard_map/ppermute | solution.py:376
  40.7 1.1 shard_map.73.refs_3_
  41.8 3.3 %shard_map.77 = (bf16[512,128]{1,0:T(8,128)(2,1)S(1)}, f32[512,128]{1,0:T(8,128)S(1)}, f32[512,128]{1,0:T(8,128)S(1)}, f32[512,128]{1,0:T(8,128)S(1)}, f32[2,128,128]{2,1,0:T(8,128)S(1)}) custom-call(bf16[2,512,128]{2,1,0:T(8,128)(2,1)S(1)} %bitcast.13, bf16[7,512,128]{2,1,0:T(8,128)(2,1)S(1)} %constant_dynamic-update-slice_fusion.received.refs_1_, ...), custom_call_target="tpu_custom_call" | custom-call | flops 2000000000 | bytes 3149840 | tf_op jit(solution)/shard_map/pallas_call | solution.py:342
  45.1 0.0 copy-start
  45.1 5.5 %collective-permute-done.5.kv = bf16[512,256]{1,0:T(8,128)(2,1)S(1)} collective-permute-done((bf16[512,256]{1,0:T(8,128)(2,1)S(1)}, bf16[512,256]{1,0:T(8,128)(2,1)S(1)}, u32[]{:S(2)}, u32[]{:S(2)}) %collective-permute-start.5) | collective-permute-done | bytes 262176 | tf_op jit(solution)/shard_map/ppermute | solution.py:376
  50.6 1.6 shard_map.78
  52.2 2.5 %all-gather.1 = bf16[1024,128]{1,0:T(8,128)(2,1)S(1)} all-gather(bf16[512,128]{1,0:T(8,128)(2,1)S(1)} %shard_map.78), channel_id=3, replica_groups=mesh['sp'=32,'y'=8,'c'=2] {'c'}, dimensions={0}, use_global_device_ids=true | all-gather | bytes 393216 | tf_op jit(solution)/shard_map/all_gather | solution.py:42
  54.7 2.7 %collective-permute-start.7 = (bf16[2,512,128]{2,1,0:T(8,128)(2,1)S(1)}, bf16[2,512,128]{2,1,0:T(8,128)(2,1)S(1)}, u32[]{:S(2)}, u32[]{:S(2)}) collective-permute-start(bf16[2,512,128]{2,1,0:T(8,128)(2,1)S(1)} %bitcast.7), channel_id=1, source_target_pairs={{0,4},{1,13},{2,6},{3,15},{4,8},{5,1},{6,10},{7,3},{8,12},{9,5},{1... | collective-permute-start | bytes 786440 | tf_op jit(solution)/shard_map/ppermute | solution.py:43
  57.3 6.3 %collective-permute-start.6 = (bf16[2,512,128]{2,1,0:T(8,128)(2,1)S(1)}, bf16[2,512,128]{2,1,0:T(8,128)(2,1)S(1)}, u32[]{:S(2)}, u32[]{:S(2)}) collective-permute-start(bf16[2,512,128]{2,1,0:T(8,128)(2,1)S(1)} %bitcast.8), channel_id=1, source_target_pairs={{0,2},{1,15},{2,4},{3,1},{4,6},{5,3},{6,8},{7,5},{8,10},{9,7},{10,... | collective-permute-start | bytes 786440 | tf_op jit(solution)/shard_map/ppermute | solution.py:44
  63.6 1.9 %collective-permute-start.11 = (bf16[2,2048,128]{2,1,0:T(8,128)(2,1)S(1)}, bf16[2,2048,128]{2,1,0:T(8,128)(2,1)S(1)}, u32[]{:S(2)}, u32[]{:S(2)}) collective-permute-start(bf16[2,2048,128]{2,1,0:T(8,128)(2,1)S(1)} %copy-done), channel_id=1, source_target_pairs={{0,1},{1,0},{2,3},{3,2},{4,5},{5,4},{6,7},{7,6},{8,9},{9,8},{10,11... | collective-permute-start | bytes 3145736 | tf_op jit(solution)/shard_map/ppermute | solution.py:386
  65.6 4.0 %collective-permute-start.8 = (bf16[2,512,128]{2,1,0:T(8,128)(2,1)S(1)}, bf16[2,512,128]{2,1,0:T(8,128)(2,1)S(1)}, u32[]{:S(2)}, u32[]{:S(2)}) collective-permute-start(bf16[2,512,128]{2,1,0:T(8,128)(2,1)S(1)} %collective-permute-done.7), channel_id=1, source_target_pairs={{0,2},{1,15},{2,4},{3,1},{4,6},{5,3},{6,8},{7,5},{8,10},{9,7},{10,... | collective-permute-start | bytes 786440 | tf_op jit(solution)/shard_map/ppermute | solution.py:46
  69.6 3.6 %collective-permute-start.9 = (bf16[1,512,128]{2,1,0:T(8,128)(2,1)S(1)}, bf16[1,512,128]{2,1,0:T(8,128)(2,1)S(1)}, u32[]{:S(2)}, u32[]{:S(2)}) collective-permute-start(bf16[1,512,128]{2,1,0:T(8,128)(2,1)S(1)} %constant_dynamic-slice_fusion.3), channel_id=1, source_target_pairs={{0,4},{1,13},{2,6},{3,15},{4,8},{5,1},{6,10},{7,3},{8,12},{9,5},{1... | collective-permute-start | bytes 393224 | tf_op jit(solution)/shard_map/ppermute | solution.py:47
  73.3 4.2 %collective-permute-done.9 = bf16[1,512,128]{2,1,0:T(8,128)(2,1)S(1)} collective-permute-done((bf16[1,512,128]{2,1,0:T(8,128)(2,1)S(1)}, bf16[1,512,128]{2,1,0:T(8,128)(2,1)S(1)}, u32[]{:S(2)}, u32[]{:S(2)}) %collective-permute-start.9) | collective-permute-done | bytes 131104 | tf_op jit(solution)/shard_map/ppermute | solution.py:47
  77.6 5.9 %collective-permute-start.10 = (bf16[7,512,128]{2,1,0:T(8,128)(2,1)S(1)}, bf16[7,512,128]{2,1,0:T(8,128)(2,1)S(1)}, u32[]{:S(2)}, u32[]{:S(2)}) collective-permute-start(bf16[7,512,128]{2,1,0:T(8,128)(2,1)S(1)} %constant_dynamic-update-slice_fusion.4.received), channel_id=1, source_target_pairs={{0,1},{1,0},{2,3},{3,2},{4,5},{5,4},{6,7},{7,6},{8,9},{9,8},{10,11... | collective-permute-start | bytes 2752520 | tf_op jit(solution)/shard_map/ppermute | solution.py:49
  83.5 0.5 shard_map.79.acc
  84.0 0.0 copy-start.2
  84.0 0.0 copy-start.3
  84.0 1.5 collective-permute-done.10.other
  85.5 0.4 shard_map.80.own.b_own
  86.0 3.8 %collective-permute-start.13 = (bf16[2,512,128]{2,1,0:T(8,128)(2,1)S(1)}, bf16[2,512,128]{2,1,0:T(8,128)(2,1)S(1)}, u32[]{:S(2)}, u32[]{:S(2)}) collective-permute-start(bf16[2,512,128]{2,1,0:T(8,128)(2,1)S(1)} %shard_map.80.own.b_own), channel_id=1, source_target_pairs={{0,4},{1,13},{2,6},{3,15},{4,8},{5,1},{6,10},{7,3},{8,12},{9,5},{1... | collective-permute-start | bytes 786440 | tf_op jit(solution)/shard_map/ppermute | solution.py:43
  89.8 2.1 %collective-permute-start.12 = (bf16[2,512,128]{2,1,0:T(8,128)(2,1)S(1)}, bf16[2,512,128]{2,1,0:T(8,128)(2,1)S(1)}, u32[]{:S(2)}, u32[]{:S(2)}) collective-permute-start(bf16[2,512,128]{2,1,0:T(8,128)(2,1)S(1)} %shard_map.80.own.b_own), channel_id=1, source_target_pairs={{0,2},{1,15},{2,4},{3,1},{4,6},{5,3},{6,8},{7,5},{8,10},{9,7},{10,... | collective-permute-start | bytes 786440 | tf_op jit(solution)/shard_map/ppermute | solution.py:44
  91.9 4.1 %collective-permute-done.13 = bf16[2,512,128]{2,1,0:T(8,128)(2,1)S(1)} collective-permute-done((bf16[2,512,128]{2,1,0:T(8,128)(2,1)S(1)}, bf16[2,512,128]{2,1,0:T(8,128)(2,1)S(1)}, u32[]{:S(2)}, u32[]{:S(2)}) %collective-permute-start.13) | collective-permute-done | bytes 262176 | tf_op jit(solution)/shard_map/ppermute | solution.py:43
  96.0 4.8 %collective-permute-start.14 = (bf16[2,512,128]{2,1,0:T(8,128)(2,1)S(1)}, bf16[2,512,128]{2,1,0:T(8,128)(2,1)S(1)}, u32[]{:S(2)}, u32[]{:S(2)}) collective-permute-start(bf16[2,512,128]{2,1,0:T(8,128)(2,1)S(1)} %collective-permute-done.13), channel_id=1, source_target_pairs={{0,2},{1,15},{2,4},{3,1},{4,6},{5,3},{6,8},{7,5},{8,10},{9,7},{10,... | collective-permute-start | bytes 786440 | tf_op jit(solution)/shard_map/ppermute | solution.py:46
  100.8 2.2 %collective-permute-start.15 = (bf16[1,512,128]{2,1,0:T(8,128)(2,1)S(1)}, bf16[1,512,128]{2,1,0:T(8,128)(2,1)S(1)}, u32[]{:S(2)}, u32[]{:S(2)}) collective-permute-start(bf16[1,512,128]{2,1,0:T(8,128)(2,1)S(1)} %constant_dynamic-slice_fusion.2), channel_id=1, source_target_pairs={{0,4},{1,13},{2,6},{3,15},{4,8},{5,1},{6,10},{7,3},{8,12},{9,5},{1... | collective-permute-start | bytes 393224 | tf_op jit(solution)/shard_map/ppermute | solution.py:47
  103.1 1.0 collective-permute-done.14
  104.1 4.6 %collective-permute-done.15 = bf16[1,512,128]{2,1,0:T(8,128)(2,1)S(1)} collective-permute-done((bf16[1,512,128]{2,1,0:T(8,128)(2,1)S(1)}, bf16[1,512,128]{2,1,0:T(8,128)(2,1)S(1)}, u32[]{:S(2)}, u32[]{:S(2)}) %collective-permute-start.15) | collective-permute-done | bytes 131104 | tf_op jit(solution)/shard_map/ppermute | solution.py:47
  108.8 3.1 %collective-permute-start.16 = (bf16[7,512,128]{2,1,0:T(8,128)(2,1)S(1)}, bf16[7,512,128]{2,1,0:T(8,128)(2,1)S(1)}, u32[]{:S(2)}, u32[]{:S(2)}) collective-permute-start(bf16[7,512,128]{2,1,0:T(8,128)(2,1)S(1)} %constant_dynamic-update-slice_fusion.8.received.b_received), channel_id=1, source_target_pairs={{0,1},{1,0},{2,3},{3,2},{4,5},{5,4},{6,7},{7,6},{8,9},{9,8},{10,11... | collective-permute-start | bytes 2752520 | tf_op jit(solution)/shard_map/ppermute | solution.py:49
  111.9 1.8 %shard_map.82.w = bf16[16,128,256]{2,1,0:T(8,128)(2,1)S(1)} custom-call(s32[1]{0:T(128)} %bitcast.place, f32[2,2,2048]{2,1,0:T(2,128)S(1)} %copy-done.1, bf16[2,2048,128]{2,1,0:T(8,128)(2,1)S(1)} %copy-done.2, bf16[2,2048,128]{2,1,0:T(8,128)(2,1)S(1)} %copy-done.3), custom_call_target="tpu_custom_call" | custom-call | flops 1000000000 | bytes 2129924 | tf_op jit(solution)/shard_map/pallas_call | solution.py:342
  113.7 0.1 shard_map.81.b_total
  113.9 0.1 collective-permute-done.16.b_other
  114.0 3.0 %shard_map.83 = (bf16[512,256]{1,0:T(8,128)(2,1)S(1)}, f32[512,128]{1,0:T(8,128)S(1)}, bf16[16,512,128]{2,1,0:T(8,128)(2,1)S(1)}, bf16[512,128]{1,0:T(8,128)(2,1)S(1)}) custom-call(s32[1]{0:T(128)} %bitcast.place, bf16[2,512,128]{2,1,0:T(8,128)(2,1)S(1)} %bitcast.14, bf16[7,512,128]{2,1,0:T(8,128)(2,1)S(1)} %constant_dynamic-update-slice_fusion.received.refs_1_, ...), custom_call_target="tpu_custom_call" | custom-call | flops 2000000000 | bytes 5537796 | tf_op jit(solution)/shard_map/pallas_call | solution.py:342
  117.0 2.1 %collective-permute-start.17 = (bf16[512,256]{1,0:T(8,128)(2,1)S(1)}, bf16[512,256]{1,0:T(8,128)(2,1)S(1)}, u32[]{:S(2)}, u32[]{:S(2)}) collective-permute-start(bf16[512,256]{1,0:T(8,128)(2,1)S(1)} %get-tuple-element.36.refs_3_), channel_id=1, source_target_pairs={{0,16},{16,32},{32,48},{48,64},{64,80},{80,96},{96,112},{112,128},... | collective-permute-start | bytes 786440 | tf_op jit(solution)/shard_map/ppermute | solution.py:376
  119.1 1.1 shard_map.84.refs_1_
  120.2 3.3 %shard_map.85 = (bf16[512,128]{1,0:T(8,128)(2,1)S(1)}, f32[512,128]{1,0:T(8,128)S(1)}, f32[512,128]{1,0:T(8,128)S(1)}, f32[512,128]{1,0:T(8,128)S(1)}, f32[2,128,128]{2,1,0:T(8,128)S(1)}) custom-call(bf16[16,512,128]{2,1,0:T(8,128)(2,1)S(1)} %get-tuple-element.34.refs_0_, bf16[16,128,128]{2,1,0:T(8,128)(2,1)S(1)} %shard_map.84.refs_1_, ...), custom_call_target="tpu_custom_call" | custom-call | flops 2000000000 | bytes 3149840 | tf_op jit(solution)/shard_map/pallas_call | solution.py:342
  123.6 6.2 %collective-permute-done.17.kv = bf16[512,256]{1,0:T(8,128)(2,1)S(1)} collective-permute-done((bf16[512,256]{1,0:T(8,128)(2,1)S(1)}, bf16[512,256]{1,0:T(8,128)(2,1)S(1)}, u32[]{:S(2)}, u32[]{:S(2)}) %collective-permute-start.17) | collective-permute-done | bytes 262176 | tf_op jit(solution)/shard_map/ppermute | solution.py:376
  129.7 1.5 shard_map.86
  131.3 2.9 %all-gather.2 = bf16[1024,128]{1,0:T(8,128)(2,1)S(1)} all-gather(bf16[512,128]{1,0:T(8,128)(2,1)S(1)} %shard_map.86), channel_id=4, replica_groups=mesh['sp'=32,'y'=8,'c'=2] {'c'}, dimensions={0}, use_global_device_ids=true | all-gather | bytes 393216 | tf_op jit(solution)/shard_map/all_gather | solution.py:42
  134.1 3.2 %collective-permute-start.19 = (bf16[2,512,128]{2,1,0:T(8,128)(2,1)S(1)}, bf16[2,512,128]{2,1,0:T(8,128)(2,1)S(1)}, u32[]{:S(2)}, u32[]{:S(2)}) collective-permute-start(bf16[2,512,128]{2,1,0:T(8,128)(2,1)S(1)} %bitcast.15), channel_id=1, source_target_pairs={{0,4},{1,13},{2,6},{3,15},{4,8},{5,1},{6,10},{7,3},{8,12},{9,5},{1... | collective-permute-start | bytes 786440 | tf_op jit(solution)/shard_map/ppermute | solution.py:43
  137.4 5.7 %collective-permute-start.18 = (bf16[2,512,128]{2,1,0:T(8,128)(2,1)S(1)}, bf16[2,512,128]{2,1,0:T(8,128)(2,1)S(1)}, u32[]{:S(2)}, u32[]{:S(2)}) collective-permute-start(bf16[2,512,128]{2,1,0:T(8,128)(2,1)S(1)} %bitcast.16), channel_id=1, source_target_pairs={{0,2},{1,15},{2,4},{3,1},{4,6},{5,3},{6,8},{7,5},{8,10},{9,7},{10,... | collective-permute-start | bytes 786440 | tf_op jit(solution)/shard_map/ppermute | solution.py:44
  143.1 6.2 %collective-permute-start.20 = (bf16[2,512,128]{2,1,0:T(8,128)(2,1)S(1)}, bf16[2,512,128]{2,1,0:T(8,128)(2,1)S(1)}, u32[]{:S(2)}, u32[]{:S(2)}) collective-permute-start(bf16[2,512,128]{2,1,0:T(8,128)(2,1)S(1)} %collective-permute-done.19), channel_id=1, source_target_pairs={{0,2},{1,15},{2,4},{3,1},{4,6},{5,3},{6,8},{7,5},{8,10},{9,7},{10,... | collective-permute-start | bytes 786440 | tf_op jit(solution)/shard_map/ppermute | solution.py:46
  149.3 3.5 %collective-permute-start.21 = (bf16[1,512,128]{2,1,0:T(8,128)(2,1)S(1)}, bf16[1,512,128]{2,1,0:T(8,128)(2,1)S(1)}, u32[]{:S(2)}, u32[]{:S(2)}) collective-permute-start(bf16[1,512,128]{2,1,0:T(8,128)(2,1)S(1)} %constant_dynamic-slice_fusion.1), channel_id=1, source_target_pairs={{0,4},{1,13},{2,6},{3,15},{4,8},{5,1},{6,10},{7,3},{8,12},{9,5},{1... | collective-permute-start | bytes 393224 | tf_op jit(solution)/shard_map/ppermute | solution.py:47
  153.0 4.0 %collective-permute-done.21 = bf16[1,512,128]{2,1,0:T(8,128)(2,1)S(1)} collective-permute-done((bf16[1,512,128]{2,1,0:T(8,128)(2,1)S(1)}, bf16[1,512,128]{2,1,0:T(8,128)(2,1)S(1)}, u32[]{:S(2)}, u32[]{:S(2)}) %collective-permute-start.21) | collective-permute-done | bytes 131104 | tf_op jit(solution)/shard_map/ppermute | solution.py:47
  157.1 5.8 %collective-permute-start.22 = (bf16[7,512,128]{2,1,0:T(8,128)(2,1)S(1)}, bf16[7,512,128]{2,1,0:T(8,128)(2,1)S(1)}, u32[]{:S(2)}, u32[]{:S(2)}) collective-permute-start(bf16[7,512,128]{2,1,0:T(8,128)(2,1)S(1)} %constant_dynamic-update-slice_fusion.12.received), channel_id=1, source_target_pairs={{0,1},{1,0},{2,3},{3,2},{4,5},{5,4},{6,7},{7,6},{8,9},{9,8},{10,11... | collective-permute-start | bytes 2752520 | tf_op jit(solution)/shard_map/ppermute | solution.py:49
  162.9 2.1 %collective-permute-done.22.other = bf16[7,512,128]{2,1,0:T(8,128)(2,1)S(1)} collective-permute-done((bf16[7,512,128]{2,1,0:T(8,128)(2,1)S(1)}, bf16[7,512,128]{2,1,0:T(8,128)(2,1)S(1)}, u32[]{:S(2)}, u32[]{:S(2)}) %collective-permute-start.22) | collective-permute-done | bytes 917536 | tf_op jit(solution)/shard_map/ppermute | solution.py:49
  164.9 1.4 shard_map.87
  166.4 6.2 %all-to-all-start = ((f32[16,4,128]{2,1,0:T(4,128)}), f32[16,4,128]{2,1,0:T(4,128)S(1)}, u32[]{:S(2)}, u32[]{:S(2)}) async-start(f32[16,4,128]{2,1,0:T(4,128)} %get-tuple-element.42), calls=%async_computation | async-start | bytes 65536 | tf_op jit(solution)/shard_map/all_to_all | solution.py:426
  172.6 7.4 %all-to-all-done.squares = f32[16,4,128]{2,1,0:T(4,128)S(1)} async-done(((f32[16,4,128]{2,1,0:T(4,128)}), f32[16,4,128]{2,1,0:T(4,128)S(1)}, u32[]{:S(2)}, u32[]{:S(2)}) %all-to-all-start) | async-done | bytes 32800 | tf_op jit(solution)/shard_map/all_to_all | solution.py:426
  180.0 0.8 shard_map.88
  (39 shorter events, 0.6 us)
Async XLA Ops:
  2.5 12.0 %collective-permute-start.1 = (bf16[2,512,128]{2,1,0:T(8,128)(2,1)S(1)}, bf16[2,512,128]{2,1,0:T(8,128)(2,1)S(1)}, u32[]{:S(2)}, u32[]{:S(2)}) collective-permute-start(bf16[2,512,128]{2,1,0:T(8,128)(2,1)S(1)} %bitcast.10), channel_id=1, source_target_pairs={{0,4},{1,13},{2,6},{3,15},{4,8},{5,1},{6,10},{7,3},{8,12},{9,5},{1... | collective-permute-start | bytes 786440 | tf_op jit(solution)/shard_map/ppermute | solution.py:43
  8.4 14.1 %collective-permute-start = (bf16[2,512,128]{2,1,0:T(8,128)(2,1)S(1)}, bf16[2,512,128]{2,1,0:T(8,128)(2,1)S(1)}, u32[]{:S(2)}, u32[]{:S(2)}) collective-permute-start(bf16[2,512,128]{2,1,0:T(8,128)(2,1)S(1)} %bitcast.11), channel_id=1, source_target_pairs={{0,2},{1,15},{2,4},{3,1},{4,6},{5,3},{6,8},{7,5},{8,10},{9,7},{10,... | collective-permute-start | bytes 786440 | tf_op jit(solution)/shard_map/ppermute | solution.py:44
  14.5 8.1 %collective-permute-start.2 = (bf16[2,512,128]{2,1,0:T(8,128)(2,1)S(1)}, bf16[2,512,128]{2,1,0:T(8,128)(2,1)S(1)}, u32[]{:S(2)}, u32[]{:S(2)}) collective-permute-start(bf16[2,512,128]{2,1,0:T(8,128)(2,1)S(1)} %collective-permute-done.1), channel_id=1, source_target_pairs={{0,2},{1,15},{2,4},{3,1},{4,6},{5,3},{6,8},{7,5},{8,10},{9,7},{10,... | collective-permute-start | bytes 786440 | tf_op jit(solution)/shard_map/ppermute | solution.py:46
  18.6 7.9 %collective-permute-start.3 = (bf16[1,512,128]{2,1,0:T(8,128)(2,1)S(1)}, bf16[1,512,128]{2,1,0:T(8,128)(2,1)S(1)}, u32[]{:S(2)}, u32[]{:S(2)}) collective-permute-start(bf16[1,512,128]{2,1,0:T(8,128)(2,1)S(1)} %constant_dynamic-slice_fusion.4), channel_id=1, source_target_pairs={{0,4},{1,13},{2,6},{3,15},{4,8},{5,1},{6,10},{7,3},{8,12},{9,5},{1... | collective-permute-start | bytes 393224 | tf_op jit(solution)/shard_map/ppermute | solution.py:47
  26.5 9.7 %collective-permute-start.4 = (bf16[7,512,128]{2,1,0:T(8,128)(2,1)S(1)}, bf16[7,512,128]{2,1,0:T(8,128)(2,1)S(1)}, u32[]{:S(2)}, u32[]{:S(2)}) collective-permute-start(bf16[7,512,128]{2,1,0:T(8,128)(2,1)S(1)} %constant_dynamic-update-slice_fusion.received.refs_1_), channel_id=1, source_target_pairs={{0,1},{1,0},{2,3},{3,2},{4,5},{5,4},{6,7},{7,6},{8,9},{9,8},{10,11... | collective-permute-start | bytes 2752520 | tf_op jit(solution)/shard_map/ppermute | solution.py:49
  34.4 1.2 copy-start.6
  36.3 4.4 %copy-start.1 = (f32[2,2,2048]{2,1,0:T(2,128)S(1)}, f32[2,2,2048]{2,1,0:T(2,128)}, u32[]{:S(2)}) copy-start(f32[2,2,2048]{2,1,0:T(2,128)} %gain.9) | copy-start | bytes 98308
  36.3 4.4 %copy-start.4 = (bf16[2,2048,128]{2,1,0:T(8,128)(2,1)S(1)}, bf16[2,2048,128]{2,1,0:T(8,128)(2,1)}, u32[]{:S(2)}) copy-start(bf16[2,2048,128]{2,1,0:T(8,128)(2,1)} %refs_0_.7) | copy-start | bytes 3145732
  37.5 4.3 %copy-start.5 = (f32[2,2,257]{2,1,0:T(2,128)S(1)}, f32[2,2,257]{2,1,0:T(2,128)}, u32[]{:S(2)}) copy-start(f32[2,2,257]{2,1,0:T(2,128)} %bias.3) | copy-start | bytes 12340
  37.5 13.1 %collective-permute-start.5 = (bf16[512,256]{1,0:T(8,128)(2,1)S(1)}, bf16[512,256]{1,0:T(8,128)(2,1)S(1)}, u32[]{:S(2)}, u32[]{:S(2)}) collective-permute-start(bf16[512,256]{1,0:T(8,128)(2,1)S(1)} %get-tuple-element.28.refs_5_), channel_id=1, source_target_pairs={{0,16},{16,32},{32,48},{48,64},{64,80},{80,96},{96,112},{112,128},... | collective-permute-start | bytes 786440 | tf_op jit(solution)/shard_map/ppermute | solution.py:376
  45.1 18.5 %copy-start = (bf16[2,2048,128]{2,1,0:T(8,128)(2,1)S(1)}, bf16[2,2048,128]{2,1,0:T(8,128)(2,1)}, u32[]{:S(2)}) copy-start(bf16[2,2048,128]{2,1,0:T(8,128)(2,1)} %w.5) | copy-start | bytes 3145732
  54.7 10.9 %collective-permute-start.7 = (bf16[2,512,128]{2,1,0:T(8,128)(2,1)S(1)}, bf16[2,512,128]{2,1,0:T(8,128)(2,1)S(1)}, u32[]{:S(2)}, u32[]{:S(2)}) collective-permute-start(bf16[2,512,128]{2,1,0:T(8,128)(2,1)S(1)} %bitcast.7), channel_id=1, source_target_pairs={{0,4},{1,13},{2,6},{3,15},{4,8},{5,1},{6,10},{7,3},{8,12},{9,5},{1... | collective-permute-start | bytes 786440 | tf_op jit(solution)/shard_map/ppermute | solution.py:43
  57.3 15.9 %collective-permute-start.6 = (bf16[2,512,128]{2,1,0:T(8,128)(2,1)S(1)}, bf16[2,512,128]{2,1,0:T(8,128)(2,1)S(1)}, u32[]{:S(2)}, u32[]{:S(2)}) collective-permute-start(bf16[2,512,128]{2,1,0:T(8,128)(2,1)S(1)} %bitcast.8), channel_id=1, source_target_pairs={{0,2},{1,15},{2,4},{3,1},{4,6},{5,3},{6,8},{7,5},{8,10},{9,7},{10,... | collective-permute-start | bytes 786440 | tf_op jit(solution)/shard_map/ppermute | solution.py:44
  63.6 19.9 %collective-permute-start.11 = (bf16[2,2048,128]{2,1,0:T(8,128)(2,1)S(1)}, bf16[2,2048,128]{2,1,0:T(8,128)(2,1)S(1)}, u32[]{:S(2)}, u32[]{:S(2)}) collective-permute-start(bf16[2,2048,128]{2,1,0:T(8,128)(2,1)S(1)} %copy-done), channel_id=1, source_target_pairs={{0,1},{1,0},{2,3},{3,2},{4,5},{5,4},{6,7},{7,6},{8,9},{9,8},{10,11... | collective-permute-start | bytes 3145736 | tf_op jit(solution)/shard_map/ppermute | solution.py:386
  65.6 7.7 %collective-permute-start.8 = (bf16[2,512,128]{2,1,0:T(8,128)(2,1)S(1)}, bf16[2,512,128]{2,1,0:T(8,128)(2,1)S(1)}, u32[]{:S(2)}, u32[]{:S(2)}) collective-permute-start(bf16[2,512,128]{2,1,0:T(8,128)(2,1)S(1)} %collective-permute-done.7), channel_id=1, source_target_pairs={{0,2},{1,15},{2,4},{3,1},{4,6},{5,3},{6,8},{7,5},{8,10},{9,7},{10,... | collective-permute-start | bytes 786440 | tf_op jit(solution)/shard_map/ppermute | solution.py:46
  69.6 8.0 %collective-permute-start.9 = (bf16[1,512,128]{2,1,0:T(8,128)(2,1)S(1)}, bf16[1,512,128]{2,1,0:T(8,128)(2,1)S(1)}, u32[]{:S(2)}, u32[]{:S(2)}) collective-permute-start(bf16[1,512,128]{2,1,0:T(8,128)(2,1)S(1)} %constant_dynamic-slice_fusion.3), channel_id=1, source_target_pairs={{0,4},{1,13},{2,6},{3,15},{4,8},{5,1},{6,10},{7,3},{8,12},{9,5},{1... | collective-permute-start | bytes 393224 | tf_op jit(solution)/shard_map/ppermute | solution.py:47
  77.6 7.9 %collective-permute-start.10 = (bf16[7,512,128]{2,1,0:T(8,128)(2,1)S(1)}, bf16[7,512,128]{2,1,0:T(8,128)(2,1)S(1)}, u32[]{:S(2)}, u32[]{:S(2)}) collective-permute-start(bf16[7,512,128]{2,1,0:T(8,128)(2,1)S(1)} %constant_dynamic-update-slice_fusion.4.received), channel_id=1, source_target_pairs={{0,1},{1,0},{2,3},{3,2},{4,5},{5,4},{6,7},{7,6},{8,9},{9,8},{10,11... | collective-permute-start | bytes 2752520 | tf_op jit(solution)/shard_map/ppermute | solution.py:49
  84.0 27.9 %copy-start.2 = (bf16[2,2048,128]{2,1,0:T(8,128)(2,1)S(1)}, bf16[2,2048,128]{2,1,0:T(8,128)(2,1)}, u32[]{:S(2)}) copy-start(bf16[2,2048,128]{2,1,0:T(8,128)(2,1)} %refs_0_.6) | copy-start | bytes 3145732
  84.0 27.9 %copy-start.3 = (bf16[2,2048,128]{2,1,0:T(8,128)(2,1)S(1)}, bf16[2,2048,128]{2,1,0:T(8,128)(2,1)}, u32[]{:S(2)}) copy-start(bf16[2,2048,128]{2,1,0:T(8,128)(2,1)} %refs_1_.3) | copy-start | bytes 3145732
  86.0 10.0 %collective-permute-start.13 = (bf16[2,512,128]{2,1,0:T(8,128)(2,1)S(1)}, bf16[2,512,128]{2,1,0:T(8,128)(2,1)S(1)}, u32[]{:S(2)}, u32[]{:S(2)}) collective-permute-start(bf16[2,512,128]{2,1,0:T(8,128)(2,1)S(1)} %shard_map.80.own.b_own), channel_id=1, source_target_pairs={{0,4},{1,13},{2,6},{3,15},{4,8},{5,1},{6,10},{7,3},{8,12},{9,5},{1... | collective-permute-start | bytes 786440 | tf_op jit(solution)/shard_map/ppermute | solution.py:43
  89.8 13.2 %collective-permute-start.12 = (bf16[2,512,128]{2,1,0:T(8,128)(2,1)S(1)}, bf16[2,512,128]{2,1,0:T(8,128)(2,1)S(1)}, u32[]{:S(2)}, u32[]{:S(2)}) collective-permute-start(bf16[2,512,128]{2,1,0:T(8,128)(2,1)S(1)} %shard_map.80.own.b_own), channel_id=1, source_target_pairs={{0,2},{1,15},{2,4},{3,1},{4,6},{5,3},{6,8},{7,5},{8,10},{9,7},{10,... | collective-permute-start | bytes 786440 | tf_op jit(solution)/shard_map/ppermute | solution.py:44
  96.0 8.1 %collective-permute-start.14 = (bf16[2,512,128]{2,1,0:T(8,128)(2,1)S(1)}, bf16[2,512,128]{2,1,0:T(8,128)(2,1)S(1)}, u32[]{:S(2)}, u32[]{:S(2)}) collective-permute-start(bf16[2,512,128]{2,1,0:T(8,128)(2,1)S(1)} %collective-permute-done.13), channel_id=1, source_target_pairs={{0,2},{1,15},{2,4},{3,1},{4,6},{5,3},{6,8},{7,5},{8,10},{9,7},{10,... | collective-permute-start | bytes 786440 | tf_op jit(solution)/shard_map/ppermute | solution.py:46
  100.8 7.9 %collective-permute-start.15 = (bf16[1,512,128]{2,1,0:T(8,128)(2,1)S(1)}, bf16[1,512,128]{2,1,0:T(8,128)(2,1)S(1)}, u32[]{:S(2)}, u32[]{:S(2)}) collective-permute-start(bf16[1,512,128]{2,1,0:T(8,128)(2,1)S(1)} %constant_dynamic-slice_fusion.2), channel_id=1, source_target_pairs={{0,4},{1,13},{2,6},{3,15},{4,8},{5,1},{6,10},{7,3},{8,12},{9,5},{1... | collective-permute-start | bytes 393224 | tf_op jit(solution)/shard_map/ppermute | solution.py:47
  108.8 5.2 %collective-permute-start.16 = (bf16[7,512,128]{2,1,0:T(8,128)(2,1)S(1)}, bf16[7,512,128]{2,1,0:T(8,128)(2,1)S(1)}, u32[]{:S(2)}, u32[]{:S(2)}) collective-permute-start(bf16[7,512,128]{2,1,0:T(8,128)(2,1)S(1)} %constant_dynamic-update-slice_fusion.8.received.b_received), channel_id=1, source_target_pairs={{0,1},{1,0},{2,3},{3,2},{4,5},{5,4},{6,7},{7,6},{8,9},{9,8},{10,11... | collective-permute-start | bytes 2752520 | tf_op jit(solution)/shard_map/ppermute | solution.py:49
  117.0 12.7 %collective-permute-start.17 = (bf16[512,256]{1,0:T(8,128)(2,1)S(1)}, bf16[512,256]{1,0:T(8,128)(2,1)S(1)}, u32[]{:S(2)}, u32[]{:S(2)}) collective-permute-start(bf16[512,256]{1,0:T(8,128)(2,1)S(1)} %get-tuple-element.36.refs_3_), channel_id=1, source_target_pairs={{0,16},{16,32},{32,48},{48,64},{64,80},{80,96},{96,112},{112,128},... | collective-permute-start | bytes 786440 | tf_op jit(solution)/shard_map/ppermute | solution.py:376
  134.1 8.9 %collective-permute-start.19 = (bf16[2,512,128]{2,1,0:T(8,128)(2,1)S(1)}, bf16[2,512,128]{2,1,0:T(8,128)(2,1)S(1)}, u32[]{:S(2)}, u32[]{:S(2)}) collective-permute-start(bf16[2,512,128]{2,1,0:T(8,128)(2,1)S(1)} %bitcast.15), channel_id=1, source_target_pairs={{0,4},{1,13},{2,6},{3,15},{4,8},{5,1},{6,10},{7,3},{8,12},{9,5},{1... | collective-permute-start | bytes 786440 | tf_op jit(solution)/shard_map/ppermute | solution.py:43
  137.4 15.5 %collective-permute-start.18 = (bf16[2,512,128]{2,1,0:T(8,128)(2,1)S(1)}, bf16[2,512,128]{2,1,0:T(8,128)(2,1)S(1)}, u32[]{:S(2)}, u32[]{:S(2)}) collective-permute-start(bf16[2,512,128]{2,1,0:T(8,128)(2,1)S(1)} %bitcast.16), channel_id=1, source_target_pairs={{0,2},{1,15},{2,4},{3,1},{4,6},{5,3},{6,8},{7,5},{8,10},{9,7},{10,... | collective-permute-start | bytes 786440 | tf_op jit(solution)/shard_map/ppermute | solution.py:44
  143.1 9.9 %collective-permute-start.20 = (bf16[2,512,128]{2,1,0:T(8,128)(2,1)S(1)}, bf16[2,512,128]{2,1,0:T(8,128)(2,1)S(1)}, u32[]{:S(2)}, u32[]{:S(2)}) collective-permute-start(bf16[2,512,128]{2,1,0:T(8,128)(2,1)S(1)} %collective-permute-done.19), channel_id=1, source_target_pairs={{0,2},{1,15},{2,4},{3,1},{4,6},{5,3},{6,8},{7,5},{8,10},{9,7},{10,... | collective-permute-start | bytes 786440 | tf_op jit(solution)/shard_map/ppermute | solution.py:46
  149.3 7.7 %collective-permute-start.21 = (bf16[1,512,128]{2,1,0:T(8,128)(2,1)S(1)}, bf16[1,512,128]{2,1,0:T(8,128)(2,1)S(1)}, u32[]{:S(2)}, u32[]{:S(2)}) collective-permute-start(bf16[1,512,128]{2,1,0:T(8,128)(2,1)S(1)} %constant_dynamic-slice_fusion.1), channel_id=1, source_target_pairs={{0,4},{1,13},{2,6},{3,15},{4,8},{5,1},{6,10},{7,3},{8,12},{9,5},{1... | collective-permute-start | bytes 393224 | tf_op jit(solution)/shard_map/ppermute | solution.py:47
  157.1 7.9 %collective-permute-start.22 = (bf16[7,512,128]{2,1,0:T(8,128)(2,1)S(1)}, bf16[7,512,128]{2,1,0:T(8,128)(2,1)S(1)}, u32[]{:S(2)}, u32[]{:S(2)}) collective-permute-start(bf16[7,512,128]{2,1,0:T(8,128)(2,1)S(1)} %constant_dynamic-update-slice_fusion.12.received), channel_id=1, source_target_pairs={{0,1},{1,0},{2,3},{3,2},{4,5},{5,4},{6,7},{7,6},{8,9},{9,8},{10,11... | collective-permute-start | bytes 2752520 | tf_op jit(solution)/shard_map/ppermute | solution.py:49
  166.4 13.6 %all-to-all-start = ((f32[16,4,128]{2,1,0:T(4,128)}), f32[16,4,128]{2,1,0:T(4,128)S(1)}, u32[]{:S(2)}, u32[]{:S(2)}) async-start(f32[16,4,128]{2,1,0:T(4,128)} %get-tuple-element.42), calls=%async_computation | async-start | bytes 65536 | tf_op jit(solution)/shard_map/all_to_all | solution.py:426

commit v5 on v4

--- a/solution.py
+++ b/solution.py
@@ -15,7 +15,8 @@
 NB = 16
 EPS = 1e-06
 BIG = 60
-CUTS = 4
+CUTS = 8
+TILE = 128
 NEG = -1e30
 VMEM = pl.BlockSpec(memory_space=pltpu.VMEM)
 SMEM = pl.BlockSpec(memory_space=pltpu.SMEM)
@@ -121,11 +122,8 @@
 
 
 def tiled(count, body):
-    def tile(i, carry):
-        body(pl.ds(pl.multiple_of(i * 64, 64), 64))
-        return carry
-
-    lax.fori_loop(0, count // 64, tile, 0)
+    for i in range(count // TILE):
+        body(pl.ds(i * TILE, TILE))
 
 
 def wide_inverse(total):
@@ -175,7 +173,7 @@
             return ref[j, rows, :].astype(jnp.float32)
 
         inv_post = wide_inverse(b_total[rows, :] + row_squares((b_other,), rows))
-        total = jnp.zeros((64, BLK), jnp.float32)
+        total = jnp.zeros((TILE, BLK), jnp.float32)
         for k in range(NB):
             x = load(refs, k) + load(b_refs, k) * inv_post * gain_row(gain, 0, 1, ids[k])
             x = x.astype(jnp.bfloat16)

time: 182 us -> 180 us (0.989)
  transfers between devices with their start and end apart: 24 -> 24, of which waited for: 13 -> 12; matrix products, arithmetic and copies ran while one was open for 0% -> 0% of each run, Pallas kernels for 8% -> 9%
where the time goes in v5:
time: 180 us; the launch traced here: 179 us
  starting transfers between devices  97.3 us (54%)
  waiting for transfers between devices  47.6 us (26%)
  Pallas kernels  23.6 us (13%)
  blocking collectives  7.85 us (4%)
    pallas_call x16, Pallas kernels, call(): pl.pallas_call(kernel, out_shape=outs, in_specs=ins, out_specs=jax.tree.m...  23.6 us
    ppermute x4, starting transfers between devices, gather_blocks(): other = lax.ppermute(received, 'c', [(0, 1), (1, 0)])  19.1 us
    ppermute x4, starting transfers between devices, gather_blocks(): three = lax.ppermute(two, ('y', 'c'), core_pairs(1))  19 us
    ppermute x4, starting transfers between devices, gather_blocks(): one = lax.ppermute(own, ('y', 'c'), core_pairs(1))  17 us
    ppermute x4, waiting for transfers between devices, gather_blocks(): four = lax.ppermute(half, ('y', 'c'), core_pairs(2))  16.9 us
    ppermute x4, starting transfers between devices, gather_blocks(): two = lax.ppermute(own, ('y', 'c'), core_pairs(2))  15.6 us
    ppermute x4, starting transfers between devices, gather_blocks(): four = lax.ppermute(half, ('y', 'c'), core_pairs(2))  13.3 us
    ppermute x2, waiting for transfers between devices, attention(): previous = lax.ppermute(kv, 'sp', shift)  11.5 us
  transfers between devices with their start and end apart: 24, of which 12 were waited for; matrix products, arithmetic and copies ran while one was open for 0% of the time, Pallas kernels for 9%

profile of v5, /device:TPU:257, one launch (start us, length us, event | category | flops | bytes accessed | tf_op | source)
XLA Modules:
  0.0 178.8 jit_solution(18234927775088544002)
XLA Ops:
  0.0 2.5 %all-gather = bf16[1024,128]{1,0:T(8,128)(2,1)S(1)} all-gather(bf16[512,128]{1,0:T(8,128)(2,1)} %param.7), channel_id=2, replica_groups=mesh['sp'=32,'y'=8,'c'=2] {'c'}, dimensions={0}, use_global_device_ids=true | all-gather | bytes 393216 | tf_op jit(solution)/shard_map/all_gather | solution.py:43
  2.5 5.9 %collective-permute-start.1 = (bf16[2,512,128]{2,1,0:T(8,128)(2,1)S(1)}, bf16[2,512,128]{2,1,0:T(8,128)(2,1)S(1)}, u32[]{:S(2)}, u32[]{:S(2)}) collective-permute-start(bf16[2,512,128]{2,1,0:T(8,128)(2,1)S(1)} %bitcast.10), channel_id=1, source_target_pairs={{0,4},{1,13},{2,6},{3,15},{4,8},{5,1},{6,10},{7,3},{8,12},{9,5},{1... | collective-permute-start | bytes 786440 | tf_op jit(solution)/shard_map/ppermute | solution.py:44
  8.4 3.0 %collective-permute-start = (bf16[2,512,128]{2,1,0:T(8,128)(2,1)S(1)}, bf16[2,512,128]{2,1,0:T(8,128)(2,1)S(1)}, u32[]{:S(2)}, u32[]{:S(2)}) collective-permute-start(bf16[2,512,128]{2,1,0:T(8,128)(2,1)S(1)} %bitcast.11), channel_id=1, source_target_pairs={{0,2},{1,15},{2,4},{3,1},{4,6},{5,3},{6,8},{7,5},{8,10},{9,7},{10,... | collective-permute-start | bytes 786440 | tf_op jit(solution)/shard_map/ppermute | solution.py:45
  11.4 3.1 %collective-permute-done.1 = bf16[2,512,128]{2,1,0:T(8,128)(2,1)S(1)} collective-permute-done((bf16[2,512,128]{2,1,0:T(8,128)(2,1)S(1)}, bf16[2,512,128]{2,1,0:T(8,128)(2,1)S(1)}, u32[]{:S(2)}, u32[]{:S(2)}) %collective-permute-start.1) | collective-permute-done | bytes 262176 | tf_op jit(solution)/shard_map/ppermute | solution.py:44
  14.5 4.1 %collective-permute-start.2 = (bf16[2,512,128]{2,1,0:T(8,128)(2,1)S(1)}, bf16[2,512,128]{2,1,0:T(8,128)(2,1)S(1)}, u32[]{:S(2)}, u32[]{:S(2)}) collective-permute-start(bf16[2,512,128]{2,1,0:T(8,128)(2,1)S(1)} %collective-permute-done.1), channel_id=1, source_target_pairs={{0,2},{1,15},{2,4},{3,1},{4,6},{5,3},{6,8},{7,5},{8,10},{9,7},{10,... | collective-permute-start | bytes 786440 | tf_op jit(solution)/shard_map/ppermute | solution.py:47
  18.6 3.9 %collective-permute-start.3 = (bf16[1,512,128]{2,1,0:T(8,128)(2,1)S(1)}, bf16[1,512,128]{2,1,0:T(8,128)(2,1)S(1)}, u32[]{:S(2)}, u32[]{:S(2)}) collective-permute-start(bf16[1,512,128]{2,1,0:T(8,128)(2,1)S(1)} %constant_dynamic-slice_fusion.4), channel_id=1, source_target_pairs={{0,4},{1,13},{2,6},{3,15},{4,8},{5,1},{6,10},{7,3},{8,12},{9,5},{1... | collective-permute-start | bytes 393224 | tf_op jit(solution)/shard_map/ppermute | solution.py:48
  22.5 0.0 collective-permute-done
  22.5 0.0 collective-permute-done.2
  22.6 3.9 %collective-permute-done.3 = bf16[1,512,128]{2,1,0:T(8,128)(2,1)S(1)} collective-permute-done((bf16[1,512,128]{2,1,0:T(8,128)(2,1)S(1)}, bf16[1,512,128]{2,1,0:T(8,128)(2,1)S(1)}, u32[]{:S(2)}, u32[]{:S(2)}) %collective-permute-start.3) | collective-permute-done | bytes 131104 | tf_op jit(solution)/shard_map/ppermute | solution.py:48
  26.5 4.4 %collective-permute-start.4 = (bf16[7,512,128]{2,1,0:T(8,128)(2,1)S(1)}, bf16[7,512,128]{2,1,0:T(8,128)(2,1)S(1)}, u32[]{:S(2)}, u32[]{:S(2)}) collective-permute-start(bf16[7,512,128]{2,1,0:T(8,128)(2,1)S(1)} %constant_dynamic-update-slice_fusion.received.refs_1_), channel_id=1, source_target_pairs={{0,1},{1,0},{2,3},{3,2},{4,5},{5,4},{6,7},{7,6},{8,9},{9,8},{10,11... | collective-permute-start | bytes 2752520 | tf_op jit(solution)/shard_map/ppermute | solution.py:50
  31.0 3.4 %shard_map.74.w = bf16[16,128,256]{2,1,0:T(8,128)(2,1)} custom-call(s32[1]{0:T(128)} %bitcast.place, f32[2,2,2048]{2,1,0:T(2,128)} %gain.9, bf16[2,2048,128]{2,1,0:T(8,128)(2,1)} %refs_0_.6, bf16[2,2048,128]{2,1,0:T(8,128)(2,1)} %refs_1_.3), custom_call_target="tpu_custom_call" | custom-call | flops 1000000000 | bytes 2129924 | tf_op jit(solution)/shard_map/pallas_call | solution.py:340
  34.5 1.2 copy-done.6
  35.7 0.6 shard_map.75
  36.2 0.0 copy-start.1
  36.3 0.0 copy-start.4
  36.3 0.5 shard_map.76
  36.7 0.0 copy-start.5
  36.7 3.1 %collective-permute-start.5 = (bf16[512,256]{1,0:T(8,128)(2,1)S(1)}, bf16[512,256]{1,0:T(8,128)(2,1)S(1)}, u32[]{:S(2)}, u32[]{:S(2)}) collective-permute-start(bf16[512,256]{1,0:T(8,128)(2,1)S(1)} %get-tuple-element.28.refs_5_), channel_id=1, source_target_pairs={{0,16},{16,32},{32,48},{48,64},{64,80},{80,96},{96,112},{112,128},... | collective-permute-start | bytes 786440 | tf_op jit(solution)/shard_map/ppermute | solution.py:374
  39.9 1.1 shard_map.73.refs_3_
  41.0 3.3 %shard_map.77 = (bf16[512,128]{1,0:T(8,128)(2,1)S(1)}, f32[512,128]{1,0:T(8,128)S(1)}, f32[512,128]{1,0:T(8,128)S(1)}, f32[512,128]{1,0:T(8,128)S(1)}, f32[2,128,128]{2,1,0:T(8,128)S(1)}) custom-call(bf16[2,512,128]{2,1,0:T(8,128)(2,1)S(1)} %bitcast.13, bf16[7,512,128]{2,1,0:T(8,128)(2,1)S(1)} %constant_dynamic-update-slice_fusion.received.refs_1_, ...), custom_call_target="tpu_custom_call" | custom-call | flops 2000000000 | bytes 3149840 | tf_op jit(solution)/shard_map/pallas_call | solution.py:340
  44.4 0.0 copy-start
  44.4 5.4 %collective-permute-done.5.kv = bf16[512,256]{1,0:T(8,128)(2,1)S(1)} collective-permute-done((bf16[512,256]{1,0:T(8,128)(2,1)S(1)}, bf16[512,256]{1,0:T(8,128)(2,1)S(1)}, u32[]{:S(2)}, u32[]{:S(2)}) %collective-permute-start.5) | collective-permute-done | bytes 262176 | tf_op jit(solution)/shard_map/ppermute | solution.py:374
  49.8 1.5 shard_map.78
  51.4 2.5 %all-gather.1 = bf16[1024,128]{1,0:T(8,128)(2,1)S(1)} all-gather(bf16[512,128]{1,0:T(8,128)(2,1)S(1)} %shard_map.78), channel_id=3, replica_groups=mesh['sp'=32,'y'=8,'c'=2] {'c'}, dimensions={0}, use_global_device_ids=true | all-gather | bytes 393216 | tf_op jit(solution)/shard_map/all_gather | solution.py:43
  53.9 2.7 %collective-permute-start.7 = (bf16[2,512,128]{2,1,0:T(8,128)(2,1)S(1)}, bf16[2,512,128]{2,1,0:T(8,128)(2,1)S(1)}, u32[]{:S(2)}, u32[]{:S(2)}) collective-permute-start(bf16[2,512,128]{2,1,0:T(8,128)(2,1)S(1)} %bitcast.7), channel_id=1, source_target_pairs={{0,4},{1,13},{2,6},{3,15},{4,8},{5,1},{6,10},{7,3},{8,12},{9,5},{1... | collective-permute-start | bytes 786440 | tf_op jit(solution)/shard_map/ppermute | solution.py:44
  56.5 6.3 %collective-permute-start.6 = (bf16[2,512,128]{2,1,0:T(8,128)(2,1)S(1)}, bf16[2,512,128]{2,1,0:T(8,128)(2,1)S(1)}, u32[]{:S(2)}, u32[]{:S(2)}) collective-permute-start(bf16[2,512,128]{2,1,0:T(8,128)(2,1)S(1)} %bitcast.8), channel_id=1, source_target_pairs={{0,2},{1,15},{2,4},{3,1},{4,6},{5,3},{6,8},{7,5},{8,10},{9,7},{10,... | collective-permute-start | bytes 786440 | tf_op jit(solution)/shard_map/ppermute | solution.py:45
  62.8 1.9 %collective-permute-start.11 = (bf16[2,2048,128]{2,1,0:T(8,128)(2,1)S(1)}, bf16[2,2048,128]{2,1,0:T(8,128)(2,1)S(1)}, u32[]{:S(2)}, u32[]{:S(2)}) collective-permute-start(bf16[2,2048,128]{2,1,0:T(8,128)(2,1)S(1)} %copy-done), channel_id=1, source_target_pairs={{0,1},{1,0},{2,3},{3,2},{4,5},{5,4},{6,7},{7,6},{8,9},{9,8},{10,11... | collective-permute-start | bytes 3145736 | tf_op jit(solution)/shard_map/ppermute | solution.py:384
  64.8 4.0 %collective-permute-start.8 = (bf16[2,512,128]{2,1,0:T(8,128)(2,1)S(1)}, bf16[2,512,128]{2,1,0:T(8,128)(2,1)S(1)}, u32[]{:S(2)}, u32[]{:S(2)}) collective-permute-start(bf16[2,512,128]{2,1,0:T(8,128)(2,1)S(1)} %collective-permute-done.7), channel_id=1, source_target_pairs={{0,2},{1,15},{2,4},{3,1},{4,6},{5,3},{6,8},{7,5},{8,10},{9,7},{10,... | collective-permute-start | bytes 786440 | tf_op jit(solution)/shard_map/ppermute | solution.py:47
  68.8 3.6 %collective-permute-start.9 = (bf16[1,512,128]{2,1,0:T(8,128)(2,1)S(1)}, bf16[1,512,128]{2,1,0:T(8,128)(2,1)S(1)}, u32[]{:S(2)}, u32[]{:S(2)}) collective-permute-start(bf16[1,512,128]{2,1,0:T(8,128)(2,1)S(1)} %constant_dynamic-slice_fusion.3), channel_id=1, source_target_pairs={{0,4},{1,13},{2,6},{3,15},{4,8},{5,1},{6,10},{7,3},{8,12},{9,5},{1... | collective-permute-start | bytes 393224 | tf_op jit(solution)/shard_map/ppermute | solution.py:48
  72.5 4.2 %collective-permute-done.9 = bf16[1,512,128]{2,1,0:T(8,128)(2,1)S(1)} collective-permute-done((bf16[1,512,128]{2,1,0:T(8,128)(2,1)S(1)}, bf16[1,512,128]{2,1,0:T(8,128)(2,1)S(1)}, u32[]{:S(2)}, u32[]{:S(2)}) %collective-permute-start.9) | collective-permute-done | bytes 131104 | tf_op jit(solution)/shard_map/ppermute | solution.py:48
  76.8 5.8 %collective-permute-start.10 = (bf16[7,512,128]{2,1,0:T(8,128)(2,1)S(1)}, bf16[7,512,128]{2,1,0:T(8,128)(2,1)S(1)}, u32[]{:S(2)}, u32[]{:S(2)}) collective-permute-start(bf16[7,512,128]{2,1,0:T(8,128)(2,1)S(1)} %constant_dynamic-update-slice_fusion.4.received), channel_id=1, source_target_pairs={{0,1},{1,0},{2,3},{3,2},{4,5},{5,4},{6,7},{7,6},{8,9},{9,8},{10,11... | collective-permute-start | bytes 2752520 | tf_op jit(solution)/shard_map/ppermute | solution.py:50
  82.6 0.5 shard_map.79.acc
  83.2 0.0 copy-start.2
  83.2 0.0 copy-start.3
  83.2 1.5 collective-permute-done.10.other
  84.7 0.4 shard_map.80.own.b_own
  85.2 3.9 %collective-permute-start.13 = (bf16[2,512,128]{2,1,0:T(8,128)(2,1)S(1)}, bf16[2,512,128]{2,1,0:T(8,128)(2,1)S(1)}, u32[]{:S(2)}, u32[]{:S(2)}) collective-permute-start(bf16[2,512,128]{2,1,0:T(8,128)(2,1)S(1)} %shard_map.80.own.b_own), channel_id=1, source_target_pairs={{0,4},{1,13},{2,6},{3,15},{4,8},{5,1},{6,10},{7,3},{8,12},{9,5},{1... | collective-permute-start | bytes 786440 | tf_op jit(solution)/shard_map/ppermute | solution.py:44
  89.0 2.1 %collective-permute-start.12 = (bf16[2,512,128]{2,1,0:T(8,128)(2,1)S(1)}, bf16[2,512,128]{2,1,0:T(8,128)(2,1)S(1)}, u32[]{:S(2)}, u32[]{:S(2)}) collective-permute-start(bf16[2,512,128]{2,1,0:T(8,128)(2,1)S(1)} %shard_map.80.own.b_own), channel_id=1, source_target_pairs={{0,2},{1,15},{2,4},{3,1},{4,6},{5,3},{6,8},{7,5},{8,10},{9,7},{10,... | collective-permute-start | bytes 786440 | tf_op jit(solution)/shard_map/ppermute | solution.py:45
  91.1 4.1 %collective-permute-done.13 = bf16[2,512,128]{2,1,0:T(8,128)(2,1)S(1)} collective-permute-done((bf16[2,512,128]{2,1,0:T(8,128)(2,1)S(1)}, bf16[2,512,128]{2,1,0:T(8,128)(2,1)S(1)}, u32[]{:S(2)}, u32[]{:S(2)}) %collective-permute-start.13) | collective-permute-done | bytes 262176 | tf_op jit(solution)/shard_map/ppermute | solution.py:44
  95.3 4.7 %collective-permute-start.14 = (bf16[2,512,128]{2,1,0:T(8,128)(2,1)S(1)}, bf16[2,512,128]{2,1,0:T(8,128)(2,1)S(1)}, u32[]{:S(2)}, u32[]{:S(2)}) collective-permute-start(bf16[2,512,128]{2,1,0:T(8,128)(2,1)S(1)} %collective-permute-done.13), channel_id=1, source_target_pairs={{0,2},{1,15},{2,4},{3,1},{4,6},{5,3},{6,8},{7,5},{8,10},{9,7},{10,... | collective-permute-start | bytes 786440 | tf_op jit(solution)/shard_map/ppermute | solution.py:47
  100.0 2.2 %collective-permute-start.15 = (bf16[1,512,128]{2,1,0:T(8,128)(2,1)S(1)}, bf16[1,512,128]{2,1,0:T(8,128)(2,1)S(1)}, u32[]{:S(2)}, u32[]{:S(2)}) collective-permute-start(bf16[1,512,128]{2,1,0:T(8,128)(2,1)S(1)} %constant_dynamic-slice_fusion.2), channel_id=1, source_target_pairs={{0,4},{1,13},{2,6},{3,15},{4,8},{5,1},{6,10},{7,3},{8,12},{9,5},{1... | collective-permute-start | bytes 393224 | tf_op jit(solution)/shard_map/ppermute | solution.py:48
  102.4 0.9 collective-permute-done.14
  103.3 4.6 %collective-permute-done.15 = bf16[1,512,128]{2,1,0:T(8,128)(2,1)S(1)} collective-permute-done((bf16[1,512,128]{2,1,0:T(8,128)(2,1)S(1)}, bf16[1,512,128]{2,1,0:T(8,128)(2,1)S(1)}, u32[]{:S(2)}, u32[]{:S(2)}) %collective-permute-start.15) | collective-permute-done | bytes 131104 | tf_op jit(solution)/shard_map/ppermute | solution.py:48
  108.0 3.1 %collective-permute-start.16 = (bf16[7,512,128]{2,1,0:T(8,128)(2,1)S(1)}, bf16[7,512,128]{2,1,0:T(8,128)(2,1)S(1)}, u32[]{:S(2)}, u32[]{:S(2)}) collective-permute-start(bf16[7,512,128]{2,1,0:T(8,128)(2,1)S(1)} %constant_dynamic-update-slice_fusion.8.received.b_received), channel_id=1, source_target_pairs={{0,1},{1,0},{2,3},{3,2},{4,5},{5,4},{6,7},{7,6},{8,9},{9,8},{10,11... | collective-permute-start | bytes 2752520 | tf_op jit(solution)/shard_map/ppermute | solution.py:50
  111.1 1.9 %shard_map.82.w = bf16[16,128,256]{2,1,0:T(8,128)(2,1)S(1)} custom-call(s32[1]{0:T(128)} %bitcast.place, f32[2,2,2048]{2,1,0:T(2,128)S(1)} %copy-done.1, bf16[2,2048,128]{2,1,0:T(8,128)(2,1)S(1)} %copy-done.2, bf16[2,2048,128]{2,1,0:T(8,128)(2,1)S(1)} %copy-done.3), custom_call_target="tpu_custom_call" | custom-call | flops 1000000000 | bytes 2129924 | tf_op jit(solution)/shard_map/pallas_call | solution.py:340
  113.0 0.1 shard_map.81.b_total
  113.2 1.9 %shard_map.83 = (bf16[512,256]{1,0:T(8,128)(2,1)S(1)}, f32[512,128]{1,0:T(8,128)S(1)}, bf16[16,512,128]{2,1,0:T(8,128)(2,1)S(1)}, bf16[512,128]{1,0:T(8,128)(2,1)S(1)}) custom-call(s32[1]{0:T(128)} %bitcast.place, bf16[2,512,128]{2,1,0:T(8,128)(2,1)S(1)} %bitcast.14, bf16[7,512,128]{2,1,0:T(8,128)(2,1)S(1)} %constant_dynamic-update-slice_fusion.received.refs_1_, ...), custom_call_target="tpu_custom_call" | custom-call | flops 2000000000 | bytes 5537796 | tf_op jit(solution)/shard_map/pallas_call | solution.py:340
  115.1 2.1 %collective-permute-start.17 = (bf16[512,256]{1,0:T(8,128)(2,1)S(1)}, bf16[512,256]{1,0:T(8,128)(2,1)S(1)}, u32[]{:S(2)}, u32[]{:S(2)}) collective-permute-start(bf16[512,256]{1,0:T(8,128)(2,1)S(1)} %get-tuple-element.36.refs_3_), channel_id=1, source_target_pairs={{0,16},{16,32},{32,48},{48,64},{64,80},{80,96},{96,112},{112,128},... | collective-permute-start | bytes 786440 | tf_op jit(solution)/shard_map/ppermute | solution.py:374
  117.2 1.1 shard_map.84.refs_1_
  118.4 3.3 %shard_map.85 = (bf16[512,128]{1,0:T(8,128)(2,1)S(1)}, f32[512,128]{1,0:T(8,128)S(1)}, f32[512,128]{1,0:T(8,128)S(1)}, f32[512,128]{1,0:T(8,128)S(1)}, f32[2,128,128]{2,1,0:T(8,128)S(1)}) custom-call(bf16[16,512,128]{2,1,0:T(8,128)(2,1)S(1)} %get-tuple-element.34.refs_0_, bf16[16,128,128]{2,1,0:T(8,128)(2,1)S(1)} %shard_map.84.refs_1_, ...), custom_call_target="tpu_custom_call" | custom-call | flops 2000000000 | bytes 3149840 | tf_op jit(solution)/shard_map/pallas_call | solution.py:340
  121.7 6.1 %collective-permute-done.17.kv = bf16[512,256]{1,0:T(8,128)(2,1)S(1)} collective-permute-done((bf16[512,256]{1,0:T(8,128)(2,1)S(1)}, bf16[512,256]{1,0:T(8,128)(2,1)S(1)}, u32[]{:S(2)}, u32[]{:S(2)}) %collective-permute-start.17) | collective-permute-done | bytes 262176 | tf_op jit(solution)/shard_map/ppermute | solution.py:374
  127.8 1.5 shard_map.86
  129.4 2.8 %all-gather.2 = bf16[1024,128]{1,0:T(8,128)(2,1)S(1)} all-gather(bf16[512,128]{1,0:T(8,128)(2,1)S(1)} %shard_map.86), channel_id=4, replica_groups=mesh['sp'=32,'y'=8,'c'=2] {'c'}, dimensions={0}, use_global_device_ids=true | all-gather | bytes 393216 | tf_op jit(solution)/shard_map/all_gather | solution.py:43
  132.2 3.2 %collective-permute-start.19 = (bf16[2,512,128]{2,1,0:T(8,128)(2,1)S(1)}, bf16[2,512,128]{2,1,0:T(8,128)(2,1)S(1)}, u32[]{:S(2)}, u32[]{:S(2)}) collective-permute-start(bf16[2,512,128]{2,1,0:T(8,128)(2,1)S(1)} %bitcast.15), channel_id=1, source_target_pairs={{0,4},{1,13},{2,6},{3,15},{4,8},{5,1},{6,10},{7,3},{8,12},{9,5},{1... | collective-permute-start | bytes 786440 | tf_op jit(solution)/shard_map/ppermute | solution.py:44
  135.5 5.7 %collective-permute-start.18 = (bf16[2,512,128]{2,1,0:T(8,128)(2,1)S(1)}, bf16[2,512,128]{2,1,0:T(8,128)(2,1)S(1)}, u32[]{:S(2)}, u32[]{:S(2)}) collective-permute-start(bf16[2,512,128]{2,1,0:T(8,128)(2,1)S(1)} %bitcast.16), channel_id=1, source_target_pairs={{0,2},{1,15},{2,4},{3,1},{4,6},{5,3},{6,8},{7,5},{8,10},{9,7},{10,... | collective-permute-start | bytes 786440 | tf_op jit(solution)/shard_map/ppermute | solution.py:45
  141.2 6.2 %collective-permute-start.20 = (bf16[2,512,128]{2,1,0:T(8,128)(2,1)S(1)}, bf16[2,512,128]{2,1,0:T(8,128)(2,1)S(1)}, u32[]{:S(2)}, u32[]{:S(2)}) collective-permute-start(bf16[2,512,128]{2,1,0:T(8,128)(2,1)S(1)} %collective-permute-done.19), channel_id=1, source_target_pairs={{0,2},{1,15},{2,4},{3,1},{4,6},{5,3},{6,8},{7,5},{8,10},{9,7},{10,... | collective-permute-start | bytes 786440 | tf_op jit(solution)/shard_map/ppermute | solution.py:47
  147.4 3.5 %collective-permute-start.21 = (bf16[1,512,128]{2,1,0:T(8,128)(2,1)S(1)}, bf16[1,512,128]{2,1,0:T(8,128)(2,1)S(1)}, u32[]{:S(2)}, u32[]{:S(2)}) collective-permute-start(bf16[1,512,128]{2,1,0:T(8,128)(2,1)S(1)} %constant_dynamic-slice_fusion.1), channel_id=1, source_target_pairs={{0,4},{1,13},{2,6},{3,15},{4,8},{5,1},{6,10},{7,3},{8,12},{9,5},{1... | collective-permute-start | bytes 393224 | tf_op jit(solution)/shard_map/ppermute | solution.py:48
  151.1 4.1 %collective-permute-done.21 = bf16[1,512,128]{2,1,0:T(8,128)(2,1)S(1)} collective-permute-done((bf16[1,512,128]{2,1,0:T(8,128)(2,1)S(1)}, bf16[1,512,128]{2,1,0:T(8,128)(2,1)S(1)}, u32[]{:S(2)}, u32[]{:S(2)}) %collective-permute-start.21) | collective-permute-done | bytes 131104 | tf_op jit(solution)/shard_map/ppermute | solution.py:48
  155.2 5.8 %collective-permute-start.22 = (bf16[7,512,128]{2,1,0:T(8,128)(2,1)S(1)}, bf16[7,512,128]{2,1,0:T(8,128)(2,1)S(1)}, u32[]{:S(2)}, u32[]{:S(2)}) collective-permute-start(bf16[7,512,128]{2,1,0:T(8,128)(2,1)S(1)} %constant_dynamic-update-slice_fusion.12.received), channel_id=1, source_target_pairs={{0,1},{1,0},{2,3},{3,2},{4,5},{5,4},{6,7},{7,6},{8,9},{9,8},{10,11... | collective-permute-start | bytes 2752520 | tf_op jit(solution)/shard_map/ppermute | solution.py:50
  161.0 2.1 %collective-permute-done.22.other = bf16[7,512,128]{2,1,0:T(8,128)(2,1)S(1)} collective-permute-done((bf16[7,512,128]{2,1,0:T(8,128)(2,1)S(1)}, bf16[7,512,128]{2,1,0:T(8,128)(2,1)S(1)}, u32[]{:S(2)}, u32[]{:S(2)}) %collective-permute-start.22) | collective-permute-done | bytes 917536 | tf_op jit(solution)/shard_map/ppermute | solution.py:50
  163.1 1.4 shard_map.87
  164.5 6.2 %all-to-all-start = ((f32[16,4,128]{2,1,0:T(4,128)}), f32[16,4,128]{2,1,0:T(4,128)S(1)}, u32[]{:S(2)}, u32[]{:S(2)}) async-start(f32[16,4,128]{2,1,0:T(4,128)} %get-tuple-element.42), calls=%async_computation | async-start | bytes 65536 | tf_op jit(solution)/shard_map/all_to_all | solution.py:424
  170.6 7.4 %all-to-all-done.squares = f32[16,4,128]{2,1,0:T(4,128)S(1)} async-done(((f32[16,4,128]{2,1,0:T(4,128)}), f32[16,4,128]{2,1,0:T(4,128)S(1)}, u32[]{:S(2)}, u32[]{:S(2)}) %all-to-all-start) | async-done | bytes 32800 | tf_op jit(solution)/shard_map/all_to_all | solution.py:424
  178.0 0.8 shard_map.88
  (39 shorter events, 0.6 us)
Async XLA Ops:
  2.5 12.0 %collective-permute-start.1 = (bf16[2,512,128]{2,1,0:T(8,128)(2,1)S(1)}, bf16[2,512,128]{2,1,0:T(8,128)(2,1)S(1)}, u32[]{:S(2)}, u32[]{:S(2)}) collective-permute-start(bf16[2,512,128]{2,1,0:T(8,128)(2,1)S(1)} %bitcast.10), channel_id=1, source_target_pairs={{0,4},{1,13},{2,6},{3,15},{4,8},{5,1},{6,10},{7,3},{8,12},{9,5},{1... | collective-permute-start | bytes 786440 | tf_op jit(solution)/shard_map/ppermute | solution.py:44
  8.4 14.1 %collective-permute-start = (bf16[2,512,128]{2,1,0:T(8,128)(2,1)S(1)}, bf16[2,512,128]{2,1,0:T(8,128)(2,1)S(1)}, u32[]{:S(2)}, u32[]{:S(2)}) collective-permute-start(bf16[2,512,128]{2,1,0:T(8,128)(2,1)S(1)} %bitcast.11), channel_id=1, source_target_pairs={{0,2},{1,15},{2,4},{3,1},{4,6},{5,3},{6,8},{7,5},{8,10},{9,7},{10,... | collective-permute-start | bytes 786440 | tf_op jit(solution)/shard_map/ppermute | solution.py:45
  14.5 8.1 %collective-permute-start.2 = (bf16[2,512,128]{2,1,0:T(8,128)(2,1)S(1)}, bf16[2,512,128]{2,1,0:T(8,128)(2,1)S(1)}, u32[]{:S(2)}, u32[]{:S(2)}) collective-permute-start(bf16[2,512,128]{2,1,0:T(8,128)(2,1)S(1)} %collective-permute-done.1), channel_id=1, source_target_pairs={{0,2},{1,15},{2,4},{3,1},{4,6},{5,3},{6,8},{7,5},{8,10},{9,7},{10,... | collective-permute-start | bytes 786440 | tf_op jit(solution)/shard_map/ppermute | solution.py:47
  18.6 7.9 %collective-permute-start.3 = (bf16[1,512,128]{2,1,0:T(8,128)(2,1)S(1)}, bf16[1,512,128]{2,1,0:T(8,128)(2,1)S(1)}, u32[]{:S(2)}, u32[]{:S(2)}) collective-permute-start(bf16[1,512,128]{2,1,0:T(8,128)(2,1)S(1)} %constant_dynamic-slice_fusion.4), channel_id=1, source_target_pairs={{0,4},{1,13},{2,6},{3,15},{4,8},{5,1},{6,10},{7,3},{8,12},{9,5},{1... | collective-permute-start | bytes 393224 | tf_op jit(solution)/shard_map/ppermute | solution.py:48
  26.5 9.7 %collective-permute-start.4 = (bf16[7,512,128]{2,1,0:T(8,128)(2,1)S(1)}, bf16[7,512,128]{2,1,0:T(8,128)(2,1)S(1)}, u32[]{:S(2)}, u32[]{:S(2)}) collective-permute-start(bf16[7,512,128]{2,1,0:T(8,128)(2,1)S(1)} %constant_dynamic-update-slice_fusion.received.refs_1_), channel_id=1, source_target_pairs={{0,1},{1,0},{2,3},{3,2},{4,5},{5,4},{6,7},{7,6},{8,9},{9,8},{10,11... | collective-permute-start | bytes 2752520 | tf_op jit(solution)/shard_map/ppermute | solution.py:50
  34.4 1.2 copy-start.6
  36.2 3.6 %copy-start.1 = (f32[2,2,2048]{2,1,0:T(2,128)S(1)}, f32[2,2,2048]{2,1,0:T(2,128)}, u32[]{:S(2)}) copy-start(f32[2,2,2048]{2,1,0:T(2,128)} %gain.9) | copy-start | bytes 98308
  36.3 3.6 %copy-start.4 = (bf16[2,2048,128]{2,1,0:T(8,128)(2,1)S(1)}, bf16[2,2048,128]{2,1,0:T(8,128)(2,1)}, u32[]{:S(2)}) copy-start(bf16[2,2048,128]{2,1,0:T(8,128)(2,1)} %refs_0_.7) | copy-start | bytes 3145732
  36.7 4.3 %copy-start.5 = (f32[2,2,257]{2,1,0:T(2,128)S(1)}, f32[2,2,257]{2,1,0:T(2,128)}, u32[]{:S(2)}) copy-start(f32[2,2,257]{2,1,0:T(2,128)} %bias.3) | copy-start | bytes 12340
  36.7 13.1 %collective-permute-start.5 = (bf16[512,256]{1,0:T(8,128)(2,1)S(1)}, bf16[512,256]{1,0:T(8,128)(2,1)S(1)}, u32[]{:S(2)}, u32[]{:S(2)}) collective-permute-start(bf16[512,256]{1,0:T(8,128)(2,1)S(1)} %get-tuple-element.28.refs_5_), channel_id=1, source_target_pairs={{0,16},{16,32},{32,48},{48,64},{64,80},{80,96},{96,112},{112,128},... | collective-permute-start | bytes 786440 | tf_op jit(solution)/shard_map/ppermute | solution.py:374
  44.4 18.4 %copy-start = (bf16[2,2048,128]{2,1,0:T(8,128)(2,1)S(1)}, bf16[2,2048,128]{2,1,0:T(8,128)(2,1)}, u32[]{:S(2)}) copy-start(bf16[2,2048,128]{2,1,0:T(8,128)(2,1)} %w.5) | copy-start | bytes 3145732
  53.9 10.9 %collective-permute-start.7 = (bf16[2,512,128]{2,1,0:T(8,128)(2,1)S(1)}, bf16[2,512,128]{2,1,0:T(8,128)(2,1)S(1)}, u32[]{:S(2)}, u32[]{:S(2)}) collective-permute-start(bf16[2,512,128]{2,1,0:T(8,128)(2,1)S(1)} %bitcast.7), channel_id=1, source_target_pairs={{0,4},{1,13},{2,6},{3,15},{4,8},{5,1},{6,10},{7,3},{8,12},{9,5},{1... | collective-permute-start | bytes 786440 | tf_op jit(solution)/shard_map/ppermute | solution.py:44
  56.5 15.9 %collective-permute-start.6 = (bf16[2,512,128]{2,1,0:T(8,128)(2,1)S(1)}, bf16[2,512,128]{2,1,0:T(8,128)(2,1)S(1)}, u32[]{:S(2)}, u32[]{:S(2)}) collective-permute-start(bf16[2,512,128]{2,1,0:T(8,128)(2,1)S(1)} %bitcast.8), channel_id=1, source_target_pairs={{0,2},{1,15},{2,4},{3,1},{4,6},{5,3},{6,8},{7,5},{8,10},{9,7},{10,... | collective-permute-start | bytes 786440 | tf_op jit(solution)/shard_map/ppermute | solution.py:45
  62.8 19.8 %collective-permute-start.11 = (bf16[2,2048,128]{2,1,0:T(8,128)(2,1)S(1)}, bf16[2,2048,128]{2,1,0:T(8,128)(2,1)S(1)}, u32[]{:S(2)}, u32[]{:S(2)}) collective-permute-start(bf16[2,2048,128]{2,1,0:T(8,128)(2,1)S(1)} %copy-done), channel_id=1, source_target_pairs={{0,1},{1,0},{2,3},{3,2},{4,5},{5,4},{6,7},{7,6},{8,9},{9,8},{10,11... | collective-permute-start | bytes 3145736 | tf_op jit(solution)/shard_map/ppermute | solution.py:384
  64.8 7.7 %collective-permute-start.8 = (bf16[2,512,128]{2,1,0:T(8,128)(2,1)S(1)}, bf16[2,512,128]{2,1,0:T(8,128)(2,1)S(1)}, u32[]{:S(2)}, u32[]{:S(2)}) collective-permute-start(bf16[2,512,128]{2,1,0:T(8,128)(2,1)S(1)} %collective-permute-done.7), channel_id=1, source_target_pairs={{0,2},{1,15},{2,4},{3,1},{4,6},{5,3},{6,8},{7,5},{8,10},{9,7},{10,... | collective-permute-start | bytes 786440 | tf_op jit(solution)/shard_map/ppermute | solution.py:47
  68.8 8.0 %collective-permute-start.9 = (bf16[1,512,128]{2,1,0:T(8,128)(2,1)S(1)}, bf16[1,512,128]{2,1,0:T(8,128)(2,1)S(1)}, u32[]{:S(2)}, u32[]{:S(2)}) collective-permute-start(bf16[1,512,128]{2,1,0:T(8,128)(2,1)S(1)} %constant_dynamic-slice_fusion.3), channel_id=1, source_target_pairs={{0,4},{1,13},{2,6},{3,15},{4,8},{5,1},{6,10},{7,3},{8,12},{9,5},{1... | collective-permute-start | bytes 393224 | tf_op jit(solution)/shard_map/ppermute | solution.py:48
  76.8 7.9 %collective-permute-start.10 = (bf16[7,512,128]{2,1,0:T(8,128)(2,1)S(1)}, bf16[7,512,128]{2,1,0:T(8,128)(2,1)S(1)}, u32[]{:S(2)}, u32[]{:S(2)}) collective-permute-start(bf16[7,512,128]{2,1,0:T(8,128)(2,1)S(1)} %constant_dynamic-update-slice_fusion.4.received), channel_id=1, source_target_pairs={{0,1},{1,0},{2,3},{3,2},{4,5},{5,4},{6,7},{7,6},{8,9},{9,8},{10,11... | collective-permute-start | bytes 2752520 | tf_op jit(solution)/shard_map/ppermute | solution.py:50
  83.2 27.9 %copy-start.2 = (bf16[2,2048,128]{2,1,0:T(8,128)(2,1)S(1)}, bf16[2,2048,128]{2,1,0:T(8,128)(2,1)}, u32[]{:S(2)}) copy-start(bf16[2,2048,128]{2,1,0:T(8,128)(2,1)} %refs_0_.6) | copy-start | bytes 3145732
  83.2 27.9 %copy-start.3 = (bf16[2,2048,128]{2,1,0:T(8,128)(2,1)S(1)}, bf16[2,2048,128]{2,1,0:T(8,128)(2,1)}, u32[]{:S(2)}) copy-start(bf16[2,2048,128]{2,1,0:T(8,128)(2,1)} %refs_1_.3) | copy-start | bytes 3145732
  85.2 10.1 %collective-permute-start.13 = (bf16[2,512,128]{2,1,0:T(8,128)(2,1)S(1)}, bf16[2,512,128]{2,1,0:T(8,128)(2,1)S(1)}, u32[]{:S(2)}, u32[]{:S(2)}) collective-permute-start(bf16[2,512,128]{2,1,0:T(8,128)(2,1)S(1)} %shard_map.80.own.b_own), channel_id=1, source_target_pairs={{0,4},{1,13},{2,6},{3,15},{4,8},{5,1},{6,10},{7,3},{8,12},{9,5},{1... | collective-permute-start | bytes 786440 | tf_op jit(solution)/shard_map/ppermute | solution.py:44
  89.0 13.3 %collective-permute-start.12 = (bf16[2,512,128]{2,1,0:T(8,128)(2,1)S(1)}, bf16[2,512,128]{2,1,0:T(8,128)(2,1)S(1)}, u32[]{:S(2)}, u32[]{:S(2)}) collective-permute-start(bf16[2,512,128]{2,1,0:T(8,128)(2,1)S(1)} %shard_map.80.own.b_own), channel_id=1, source_target_pairs={{0,2},{1,15},{2,4},{3,1},{4,6},{5,3},{6,8},{7,5},{8,10},{9,7},{10,... | collective-permute-start | bytes 786440 | tf_op jit(solution)/shard_map/ppermute | solution.py:45
  95.3 8.0 %collective-permute-start.14 = (bf16[2,512,128]{2,1,0:T(8,128)(2,1)S(1)}, bf16[2,512,128]{2,1,0:T(8,128)(2,1)S(1)}, u32[]{:S(2)}, u32[]{:S(2)}) collective-permute-start(bf16[2,512,128]{2,1,0:T(8,128)(2,1)S(1)} %collective-permute-done.13), channel_id=1, source_target_pairs={{0,2},{1,15},{2,4},{3,1},{4,6},{5,3},{6,8},{7,5},{8,10},{9,7},{10,... | collective-permute-start | bytes 786440 | tf_op jit(solution)/shard_map/ppermute | solution.py:47
  100.0 7.9 %collective-permute-start.15 = (bf16[1,512,128]{2,1,0:T(8,128)(2,1)S(1)}, bf16[1,512,128]{2,1,0:T(8,128)(2,1)S(1)}, u32[]{:S(2)}, u32[]{:S(2)}) collective-permute-start(bf16[1,512,128]{2,1,0:T(8,128)(2,1)S(1)} %constant_dynamic-slice_fusion.2), channel_id=1, source_target_pairs={{0,4},{1,13},{2,6},{3,15},{4,8},{5,1},{6,10},{7,3},{8,12},{9,5},{1... | collective-permute-start | bytes 393224 | tf_op jit(solution)/shard_map/ppermute | solution.py:48
  108.0 5.2 %collective-permute-start.16 = (bf16[7,512,128]{2,1,0:T(8,128)(2,1)S(1)}, bf16[7,512,128]{2,1,0:T(8,128)(2,1)S(1)}, u32[]{:S(2)}, u32[]{:S(2)}) collective-permute-start(bf16[7,512,128]{2,1,0:T(8,128)(2,1)S(1)} %constant_dynamic-update-slice_fusion.8.received.b_received), channel_id=1, source_target_pairs={{0,1},{1,0},{2,3},{3,2},{4,5},{5,4},{6,7},{7,6},{8,9},{9,8},{10,11... | collective-permute-start | bytes 2752520 | tf_op jit(solution)/shard_map/ppermute | solution.py:50
  115.1 12.7 %collective-permute-start.17 = (bf16[512,256]{1,0:T(8,128)(2,1)S(1)}, bf16[512,256]{1,0:T(8,128)(2,1)S(1)}, u32[]{:S(2)}, u32[]{:S(2)}) collective-permute-start(bf16[512,256]{1,0:T(8,128)(2,1)S(1)} %get-tuple-element.36.refs_3_), channel_id=1, source_target_pairs={{0,16},{16,32},{32,48},{48,64},{64,80},{80,96},{96,112},{112,128},... | collective-permute-start | bytes 786440 | tf_op jit(solution)/shard_map/ppermute | solution.py:374
  132.2 9.0 %collective-permute-start.19 = (bf16[2,512,128]{2,1,0:T(8,128)(2,1)S(1)}, bf16[2,512,128]{2,1,0:T(8,128)(2,1)S(1)}, u32[]{:S(2)}, u32[]{:S(2)}) collective-permute-start(bf16[2,512,128]{2,1,0:T(8,128)(2,1)S(1)} %bitcast.15), channel_id=1, source_target_pairs={{0,4},{1,13},{2,6},{3,15},{4,8},{5,1},{6,10},{7,3},{8,12},{9,5},{1... | collective-permute-start | bytes 786440 | tf_op jit(solution)/shard_map/ppermute | solution.py:44
  135.5 15.5 %collective-permute-start.18 = (bf16[2,512,128]{2,1,0:T(8,128)(2,1)S(1)}, bf16[2,512,128]{2,1,0:T(8,128)(2,1)S(1)}, u32[]{:S(2)}, u32[]{:S(2)}) collective-permute-start(bf16[2,512,128]{2,1,0:T(8,128)(2,1)S(1)} %bitcast.16), channel_id=1, source_target_pairs={{0,2},{1,15},{2,4},{3,1},{4,6},{5,3},{6,8},{7,5},{8,10},{9,7},{10,... | collective-permute-start | bytes 786440 | tf_op jit(solution)/shard_map/ppermute | solution.py:45
  141.2 9.9 %collective-permute-start.20 = (bf16[2,512,128]{2,1,0:T(8,128)(2,1)S(1)}, bf16[2,512,128]{2,1,0:T(8,128)(2,1)S(1)}, u32[]{:S(2)}, u32[]{:S(2)}) collective-permute-start(bf16[2,512,128]{2,1,0:T(8,128)(2,1)S(1)} %collective-permute-done.19), channel_id=1, source_target_pairs={{0,2},{1,15},{2,4},{3,1},{4,6},{5,3},{6,8},{7,5},{8,10},{9,7},{10,... | collective-permute-start | bytes 786440 | tf_op jit(solution)/shard_map/ppermute | solution.py:47
  147.4 7.8 %collective-permute-start.21 = (bf16[1,512,128]{2,1,0:T(8,128)(2,1)S(1)}, bf16[1,512,128]{2,1,0:T(8,128)(2,1)S(1)}, u32[]{:S(2)}, u32[]{:S(2)}) collective-permute-start(bf16[1,512,128]{2,1,0:T(8,128)(2,1)S(1)} %constant_dynamic-slice_fusion.1), channel_id=1, source_target_pairs={{0,4},{1,13},{2,6},{3,15},{4,8},{5,1},{6,10},{7,3},{8,12},{9,5},{1... | collective-permute-start | bytes 393224 | tf_op jit(solution)/shard_map/ppermute | solution.py:48
  155.2 7.9 %collective-permute-start.22 = (bf16[7,512,128]{2,1,0:T(8,128)(2,1)S(1)}, bf16[7,512,128]{2,1,0:T(8,128)(2,1)S(1)}, u32[]{:S(2)}, u32[]{:S(2)}) collective-permute-start(bf16[7,512,128]{2,1,0:T(8,128)(2,1)S(1)} %constant_dynamic-update-slice_fusion.12.received), channel_id=1, source_target_pairs={{0,1},{1,0},{2,3},{3,2},{4,5},{5,4},{6,7},{7,6},{8,9},{9,8},{10,11... | collective-permute-start | bytes 2752520 | tf_op jit(solution)/shard_map/ppermute | solution.py:50
  164.5 13.5 %all-to-all-start = ((f32[16,4,128]{2,1,0:T(4,128)}), f32[16,4,128]{2,1,0:T(4,128)S(1)}, u32[]{:S(2)}, u32[]{:S(2)}) async-start(f32[16,4,128]{2,1,0:T(4,128)} %get-tuple-element.42), calls=%async_computation | async-start | bytes 65536 | tf_op jit(solution)/shard_map/all_to_all | solution.py:424

commit v6 on v5

--- a/solution.py
+++ b/solution.py
@@ -316,10 +316,15 @@
     out[1 - core] = total[:, BLK:].astype(jnp.bfloat16)
 
 
-def last_kernel(place, own, received, other, w, out, squares):
-    out[...] = rows_product(1, block_ids(place), 0, (own, received, other), (w,))
+def last_part_kernel(place, own, received, w, acc):
+    acc[...] = rows_product(1, block_ids(place), 0, (own, received), (w,))
+
+
+def last_kernel(place, other, w, acc, out, squares):
+    total = acc[...] + rows_product(1, block_ids(place), 9, (other,), (w,))
+    out[...] = total
     for i in range(4):
-        x = out[i * BLK : (i + 1) * BLK, :]
+        x = total[i * BLK : (i + 1) * BLK, :]
         sums = jnp.sum((x * x).T, axis=0, keepdims=True)
         for n in range(NB):
             squares[n, i : i + 1, :] = sums
@@ -413,10 +418,14 @@
         (place, *stream, *branch, total, gains, wkv),
     )
     attended = gather_blocks(attention(1, (full,), wq, kv, inv))
+    acc = call(
+        last_part_kernel, [SMEM] + [VMEM] * 3, wide, [], 4, 10**9,
+        (place, *attended[:2], w_out),
+    )
     branch, squares = call(
-        last_kernel, [SMEM] + [VMEM] * 4,
+        last_kernel, [SMEM] + [VMEM] * 3,
         (wide, jax.ShapeDtypeStruct((NB, tokens // BLK, BLK), jnp.float32)), [], 4, 10**9,
-        (place, *attended, w_out),
+        (place, attended[2], w_out, acc),
     )
     own_gain = lax.dynamic_slice_in_dim(
         gains[1, 1].reshape(1, D), lax.axis_index(("y", "c")) * BLK, BLK, 1

time: 180 us -> 180 us (level)
    pallas_call x16 -> x17, Pallas kernels: 23.6 us -> 23.8 us  [call(): pl.pallas_call(kernel, out_shape=outs, in_specs=ins, out_specs=jax.tree.m...]
where the time goes in v6:
time: 180 us; the launch traced here: 179 us
  starting transfers between devices  97.4 us (54%)
  waiting for transfers between devices  47.1 us (26%)
  Pallas kernels  23.8 us (13%)
  blocking collectives  7.85 us (4%)
    pallas_call x17, Pallas kernels, call(): pl.pallas_call(kernel, out_shape=outs, in_specs=ins, out_specs=jax.tree.m...  23.8 us
    ppermute x4, starting transfers between devices, gather_blocks(): other = lax.ppermute(received, 'c', [(0, 1), (1, 0)])  19.1 us
    ppermute x4, starting transfers between devices, gather_blocks(): three = lax.ppermute(two, ('y', 'c'), core_pairs(1))  19 us
    ppermute x4, starting transfers between devices, gather_blocks(): one = lax.ppermute(own, ('y', 'c'), core_pairs(1))  17 us
    ppermute x4, waiting for transfers between devices, gather_blocks(): four = lax.ppermute(half, ('y', 'c'), core_pairs(2))  16.9 us
    ppermute x4, starting transfers between devices, gather_blocks(): two = lax.ppermute(own, ('y', 'c'), core_pairs(2))  15.6 us
    ppermute x4, starting transfers between devices, gather_blocks(): four = lax.ppermute(half, ('y', 'c'), core_pairs(2))  13.2 us
    ppermute x2, waiting for transfers between devices, attention(): previous = lax.ppermute(kv, 'sp', shift)  11.5 us
  transfers between devices with their start and end apart: 24, of which 12 were waited for; matrix products, arithmetic and copies ran while one was open for 0% of the time, Pallas kernels for 9%

profile of v6, /device:TPU:257, one launch (start us, length us, event | category | flops | bytes accessed | tf_op | source)
XLA Modules:
  0.0 178.6 jit_solution(3415280335563548489)
XLA Ops:
  0.0 2.5 %all-gather = bf16[1024,128]{1,0:T(8,128)(2,1)S(1)} all-gather(bf16[512,128]{1,0:T(8,128)(2,1)} %param.7), channel_id=2, replica_groups=mesh['sp'=32,'y'=8,'c'=2] {'c'}, dimensions={0}, use_global_device_ids=true | all-gather | bytes 393216 | tf_op jit(solution)/shard_map/all_gather | solution.py:43
  2.5 5.9 %collective-permute-start.1 = (bf16[2,512,128]{2,1,0:T(8,128)(2,1)S(1)}, bf16[2,512,128]{2,1,0:T(8,128)(2,1)S(1)}, u32[]{:S(2)}, u32[]{:S(2)}) collective-permute-start(bf16[2,512,128]{2,1,0:T(8,128)(2,1)S(1)} %bitcast.10), channel_id=1, source_target_pairs={{0,4},{1,13},{2,6},{3,15},{4,8},{5,1},{6,10},{7,3},{8,12},{9,5},{1... | collective-permute-start | bytes 786440 | tf_op jit(solution)/shard_map/ppermute | solution.py:44
  8.4 3.0 %collective-permute-start = (bf16[2,512,128]{2,1,0:T(8,128)(2,1)S(1)}, bf16[2,512,128]{2,1,0:T(8,128)(2,1)S(1)}, u32[]{:S(2)}, u32[]{:S(2)}) collective-permute-start(bf16[2,512,128]{2,1,0:T(8,128)(2,1)S(1)} %bitcast.11), channel_id=1, source_target_pairs={{0,2},{1,15},{2,4},{3,1},{4,6},{5,3},{6,8},{7,5},{8,10},{9,7},{10,... | collective-permute-start | bytes 786440 | tf_op jit(solution)/shard_map/ppermute | solution.py:45
  11.4 3.1 %collective-permute-done.1 = bf16[2,512,128]{2,1,0:T(8,128)(2,1)S(1)} collective-permute-done((bf16[2,512,128]{2,1,0:T(8,128)(2,1)S(1)}, bf16[2,512,128]{2,1,0:T(8,128)(2,1)S(1)}, u32[]{:S(2)}, u32[]{:S(2)}) %collective-permute-start.1) | collective-permute-done | bytes 262176 | tf_op jit(solution)/shard_map/ppermute | solution.py:44
  14.5 4.1 %collective-permute-start.2 = (bf16[2,512,128]{2,1,0:T(8,128)(2,1)S(1)}, bf16[2,512,128]{2,1,0:T(8,128)(2,1)S(1)}, u32[]{:S(2)}, u32[]{:S(2)}) collective-permute-start(bf16[2,512,128]{2,1,0:T(8,128)(2,1)S(1)} %collective-permute-done.1), channel_id=1, source_target_pairs={{0,2},{1,15},{2,4},{3,1},{4,6},{5,3},{6,8},{7,5},{8,10},{9,7},{10,... | collective-permute-start | bytes 786440 | tf_op jit(solution)/shard_map/ppermute | solution.py:47
  18.6 3.9 %collective-permute-start.3 = (bf16[1,512,128]{2,1,0:T(8,128)(2,1)S(1)}, bf16[1,512,128]{2,1,0:T(8,128)(2,1)S(1)}, u32[]{:S(2)}, u32[]{:S(2)}) collective-permute-start(bf16[1,512,128]{2,1,0:T(8,128)(2,1)S(1)} %constant_dynamic-slice_fusion.4), channel_id=1, source_target_pairs={{0,4},{1,13},{2,6},{3,15},{4,8},{5,1},{6,10},{7,3},{8,12},{9,5},{1... | collective-permute-start | bytes 393224 | tf_op jit(solution)/shard_map/ppermute | solution.py:48
  22.5 0.0 collective-permute-done
  22.6 3.9 %collective-permute-done.3 = bf16[1,512,128]{2,1,0:T(8,128)(2,1)S(1)} collective-permute-done((bf16[1,512,128]{2,1,0:T(8,128)(2,1)S(1)}, bf16[1,512,128]{2,1,0:T(8,128)(2,1)S(1)}, u32[]{:S(2)}, u32[]{:S(2)}) %collective-permute-start.3) | collective-permute-done | bytes 131104 | tf_op jit(solution)/shard_map/ppermute | solution.py:48
  26.5 4.4 %collective-permute-start.4 = (bf16[7,512,128]{2,1,0:T(8,128)(2,1)S(1)}, bf16[7,512,128]{2,1,0:T(8,128)(2,1)S(1)}, u32[]{:S(2)}, u32[]{:S(2)}) collective-permute-start(bf16[7,512,128]{2,1,0:T(8,128)(2,1)S(1)} %constant_dynamic-update-slice_fusion.received.refs_1_), channel_id=1, source_target_pairs={{0,1},{1,0},{2,3},{3,2},{4,5},{5,4},{6,7},{7,6},{8,9},{9,8},{10,11... | collective-permute-start | bytes 2752520 | tf_op jit(solution)/shard_map/ppermute | solution.py:50
  31.0 3.4 %shard_map.74.w = bf16[16,128,256]{2,1,0:T(8,128)(2,1)} custom-call(s32[1]{0:T(128)} %bitcast.place, f32[2,2,2048]{2,1,0:T(2,128)} %gain.9, bf16[2,2048,128]{2,1,0:T(8,128)(2,1)} %refs_0_.6, bf16[2,2048,128]{2,1,0:T(8,128)(2,1)} %refs_1_.3), custom_call_target="tpu_custom_call" | custom-call | flops 1000000000 | bytes 2129924 | tf_op jit(solution)/shard_map/pallas_call | solution.py:345
  34.5 1.2 copy-done.6
  35.7 0.6 shard_map.75
  36.2 0.0 copy-start.1
  36.3 0.0 copy-start.4
  36.3 0.4 shard_map.76
  36.7 0.0 copy-start.5
  36.7 3.1 %collective-permute-start.5 = (bf16[512,256]{1,0:T(8,128)(2,1)S(1)}, bf16[512,256]{1,0:T(8,128)(2,1)S(1)}, u32[]{:S(2)}, u32[]{:S(2)}) collective-permute-start(bf16[512,256]{1,0:T(8,128)(2,1)S(1)} %get-tuple-element.28.refs_5_), channel_id=1, source_target_pairs={{0,16},{16,32},{32,48},{48,64},{64,80},{80,96},{96,112},{112,128},... | collective-permute-start | bytes 786440 | tf_op jit(solution)/shard_map/ppermute | solution.py:379
  39.9 1.1 shard_map.73.refs_3_
  41.0 3.3 %shard_map.77 = (bf16[512,128]{1,0:T(8,128)(2,1)S(1)}, f32[512,128]{1,0:T(8,128)S(1)}, f32[512,128]{1,0:T(8,128)S(1)}, f32[512,128]{1,0:T(8,128)S(1)}, f32[2,128,128]{2,1,0:T(8,128)S(1)}) custom-call(bf16[2,512,128]{2,1,0:T(8,128)(2,1)S(1)} %bitcast.13, bf16[7,512,128]{2,1,0:T(8,128)(2,1)S(1)} %constant_dynamic-update-slice_fusion.received.refs_1_, ...), custom_call_target="tpu_custom_call" | custom-call | flops 2000000000 | bytes 3149840 | tf_op jit(solution)/shard_map/pallas_call | solution.py:345
  44.4 0.0 copy-start
  44.4 5.4 %collective-permute-done.5.kv = bf16[512,256]{1,0:T(8,128)(2,1)S(1)} collective-permute-done((bf16[512,256]{1,0:T(8,128)(2,1)S(1)}, bf16[512,256]{1,0:T(8,128)(2,1)S(1)}, u32[]{:S(2)}, u32[]{:S(2)}) %collective-permute-start.5) | collective-permute-done | bytes 262176 | tf_op jit(solution)/shard_map/ppermute | solution.py:379
  49.8 1.5 shard_map.78
  51.4 2.5 %all-gather.1 = bf16[1024,128]{1,0:T(8,128)(2,1)S(1)} all-gather(bf16[512,128]{1,0:T(8,128)(2,1)S(1)} %shard_map.78), channel_id=3, replica_groups=mesh['sp'=32,'y'=8,'c'=2] {'c'}, dimensions={0}, use_global_device_ids=true | all-gather | bytes 393216 | tf_op jit(solution)/shard_map/all_gather | solution.py:43
  53.9 2.7 %collective-permute-start.7 = (bf16[2,512,128]{2,1,0:T(8,128)(2,1)S(1)}, bf16[2,512,128]{2,1,0:T(8,128)(2,1)S(1)}, u32[]{:S(2)}, u32[]{:S(2)}) collective-permute-start(bf16[2,512,128]{2,1,0:T(8,128)(2,1)S(1)} %bitcast.7), channel_id=1, source_target_pairs={{0,4},{1,13},{2,6},{3,15},{4,8},{5,1},{6,10},{7,3},{8,12},{9,5},{1... | collective-permute-start | bytes 786440 | tf_op jit(solution)/shard_map/ppermute | solution.py:44
  56.5 6.3 %collective-permute-start.6 = (bf16[2,512,128]{2,1,0:T(8,128)(2,1)S(1)}, bf16[2,512,128]{2,1,0:T(8,128)(2,1)S(1)}, u32[]{:S(2)}, u32[]{:S(2)}) collective-permute-start(bf16[2,512,128]{2,1,0:T(8,128)(2,1)S(1)} %bitcast.8), channel_id=1, source_target_pairs={{0,2},{1,15},{2,4},{3,1},{4,6},{5,3},{6,8},{7,5},{8,10},{9,7},{10,... | collective-permute-start | bytes 786440 | tf_op jit(solution)/shard_map/ppermute | solution.py:45
  62.8 1.9 %collective-permute-start.11 = (bf16[2,2048,128]{2,1,0:T(8,128)(2,1)S(1)}, bf16[2,2048,128]{2,1,0:T(8,128)(2,1)S(1)}, u32[]{:S(2)}, u32[]{:S(2)}) collective-permute-start(bf16[2,2048,128]{2,1,0:T(8,128)(2,1)S(1)} %copy-done), channel_id=1, source_target_pairs={{0,1},{1,0},{2,3},{3,2},{4,5},{5,4},{6,7},{7,6},{8,9},{9,8},{10,11... | collective-permute-start | bytes 3145736 | tf_op jit(solution)/shard_map/ppermute | solution.py:389
  64.7 4.0 %collective-permute-start.8 = (bf16[2,512,128]{2,1,0:T(8,128)(2,1)S(1)}, bf16[2,512,128]{2,1,0:T(8,128)(2,1)S(1)}, u32[]{:S(2)}, u32[]{:S(2)}) collective-permute-start(bf16[2,512,128]{2,1,0:T(8,128)(2,1)S(1)} %collective-permute-done.7), channel_id=1, source_target_pairs={{0,2},{1,15},{2,4},{3,1},{4,6},{5,3},{6,8},{7,5},{8,10},{9,7},{10,... | collective-permute-start | bytes 786440 | tf_op jit(solution)/shard_map/ppermute | solution.py:47
  68.8 3.6 %collective-permute-start.9 = (bf16[1,512,128]{2,1,0:T(8,128)(2,1)S(1)}, bf16[1,512,128]{2,1,0:T(8,128)(2,1)S(1)}, u32[]{:S(2)}, u32[]{:S(2)}) collective-permute-start(bf16[1,512,128]{2,1,0:T(8,128)(2,1)S(1)} %constant_dynamic-slice_fusion.3), channel_id=1, source_target_pairs={{0,4},{1,13},{2,6},{3,15},{4,8},{5,1},{6,10},{7,3},{8,12},{9,5},{1... | collective-permute-start | bytes 393224 | tf_op jit(solution)/shard_map/ppermute | solution.py:48
  72.5 4.2 %collective-permute-done.9 = bf16[1,512,128]{2,1,0:T(8,128)(2,1)S(1)} collective-permute-done((bf16[1,512,128]{2,1,0:T(8,128)(2,1)S(1)}, bf16[1,512,128]{2,1,0:T(8,128)(2,1)S(1)}, u32[]{:S(2)}, u32[]{:S(2)}) %collective-permute-start.9) | collective-permute-done | bytes 131104 | tf_op jit(solution)/shard_map/ppermute | solution.py:48
  76.8 5.9 %collective-permute-start.10 = (bf16[7,512,128]{2,1,0:T(8,128)(2,1)S(1)}, bf16[7,512,128]{2,1,0:T(8,128)(2,1)S(1)}, u32[]{:S(2)}, u32[]{:S(2)}) collective-permute-start(bf16[7,512,128]{2,1,0:T(8,128)(2,1)S(1)} %constant_dynamic-update-slice_fusion.4.received), channel_id=1, source_target_pairs={{0,1},{1,0},{2,3},{3,2},{4,5},{5,4},{6,7},{7,6},{8,9},{9,8},{10,11... | collective-permute-start | bytes 2752520 | tf_op jit(solution)/shard_map/ppermute | solution.py:50
  82.7 0.5 shard_map.79.acc
  83.2 0.0 copy-start.2
  83.2 0.0 copy-start.3
  83.2 1.5 collective-permute-done.10.other
  84.7 0.4 shard_map.80.own.b_own
  85.2 3.8 %collective-permute-start.13 = (bf16[2,512,128]{2,1,0:T(8,128)(2,1)S(1)}, bf16[2,512,128]{2,1,0:T(8,128)(2,1)S(1)}, u32[]{:S(2)}, u32[]{:S(2)}) collective-permute-start(bf16[2,512,128]{2,1,0:T(8,128)(2,1)S(1)} %shard_map.80.own.b_own), channel_id=1, source_target_pairs={{0,4},{1,13},{2,6},{3,15},{4,8},{5,1},{6,10},{7,3},{8,12},{9,5},{1... | collective-permute-start | bytes 786440 | tf_op jit(solution)/shard_map/ppermute | solution.py:44
  89.0 2.1 %collective-permute-start.12 = (bf16[2,512,128]{2,1,0:T(8,128)(2,1)S(1)}, bf16[2,512,128]{2,1,0:T(8,128)(2,1)S(1)}, u32[]{:S(2)}, u32[]{:S(2)}) collective-permute-start(bf16[2,512,128]{2,1,0:T(8,128)(2,1)S(1)} %shard_map.80.own.b_own), channel_id=1, source_target_pairs={{0,2},{1,15},{2,4},{3,1},{4,6},{5,3},{6,8},{7,5},{8,10},{9,7},{10,... | collective-permute-start | bytes 786440 | tf_op jit(solution)/shard_map/ppermute | solution.py:45
  91.1 4.1 %collective-permute-done.13 = bf16[2,512,128]{2,1,0:T(8,128)(2,1)S(1)} collective-permute-done((bf16[2,512,128]{2,1,0:T(8,128)(2,1)S(1)}, bf16[2,512,128]{2,1,0:T(8,128)(2,1)S(1)}, u32[]{:S(2)}, u32[]{:S(2)}) %collective-permute-start.13) | collective-permute-done | bytes 262176 | tf_op jit(solution)/shard_map/ppermute | solution.py:44
  95.2 4.7 %collective-permute-start.14 = (bf16[2,512,128]{2,1,0:T(8,128)(2,1)S(1)}, bf16[2,512,128]{2,1,0:T(8,128)(2,1)S(1)}, u32[]{:S(2)}, u32[]{:S(2)}) collective-permute-start(bf16[2,512,128]{2,1,0:T(8,128)(2,1)S(1)} %collective-permute-done.13), channel_id=1, source_target_pairs={{0,2},{1,15},{2,4},{3,1},{4,6},{5,3},{6,8},{7,5},{8,10},{9,7},{10,... | collective-permute-start | bytes 786440 | tf_op jit(solution)/shard_map/ppermute | solution.py:47
  100.0 2.2 %collective-permute-start.15 = (bf16[1,512,128]{2,1,0:T(8,128)(2,1)S(1)}, bf16[1,512,128]{2,1,0:T(8,128)(2,1)S(1)}, u32[]{:S(2)}, u32[]{:S(2)}) collective-permute-start(bf16[1,512,128]{2,1,0:T(8,128)(2,1)S(1)} %constant_dynamic-slice_fusion.2), channel_id=1, source_target_pairs={{0,4},{1,13},{2,6},{3,15},{4,8},{5,1},{6,10},{7,3},{8,12},{9,5},{1... | collective-permute-start | bytes 393224 | tf_op jit(solution)/shard_map/ppermute | solution.py:48
  102.3 1.0 collective-permute-done.14
  103.3 4.6 %collective-permute-done.15 = bf16[1,512,128]{2,1,0:T(8,128)(2,1)S(1)} collective-permute-done((bf16[1,512,128]{2,1,0:T(8,128)(2,1)S(1)}, bf16[1,512,128]{2,1,0:T(8,128)(2,1)S(1)}, u32[]{:S(2)}, u32[]{:S(2)}) %collective-permute-start.15) | collective-permute-done | bytes 131104 | tf_op jit(solution)/shard_map/ppermute | solution.py:48
  108.0 3.1 %collective-permute-start.16 = (bf16[7,512,128]{2,1,0:T(8,128)(2,1)S(1)}, bf16[7,512,128]{2,1,0:T(8,128)(2,1)S(1)}, u32[]{:S(2)}, u32[]{:S(2)}) collective-permute-start(bf16[7,512,128]{2,1,0:T(8,128)(2,1)S(1)} %constant_dynamic-update-slice_fusion.8.received.b_received), channel_id=1, source_target_pairs={{0,1},{1,0},{2,3},{3,2},{4,5},{5,4},{6,7},{7,6},{8,9},{9,8},{10,11... | collective-permute-start | bytes 2752520 | tf_op jit(solution)/shard_map/ppermute | solution.py:50
  111.1 1.9 %shard_map.82.w = bf16[16,128,256]{2,1,0:T(8,128)(2,1)S(1)} custom-call(s32[1]{0:T(128)} %bitcast.place, f32[2,2,2048]{2,1,0:T(2,128)S(1)} %copy-done.1, bf16[2,2048,128]{2,1,0:T(8,128)(2,1)S(1)} %copy-done.2, bf16[2,2048,128]{2,1,0:T(8,128)(2,1)S(1)} %copy-done.3), custom_call_target="tpu_custom_call" | custom-call | flops 1000000000 | bytes 2129924 | tf_op jit(solution)/shard_map/pallas_call | solution.py:345
  113.0 0.1 shard_map.81.b_total
  113.2 1.9 %shard_map.83 = (bf16[512,256]{1,0:T(8,128)(2,1)S(1)}, f32[512,128]{1,0:T(8,128)S(1)}, bf16[16,512,128]{2,1,0:T(8,128)(2,1)S(1)}, bf16[512,128]{1,0:T(8,128)(2,1)S(1)}) custom-call(s32[1]{0:T(128)} %bitcast.place, bf16[2,512,128]{2,1,0:T(8,128)(2,1)S(1)} %bitcast.14, bf16[7,512,128]{2,1,0:T(8,128)(2,1)S(1)} %constant_dynamic-update-slice_fusion.received.refs_1_, ...), custom_call_target="tpu_custom_call" | custom-call | flops 2000000000 | bytes 5537796 | tf_op jit(solution)/shard_map/pallas_call | solution.py:345
  115.1 2.1 %collective-permute-start.17 = (bf16[512,256]{1,0:T(8,128)(2,1)S(1)}, bf16[512,256]{1,0:T(8,128)(2,1)S(1)}, u32[]{:S(2)}, u32[]{:S(2)}) collective-permute-start(bf16[512,256]{1,0:T(8,128)(2,1)S(1)} %get-tuple-element.36.refs_3_), channel_id=1, source_target_pairs={{0,16},{16,32},{32,48},{48,64},{64,80},{80,96},{96,112},{112,128},... | collective-permute-start | bytes 786440 | tf_op jit(solution)/shard_map/ppermute | solution.py:379
  117.2 1.1 shard_map.84.refs_1_
  118.3 3.3 %shard_map.85 = (bf16[512,128]{1,0:T(8,128)(2,1)S(1)}, f32[512,128]{1,0:T(8,128)S(1)}, f32[512,128]{1,0:T(8,128)S(1)}, f32[512,128]{1,0:T(8,128)S(1)}, f32[2,128,128]{2,1,0:T(8,128)S(1)}) custom-call(bf16[16,512,128]{2,1,0:T(8,128)(2,1)S(1)} %get-tuple-element.34.refs_0_, bf16[16,128,128]{2,1,0:T(8,128)(2,1)S(1)} %shard_map.84.refs_1_, ...), custom_call_target="tpu_custom_call" | custom-call | flops 2000000000 | bytes 3149840 | tf_op jit(solution)/shard_map/pallas_call | solution.py:345
  121.7 6.1 %collective-permute-done.17.kv = bf16[512,256]{1,0:T(8,128)(2,1)S(1)} collective-permute-done((bf16[512,256]{1,0:T(8,128)(2,1)S(1)}, bf16[512,256]{1,0:T(8,128)(2,1)S(1)}, u32[]{:S(2)}, u32[]{:S(2)}) %collective-permute-start.17) | collective-permute-done | bytes 262176 | tf_op jit(solution)/shard_map/ppermute | solution.py:379
  127.8 1.6 shard_map.86
  129.4 2.8 %all-gather.2 = bf16[1024,128]{1,0:T(8,128)(2,1)S(1)} all-gather(bf16[512,128]{1,0:T(8,128)(2,1)S(1)} %shard_map.86), channel_id=4, replica_groups=mesh['sp'=32,'y'=8,'c'=2] {'c'}, dimensions={0}, use_global_device_ids=true | all-gather | bytes 393216 | tf_op jit(solution)/shard_map/all_gather | solution.py:43
  132.2 3.2 %collective-permute-start.19 = (bf16[2,512,128]{2,1,0:T(8,128)(2,1)S(1)}, bf16[2,512,128]{2,1,0:T(8,128)(2,1)S(1)}, u32[]{:S(2)}, u32[]{:S(2)}) collective-permute-start(bf16[2,512,128]{2,1,0:T(8,128)(2,1)S(1)} %bitcast.15), channel_id=1, source_target_pairs={{0,4},{1,13},{2,6},{3,15},{4,8},{5,1},{6,10},{7,3},{8,12},{9,5},{1... | collective-permute-start | bytes 786440 | tf_op jit(solution)/shard_map/ppermute | solution.py:44
  135.5 5.7 %collective-permute-start.18 = (bf16[2,512,128]{2,1,0:T(8,128)(2,1)S(1)}, bf16[2,512,128]{2,1,0:T(8,128)(2,1)S(1)}, u32[]{:S(2)}, u32[]{:S(2)}) collective-permute-start(bf16[2,512,128]{2,1,0:T(8,128)(2,1)S(1)} %bitcast.16), channel_id=1, source_target_pairs={{0,2},{1,15},{2,4},{3,1},{4,6},{5,3},{6,8},{7,5},{8,10},{9,7},{10,... | collective-permute-start | bytes 786440 | tf_op jit(solution)/shard_map/ppermute | solution.py:45
  141.2 6.2 %collective-permute-start.20 = (bf16[2,512,128]{2,1,0:T(8,128)(2,1)S(1)}, bf16[2,512,128]{2,1,0:T(8,128)(2,1)S(1)}, u32[]{:S(2)}, u32[]{:S(2)}) collective-permute-start(bf16[2,512,128]{2,1,0:T(8,128)(2,1)S(1)} %collective-permute-done.19), channel_id=1, source_target_pairs={{0,2},{1,15},{2,4},{3,1},{4,6},{5,3},{6,8},{7,5},{8,10},{9,7},{10,... | collective-permute-start | bytes 786440 | tf_op jit(solution)/shard_map/ppermute | solution.py:47
  147.4 3.5 %collective-permute-start.21 = (bf16[1,512,128]{2,1,0:T(8,128)(2,1)S(1)}, bf16[1,512,128]{2,1,0:T(8,128)(2,1)S(1)}, u32[]{:S(2)}, u32[]{:S(2)}) collective-permute-start(bf16[1,512,128]{2,1,0:T(8,128)(2,1)S(1)} %constant_dynamic-slice_fusion.1), channel_id=1, source_target_pairs={{0,4},{1,13},{2,6},{3,15},{4,8},{5,1},{6,10},{7,3},{8,12},{9,5},{1... | collective-permute-start | bytes 393224 | tf_op jit(solution)/shard_map/ppermute | solution.py:48
  151.1 4.1 %collective-permute-done.21 = bf16[1,512,128]{2,1,0:T(8,128)(2,1)S(1)} collective-permute-done((bf16[1,512,128]{2,1,0:T(8,128)(2,1)S(1)}, bf16[1,512,128]{2,1,0:T(8,128)(2,1)S(1)}, u32[]{:S(2)}, u32[]{:S(2)}) %collective-permute-start.21) | collective-permute-done | bytes 131104 | tf_op jit(solution)/shard_map/ppermute | solution.py:48
  155.2 5.8 %collective-permute-start.22 = (bf16[7,512,128]{2,1,0:T(8,128)(2,1)S(1)}, bf16[7,512,128]{2,1,0:T(8,128)(2,1)S(1)}, u32[]{:S(2)}, u32[]{:S(2)}) collective-permute-start(bf16[7,512,128]{2,1,0:T(8,128)(2,1)S(1)} %constant_dynamic-update-slice_fusion.12.received), channel_id=1, source_target_pairs={{0,1},{1,0},{2,3},{3,2},{4,5},{5,4},{6,7},{7,6},{8,9},{9,8},{10,11... | collective-permute-start | bytes 2752520 | tf_op jit(solution)/shard_map/ppermute | solution.py:50
  161.0 0.5 shard_map.87.acc
  161.5 1.6 collective-permute-done.22.other
  163.0 1.1 shard_map.88
  164.2 6.2 %all-to-all-start = ((f32[16,4,128]{2,1,0:T(4,128)}), f32[16,4,128]{2,1,0:T(4,128)S(1)}, u32[]{:S(2)}, u32[]{:S(2)}) async-start(f32[16,4,128]{2,1,0:T(4,128)} %get-tuple-element.42), calls=%async_computation | async-start | bytes 65536 | tf_op jit(solution)/shard_map/all_to_all | solution.py:433
  170.4 7.4 %all-to-all-done.squares = f32[16,4,128]{2,1,0:T(4,128)S(1)} async-done(((f32[16,4,128]{2,1,0:T(4,128)}), f32[16,4,128]{2,1,0:T(4,128)S(1)}, u32[]{:S(2)}, u32[]{:S(2)}) %all-to-all-start) | async-done | bytes 32800 | tf_op jit(solution)/shard_map/all_to_all | solution.py:433
  177.8 0.8 shard_map.89
  (40 shorter events, 0.6 us)
Async XLA Ops:
  2.5 12.0 %collective-permute-start.1 = (bf16[2,512,128]{2,1,0:T(8,128)(2,1)S(1)}, bf16[2,512,128]{2,1,0:T(8,128)(2,1)S(1)}, u32[]{:S(2)}, u32[]{:S(2)}) collective-permute-start(bf16[2,512,128]{2,1,0:T(8,128)(2,1)S(1)} %bitcast.10), channel_id=1, source_target_pairs={{0,4},{1,13},{2,6},{3,15},{4,8},{5,1},{6,10},{7,3},{8,12},{9,5},{1... | collective-permute-start | bytes 786440 | tf_op jit(solution)/shard_map/ppermute | solution.py:44
  8.4 14.1 %collective-permute-start = (bf16[2,512,128]{2,1,0:T(8,128)(2,1)S(1)}, bf16[2,512,128]{2,1,0:T(8,128)(2,1)S(1)}, u32[]{:S(2)}, u32[]{:S(2)}) collective-permute-start(bf16[2,512,128]{2,1,0:T(8,128)(2,1)S(1)} %bitcast.11), channel_id=1, source_target_pairs={{0,2},{1,15},{2,4},{3,1},{4,6},{5,3},{6,8},{7,5},{8,10},{9,7},{10,... | collective-permute-start | bytes 786440 | tf_op jit(solution)/shard_map/ppermute | solution.py:45
  14.5 8.1 %collective-permute-start.2 = (bf16[2,512,128]{2,1,0:T(8,128)(2,1)S(1)}, bf16[2,512,128]{2,1,0:T(8,128)(2,1)S(1)}, u32[]{:S(2)}, u32[]{:S(2)}) collective-permute-start(bf16[2,512,128]{2,1,0:T(8,128)(2,1)S(1)} %collective-permute-done.1), channel_id=1, source_target_pairs={{0,2},{1,15},{2,4},{3,1},{4,6},{5,3},{6,8},{7,5},{8,10},{9,7},{10,... | collective-permute-start | bytes 786440 | tf_op jit(solution)/shard_map/ppermute | solution.py:47
  18.6 7.9 %collective-permute-start.3 = (bf16[1,512,128]{2,1,0:T(8,128)(2,1)S(1)}, bf16[1,512,128]{2,1,0:T(8,128)(2,1)S(1)}, u32[]{:S(2)}, u32[]{:S(2)}) collective-permute-start(bf16[1,512,128]{2,1,0:T(8,128)(2,1)S(1)} %constant_dynamic-slice_fusion.4), channel_id=1, source_target_pairs={{0,4},{1,13},{2,6},{3,15},{4,8},{5,1},{6,10},{7,3},{8,12},{9,5},{1... | collective-permute-start | bytes 393224 | tf_op jit(solution)/shard_map/ppermute | solution.py:48
  26.5 9.7 %collective-permute-start.4 = (bf16[7,512,128]{2,1,0:T(8,128)(2,1)S(1)}, bf16[7,512,128]{2,1,0:T(8,128)(2,1)S(1)}, u32[]{:S(2)}, u32[]{:S(2)}) collective-permute-start(bf16[7,512,128]{2,1,0:T(8,128)(2,1)S(1)} %constant_dynamic-update-slice_fusion.received.refs_1_), channel_id=1, source_target_pairs={{0,1},{1,0},{2,3},{3,2},{4,5},{5,4},{6,7},{7,6},{8,9},{9,8},{10,11... | collective-permute-start | bytes 2752520 | tf_op jit(solution)/shard_map/ppermute | solution.py:50
  34.4 1.2 copy-start.6
  36.2 3.6 %copy-start.1 = (f32[2,2,2048]{2,1,0:T(2,128)S(1)}, f32[2,2,2048]{2,1,0:T(2,128)}, u32[]{:S(2)}) copy-start(f32[2,2,2048]{2,1,0:T(2,128)} %gain.9) | copy-start | bytes 98308
  36.3 3.6 %copy-start.4 = (bf16[2,2048,128]{2,1,0:T(8,128)(2,1)S(1)}, bf16[2,2048,128]{2,1,0:T(8,128)(2,1)}, u32[]{:S(2)}) copy-start(bf16[2,2048,128]{2,1,0:T(8,128)(2,1)} %refs_0_.7) | copy-start | bytes 3145732
  36.7 4.3 %copy-start.5 = (f32[2,2,257]{2,1,0:T(2,128)S(1)}, f32[2,2,257]{2,1,0:T(2,128)}, u32[]{:S(2)}) copy-start(f32[2,2,257]{2,1,0:T(2,128)} %bias.3) | copy-start | bytes 12340
  36.7 13.1 %collective-permute-start.5 = (bf16[512,256]{1,0:T(8,128)(2,1)S(1)}, bf16[512,256]{1,0:T(8,128)(2,1)S(1)}, u32[]{:S(2)}, u32[]{:S(2)}) collective-permute-start(bf16[512,256]{1,0:T(8,128)(2,1)S(1)} %get-tuple-element.28.refs_5_), channel_id=1, source_target_pairs={{0,16},{16,32},{32,48},{48,64},{64,80},{80,96},{96,112},{112,128},... | collective-permute-start | bytes 786440 | tf_op jit(solution)/shard_map/ppermute | solution.py:379
  44.4 18.4 %copy-start = (bf16[2,2048,128]{2,1,0:T(8,128)(2,1)S(1)}, bf16[2,2048,128]{2,1,0:T(8,128)(2,1)}, u32[]{:S(2)}) copy-start(bf16[2,2048,128]{2,1,0:T(8,128)(2,1)} %w.7) | copy-start | bytes 3145732
  53.9 10.9 %collective-permute-start.7 = (bf16[2,512,128]{2,1,0:T(8,128)(2,1)S(1)}, bf16[2,512,128]{2,1,0:T(8,128)(2,1)S(1)}, u32[]{:S(2)}, u32[]{:S(2)}) collective-permute-start(bf16[2,512,128]{2,1,0:T(8,128)(2,1)S(1)} %bitcast.7), channel_id=1, source_target_pairs={{0,4},{1,13},{2,6},{3,15},{4,8},{5,1},{6,10},{7,3},{8,12},{9,5},{1... | collective-permute-start | bytes 786440 | tf_op jit(solution)/shard_map/ppermute | solution.py:44
  56.5 15.9 %collective-permute-start.6 = (bf16[2,512,128]{2,1,0:T(8,128)(2,1)S(1)}, bf16[2,512,128]{2,1,0:T(8,128)(2,1)S(1)}, u32[]{:S(2)}, u32[]{:S(2)}) collective-permute-start(bf16[2,512,128]{2,1,0:T(8,128)(2,1)S(1)} %bitcast.8), channel_id=1, source_target_pairs={{0,2},{1,15},{2,4},{3,1},{4,6},{5,3},{6,8},{7,5},{8,10},{9,7},{10,... | collective-permute-start | bytes 786440 | tf_op jit(solution)/shard_map/ppermute | solution.py:45
  62.8 19.8 %collective-permute-start.11 = (bf16[2,2048,128]{2,1,0:T(8,128)(2,1)S(1)}, bf16[2,2048,128]{2,1,0:T(8,128)(2,1)S(1)}, u32[]{:S(2)}, u32[]{:S(2)}) collective-permute-start(bf16[2,2048,128]{2,1,0:T(8,128)(2,1)S(1)} %copy-done), channel_id=1, source_target_pairs={{0,1},{1,0},{2,3},{3,2},{4,5},{5,4},{6,7},{7,6},{8,9},{9,8},{10,11... | collective-permute-start | bytes 3145736 | tf_op jit(solution)/shard_map/ppermute | solution.py:389
  64.7 7.7 %collective-permute-start.8 = (bf16[2,512,128]{2,1,0:T(8,128)(2,1)S(1)}, bf16[2,512,128]{2,1,0:T(8,128)(2,1)S(1)}, u32[]{:S(2)}, u32[]{:S(2)}) collective-permute-start(bf16[2,512,128]{2,1,0:T(8,128)(2,1)S(1)} %collective-permute-done.7), channel_id=1, source_target_pairs={{0,2},{1,15},{2,4},{3,1},{4,6},{5,3},{6,8},{7,5},{8,10},{9,7},{10,... | collective-permute-start | bytes 786440 | tf_op jit(solution)/shard_map/ppermute | solution.py:47
  68.8 8.0 %collective-permute-start.9 = (bf16[1,512,128]{2,1,0:T(8,128)(2,1)S(1)}, bf16[1,512,128]{2,1,0:T(8,128)(2,1)S(1)}, u32[]{:S(2)}, u32[]{:S(2)}) collective-permute-start(bf16[1,512,128]{2,1,0:T(8,128)(2,1)S(1)} %constant_dynamic-slice_fusion.3), channel_id=1, source_target_pairs={{0,4},{1,13},{2,6},{3,15},{4,8},{5,1},{6,10},{7,3},{8,12},{9,5},{1... | collective-permute-start | bytes 393224 | tf_op jit(solution)/shard_map/ppermute | solution.py:48
  76.8 7.9 %collective-permute-start.10 = (bf16[7,512,128]{2,1,0:T(8,128)(2,1)S(1)}, bf16[7,512,128]{2,1,0:T(8,128)(2,1)S(1)}, u32[]{:S(2)}, u32[]{:S(2)}) collective-permute-start(bf16[7,512,128]{2,1,0:T(8,128)(2,1)S(1)} %constant_dynamic-update-slice_fusion.4.received), channel_id=1, source_target_pairs={{0,1},{1,0},{2,3},{3,2},{4,5},{5,4},{6,7},{7,6},{8,9},{9,8},{10,11... | collective-permute-start | bytes 2752520 | tf_op jit(solution)/shard_map/ppermute | solution.py:50
  83.2 27.9 %copy-start.2 = (bf16[2,2048,128]{2,1,0:T(8,128)(2,1)S(1)}, bf16[2,2048,128]{2,1,0:T(8,128)(2,1)}, u32[]{:S(2)}) copy-start(bf16[2,2048,128]{2,1,0:T(8,128)(2,1)} %refs_0_.6) | copy-start | bytes 3145732
  83.2 27.9 %copy-start.3 = (bf16[2,2048,128]{2,1,0:T(8,128)(2,1)S(1)}, bf16[2,2048,128]{2,1,0:T(8,128)(2,1)}, u32[]{:S(2)}) copy-start(bf16[2,2048,128]{2,1,0:T(8,128)(2,1)} %refs_1_.3) | copy-start | bytes 3145732
  85.2 10.1 %collective-permute-start.13 = (bf16[2,512,128]{2,1,0:T(8,128)(2,1)S(1)}, bf16[2,512,128]{2,1,0:T(8,128)(2,1)S(1)}, u32[]{:S(2)}, u32[]{:S(2)}) collective-permute-start(bf16[2,512,128]{2,1,0:T(8,128)(2,1)S(1)} %shard_map.80.own.b_own), channel_id=1, source_target_pairs={{0,4},{1,13},{2,6},{3,15},{4,8},{5,1},{6,10},{7,3},{8,12},{9,5},{1... | collective-permute-start | bytes 786440 | tf_op jit(solution)/shard_map/ppermute | solution.py:44
  89.0 13.2 %collective-permute-start.12 = (bf16[2,512,128]{2,1,0:T(8,128)(2,1)S(1)}, bf16[2,512,128]{2,1,0:T(8,128)(2,1)S(1)}, u32[]{:S(2)}, u32[]{:S(2)}) collective-permute-start(bf16[2,512,128]{2,1,0:T(8,128)(2,1)S(1)} %shard_map.80.own.b_own), channel_id=1, source_target_pairs={{0,2},{1,15},{2,4},{3,1},{4,6},{5,3},{6,8},{7,5},{8,10},{9,7},{10,... | collective-permute-start | bytes 786440 | tf_op jit(solution)/shard_map/ppermute | solution.py:45
  95.2 8.1 %collective-permute-start.14 = (bf16[2,512,128]{2,1,0:T(8,128)(2,1)S(1)}, bf16[2,512,128]{2,1,0:T(8,128)(2,1)S(1)}, u32[]{:S(2)}, u32[]{:S(2)}) collective-permute-start(bf16[2,512,128]{2,1,0:T(8,128)(2,1)S(1)} %collective-permute-done.13), channel_id=1, source_target_pairs={{0,2},{1,15},{2,4},{3,1},{4,6},{5,3},{6,8},{7,5},{8,10},{9,7},{10,... | collective-permute-start | bytes 786440 | tf_op jit(solution)/shard_map/ppermute | solution.py:47
  100.0 7.9 %collective-permute-start.15 = (bf16[1,512,128]{2,1,0:T(8,128)(2,1)S(1)}, bf16[1,512,128]{2,1,0:T(8,128)(2,1)S(1)}, u32[]{:S(2)}, u32[]{:S(2)}) collective-permute-start(bf16[1,512,128]{2,1,0:T(8,128)(2,1)S(1)} %constant_dynamic-slice_fusion.2), channel_id=1, source_target_pairs={{0,4},{1,13},{2,6},{3,15},{4,8},{5,1},{6,10},{7,3},{8,12},{9,5},{1... | collective-permute-start | bytes 393224 | tf_op jit(solution)/shard_map/ppermute | solution.py:48
  108.0 5.2 %collective-permute-start.16 = (bf16[7,512,128]{2,1,0:T(8,128)(2,1)S(1)}, bf16[7,512,128]{2,1,0:T(8,128)(2,1)S(1)}, u32[]{:S(2)}, u32[]{:S(2)}) collective-permute-start(bf16[7,512,128]{2,1,0:T(8,128)(2,1)S(1)} %constant_dynamic-update-slice_fusion.8.received.b_received), channel_id=1, source_target_pairs={{0,1},{1,0},{2,3},{3,2},{4,5},{5,4},{6,7},{7,6},{8,9},{9,8},{10,11... | collective-permute-start | bytes 2752520 | tf_op jit(solution)/shard_map/ppermute | solution.py:50
  115.1 12.7 %collective-permute-start.17 = (bf16[512,256]{1,0:T(8,128)(2,1)S(1)}, bf16[512,256]{1,0:T(8,128)(2,1)S(1)}, u32[]{:S(2)}, u32[]{:S(2)}) collective-permute-start(bf16[512,256]{1,0:T(8,128)(2,1)S(1)} %get-tuple-element.36.refs_3_), channel_id=1, source_target_pairs={{0,16},{16,32},{32,48},{48,64},{64,80},{80,96},{96,112},{112,128},... | collective-permute-start | bytes 786440 | tf_op jit(solution)/shard_map/ppermute | solution.py:379
  132.2 8.9 %collective-permute-start.19 = (bf16[2,512,128]{2,1,0:T(8,128)(2,1)S(1)}, bf16[2,512,128]{2,1,0:T(8,128)(2,1)S(1)}, u32[]{:S(2)}, u32[]{:S(2)}) collective-permute-start(bf16[2,512,128]{2,1,0:T(8,128)(2,1)S(1)} %bitcast.15), channel_id=1, source_target_pairs={{0,4},{1,13},{2,6},{3,15},{4,8},{5,1},{6,10},{7,3},{8,12},{9,5},{1... | collective-permute-start | bytes 786440 | tf_op jit(solution)/shard_map/ppermute | solution.py:44
  135.5 15.5 %collective-permute-start.18 = (bf16[2,512,128]{2,1,0:T(8,128)(2,1)S(1)}, bf16[2,512,128]{2,1,0:T(8,128)(2,1)S(1)}, u32[]{:S(2)}, u32[]{:S(2)}) collective-permute-start(bf16[2,512,128]{2,1,0:T(8,128)(2,1)S(1)} %bitcast.16), channel_id=1, source_target_pairs={{0,2},{1,15},{2,4},{3,1},{4,6},{5,3},{6,8},{7,5},{8,10},{9,7},{10,... | collective-permute-start | bytes 786440 | tf_op jit(solution)/shard_map/ppermute | solution.py:45
  141.2 9.9 %collective-permute-start.20 = (bf16[2,512,128]{2,1,0:T(8,128)(2,1)S(1)}, bf16[2,512,128]{2,1,0:T(8,128)(2,1)S(1)}, u32[]{:S(2)}, u32[]{:S(2)}) collective-permute-start(bf16[2,512,128]{2,1,0:T(8,128)(2,1)S(1)} %collective-permute-done.19), channel_id=1, source_target_pairs={{0,2},{1,15},{2,4},{3,1},{4,6},{5,3},{6,8},{7,5},{8,10},{9,7},{10,... | collective-permute-start | bytes 786440 | tf_op jit(solution)/shard_map/ppermute | solution.py:47
  147.4 7.7 %collective-permute-start.21 = (bf16[1,512,128]{2,1,0:T(8,128)(2,1)S(1)}, bf16[1,512,128]{2,1,0:T(8,128)(2,1)S(1)}, u32[]{:S(2)}, u32[]{:S(2)}) collective-permute-start(bf16[1,512,128]{2,1,0:T(8,128)(2,1)S(1)} %constant_dynamic-slice_fusion.1), channel_id=1, source_target_pairs={{0,4},{1,13},{2,6},{3,15},{4,8},{5,1},{6,10},{7,3},{8,12},{9,5},{1... | collective-permute-start | bytes 393224 | tf_op jit(solution)/shard_map/ppermute | solution.py:48
  155.2 7.9 %collective-permute-start.22 = (bf16[7,512,128]{2,1,0:T(8,128)(2,1)S(1)}, bf16[7,512,128]{2,1,0:T(8,128)(2,1)S(1)}, u32[]{:S(2)}, u32[]{:S(2)}) collective-permute-start(bf16[7,512,128]{2,1,0:T(8,128)(2,1)S(1)} %constant_dynamic-update-slice_fusion.12.received), channel_id=1, source_target_pairs={{0,1},{1,0},{2,3},{3,2},{4,5},{5,4},{6,7},{7,6},{8,9},{9,8},{10,11... | collective-permute-start | bytes 2752520 | tf_op jit(solution)/shard_map/ppermute | solution.py:50
  164.2 13.6 %all-to-all-start = ((f32[16,4,128]{2,1,0:T(4,128)}), f32[16,4,128]{2,1,0:T(4,128)S(1)}, u32[]{:S(2)}, u32[]{:S(2)}) async-start(f32[16,4,128]{2,1,0:T(4,128)} %get-tuple-element.42), calls=%async_computation | async-start | bytes 65536 | tf_op jit(solution)/shard_map/all_to_all | solution.py:433
